TPU v7x, 512 devices: a whole 4x8x8 slice. The times are simulated.
512 devices in a mesh: sp: 128 (over z, y, core), tp: 4 (over x).
Axes of the slice: x: 4, y: 8, z: 8, core: 2. Of those that a mesh axis runs over, the one named last changes fastest.
Arguments:
- tokens: bfloat16 [32768, 2048], P(('sp', 'tp')), may hold values from -6 to 6
- pre_gain: float32 [2048], replicated, may hold values from 0.1 to 1.9
- w_query_ret: bfloat16 [2048, 768], P('sp', 'tp'), may hold values from -0.125 to 0.125
- w_key_ret: bfloat16 [2048, 768], P('sp', 'tp'), may hold values from -0.125 to 0.125
- w_value_ret: bfloat16 [2048, 768], P('sp', 'tp'), may hold values from -0.125 to 0.125
- w_query_att: bfloat16 [2048, 768], P('sp', 'tp'), may hold values from -0.5 to 0.5
- w_key_att: bfloat16 [2048, 256], P('sp', 'tp'), may hold values from -0.125 to 0.125
- w_value_att: bfloat16 [2048, 256], P('sp', 'tp'), may hold values from -0.125 to 0.125
- w_out_ret: bfloat16 [768, 2048], P('tp', 'sp'), may hold values from -0.15625 to 0.15625
- w_out_att: bfloat16 [768, 2048], P('tp', 'sp'), may hold values from -0.15625 to 0.15625
- retain_log: float32 [32768, 12], P('sp', 'tp')
- forget_total: float32 [12, 32768], P('tp'), as said below
Outputs:
- mixed: bfloat16 [32768, 2048], P(('sp', 'tp'))
Inputs may be any that keep to these rules, and one draw needn't show every extreme that they name: `forget_total`: never rises along positions.
All inputs are finite; a program needn't handle non-finite values.
Results may differ from a plain program's by a relative error of at most 0.019.
Values may be sent and summed in bfloat16 or wider, within the bound.
No kernel may reach another device: no remote copies, remote signals or barrier semaphores. Data moves between devices by JAX's collectives and lax.ppermute only.
A program may use at most 64 MiB of HBM per device.

v0:
```python
import jax
import jax.numpy as jnp
from jax import lax
from jax.experimental import pallas as pl
from jax.experimental.pallas import tpu as pltpu
from jax.sharding import Mesh
from jax.sharding import PartitionSpec as P

HEAD = 64
SPAN = 256
SP = ("z", "y", "c")
EPS = 1e-06
THETA = 10000.0
LOG2E = 1.4426950408889634
F32 = jnp.float32
BF16 = jnp.bfloat16
SKEW = [[((m - y) % 8) * 8 + y for y in range(8)] for m in range(8)]
NT = (((1,), (1,)), ((), ()))
TN = (((0,), (0,)), ((), ()))
VMEM = pl.BlockSpec(memory_space=pltpu.VMEM)
SMEM = pl.BlockSpec(memory_space=pltpu.SMEM)
PARAMS = pltpu.CompilerParams(vmem_limit_bytes=56 * 1024 * 1024)


def copies_from(shard, axis, groups=None):
    count = len(groups[0]) if groups else lax.axis_size(axis)
    copies = jnp.broadcast_to(shard, (count, *shard.shape))
    return lax.all_to_all(
        copies, axis, split_axis=0, concat_axis=0, tiled=True, axis_index_groups=groups
    )


def swapped_cores(value):
    return lax.ppermute(value, "c", [(0, 1), (1, 0)])


def three_parts(values):
    high = lax.reduce_precision(values, 8, 7)
    rest = values - high
    middle = lax.reduce_precision(rest, 8, 7)
    low = lax.reduce_precision(rest - middle, 8, 7)
    return [part.astype(BF16) for part in (high, middle, low)]


def front_kernel(
    rows, w_own, w_oth, cosine, sine, decay, decay_row, q_out, kv_out, local_out, lifted_out, state_out, proj
):
    proj[...] = jnp.dot(
        rows[:, 0].reshape(SPAN, -1), w_own[...], preferred_element_type=F32
    ) + jnp.dot(rows[:, 1].reshape(SPAN, -1), w_oth[...], preferred_element_type=F32)
    cos = cosine[...]
    sin = sine[...]
    place = lax.broadcasted_iota(jnp.int32, (SPAN, SPAN), 0)
    other = lax.broadcasted_iota(jnp.int32, (SPAN, SPAN), 1)
    causal = place >= other

    def turned(at):
        first = proj[:, at : at + 32]
        second = proj[:, at + 32 : at + 64]
        return jnp.concatenate(
            [first * cos - second * sin, first * sin + second * cos], axis=1
        )

    for h in range(3):
        query = (turned(h * HEAD) * HEAD ** (-0.5)).astype(BF16)
        key = turned(192 + h * HEAD).astype(BF16)
        value = proj[:, 384 + h * HEAD : 384 + (h + 1) * HEAD].astype(BF16)
        column = decay[:, h : h + 1]
        row = decay_row[h : h + 1, :]
        last = decay[SPAN - 1 : SPAN, h : h + 1]
        scores = lax.dot_general(query, key, NT, preferred_element_type=F32)
        gap = jnp.where(causal, column - row, 0.0)
        weights = jnp.where(causal, scores * jnp.exp(gap), 0.0).astype(BF16)
        local_out[:, h * HEAD : (h + 1) * HEAD] = jnp.dot(
            weights, value, preferred_element_type=F32
        )
        faded = (key.astype(F32) * jnp.exp(last - column)).astype(BF16)
        update = lax.dot_general(faded, value, TN, preferred_element_type=F32)
        state_out[(h // 2) * HEAD : (h // 2 + 1) * HEAD, (h % 2) * HEAD : (h % 2 + 1) * HEAD] = (
            update.astype(BF16)
        )
        lifted_out[:, h * HEAD : (h + 1) * HEAD] = (
            query.astype(F32) * jnp.exp(column)
        ).astype(BF16)
    ends = decay_row[:, SPAN - 1 : SPAN]
    high = ends.astype(BF16).astype(F32)
    middle = (ends - high).astype(BF16).astype(F32)
    low = ends - high - middle
    lane = lax.broadcasted_iota(jnp.int32, (8, HEAD), 1)
    tail = jnp.where(lane == 0, high, jnp.where(lane == 1, middle, jnp.where(lane == 2, low, 0.0)))
    state_out[HEAD:, HEAD:] = jnp.concatenate(
        [tail, jnp.zeros((HEAD - 8, HEAD), F32)], axis=0
    ).astype(BF16)
    q_out[...] = jnp.transpose(proj[:, 576:768] * (HEAD ** (-0.5) * LOG2E)).astype(BF16)
    both = proj[:, 768:896]
    flipped = jnp.transpose(both)[HEAD:, :].astype(BF16)
    kv_out[:128] = jnp.concatenate([both[:128, :HEAD], both[128:, :HEAD]], axis=1).astype(BF16)
    kv_out[128:] = jnp.concatenate([flipped[:, :128], flipped[:, 128:]], axis=0)


def attend_kernel(
    plan, query, kv_own, kv_oth, key_gate, query_gate, out, keys, values, queries, total
):
    extra = lax.broadcasted_iota(jnp.int32, (16, 2 * SPAN), 0)
    ones = jnp.where(extra == 0, 1.0, 0.0).astype(BF16)
    for y in range(8):
        for side, held in enumerate((kv_own, kv_oth)):
            packed = held[y, :128]
            at = side * SPAN
            keys[y, at : at + 128, :HEAD] = packed[:, :HEAD]
            keys[y, at + 128 : at + SPAN, :HEAD] = packed[:, HEAD:]
            keys[y, at : at + SPAN, HEAD:] = key_gate[side, y]
            values[y, :HEAD, at : at + 128] = held[y, 128:192]
            values[y, :HEAD, at + 128 : at + SPAN] = held[y, 192:]
        values[y, HEAD:, :] = ones
    for z in range(8):
        for h in range(3):
            queries[z, :HEAD, h * SPAN : (h + 1) * SPAN] = query[z, h * HEAD : (h + 1) * HEAD]
        queries[z, HEAD:, :] = query_gate[z]
    total[...] = jnp.zeros_like(total)
    mine_z, mine_y, mine_c = (plan[65], plan[66], plan[67])

    scores = jnp.dot(keys[mine_y], queries[mine_z], preferred_element_type=F32)
    place = lax.broadcasted_iota(jnp.int32, (2 * SPAN, 3 * SPAN), 0)
    wanted = lax.broadcasted_iota(jnp.int32, (2 * SPAN, 3 * SPAN), 1) % SPAN
    limit = jnp.where(place < SPAN, wanted, mine_c * (4 * SPAN) - 1)
    weights = jnp.where(place <= limit, jnp.exp2(scores), 0.0).astype(BF16)
    total[mine_z] += jnp.dot(values[mine_y], weights, preferred_element_type=F32)

    def unit(i, carry):
        code = plan[i]
        z = code // 8
        y = code % 8
        weights = jnp.exp2(
            jnp.dot(keys[y], queries[z], preferred_element_type=F32)
        ).astype(BF16)
        total[z] += jnp.dot(values[y], weights, preferred_element_type=F32)
        return carry

    lax.fori_loop(0, plan[64], unit, 0)
    for z in range(8):
        rows = []
        for h in range(3):
            out[z, h * HEAD : (h + 1) * HEAD] = total[z, :HEAD, h * SPAN : (h + 1) * SPAN].astype(
                BF16
            )
            rows.append(total[z, HEAD : HEAD + 1, h * SPAN : (h + 1) * SPAN])
        high = [row.astype(BF16).astype(F32) for row in rows]
        low = [row - big for row, big in zip(rows, high)]
        out[z, 192:] = jnp.concatenate(high + low + [jnp.zeros((10, SPAN), F32)], axis=0).astype(
            BF16
        )


def combine_kernel(states, above, below, out):
    def add(j, carry):
        upper, lower = carry
        upper = upper + states[j, :HEAD].astype(F32) * above[pl.ds(j, 1), :]
        lower = lower + states[j, HEAD:].astype(F32) * below[pl.ds(j, 1), :]
        return (upper, lower)

    zero = jnp.zeros((HEAD, 128), F32)
    upper, lower = lax.fori_loop(0, states.shape[0], add, (zero, zero))
    out[:HEAD] = upper.astype(BF16)
    out[HEAD:] = lower.astype(BF16)


def back_kernel(parts, local, lifted, state, w_out, out, mixed):
    total = parts[0].astype(F32)
    for z in range(1, 8):
        total = total + parts[z].astype(F32)
    for h in range(3):
        held = state[
            (h // 2) * HEAD : (h // 2 + 1) * HEAD, (h % 2) * HEAD : (h % 2 + 1) * HEAD
        ]
        raw = local[:, h * HEAD : (h + 1) * HEAD] + jnp.dot(
            lifted[:, h * HEAD : (h + 1) * HEAD], held, preferred_element_type=F32
        )
        centred = raw - jnp.mean(raw, axis=-1, keepdims=True)
        spread = jnp.mean(centred * centred, axis=-1, keepdims=True)
        mixed[:, h * HEAD : (h + 1) * HEAD] = (centred * lax.rsqrt(spread + EPS)).astype(BF16)
        weight = total[192 + h : 193 + h] + total[195 + h : 196 + h]
        attended = total[h * HEAD : (h + 1) * HEAD] / weight
        mixed[:, 192 + h * HEAD : 192 + (h + 1) * HEAD] = jnp.transpose(attended).astype(BF16)
    out[...] = lax.dot_general(
        mixed[...], w_out[...], NT, preferred_element_type=F32
    ).astype(BF16)


def body(
    tokens,
    pre_gain,
    w_query_ret,
    w_key_ret,
    w_value_ret,
    w_query_att,
    w_key_att,
    w_value_att,
    w_out_ret,
    w_out_att,
    retain_log,
    forget_total,
):
    z, y, c = (lax.axis_index("z"), lax.axis_index("y"), lax.axis_index("c"))
    shard = jnp.concatenate(
        [
            w_query_ret,
            w_key_ret,
            w_value_ret,
            w_query_att,
            w_key_att,
            w_value_att,
            w_out_ret.T,
            w_out_att.T,
        ],
        axis=1,
    )
    width = shard.shape[1]
    w_row = copies_from(shard, "y").reshape(-1, width)
    w_own = lax.all_gather(w_row, "z", axis=0, tiled=True)
    w_oth = swapped_cores(w_own)

    raw = tokens.astype(F32)
    normed = (
        raw * lax.rsqrt(jnp.mean(raw * raw, axis=-1, keepdims=True) + EPS) * pre_gain
    ).astype(BF16)
    halves = jnp.transpose(normed.reshape(64, 64, 2, 16), (2, 0, 1, 3)).reshape(2, 64, 1024)
    halves = jnp.where(c == 0, halves, halves[::-1])
    rows = copies_from(halves, "tp")

    here = z * 16 + y * 2 + c
    positions = (here * SPAN + jnp.arange(SPAN, dtype=jnp.int32)).astype(F32)
    inverse = THETA ** (-jnp.arange(32, dtype=F32) / 32)
    angles = positions[:, None] * inverse[None, :]
    cosine, sine = (jnp.cos(angles), jnp.sin(angles))
    decay = jnp.cumsum(retain_log, axis=0)
    decay_row = jnp.pad(decay.T, ((0, 5), (0, 0)))

    gate = (forget_total * LOG2E).reshape(3, 8, 8, 2, SPAN)
    spans = jnp.arange(8, dtype=jnp.int32)
    key_z = (z + y - spans) % 8
    chosen = (spans[:, None] == key_z[None, :])[None, :, :, None, None]
    key_side = jnp.sum(jnp.where(chosen, gate, 0.0), axis=1)
    key_side = jnp.where(c == 0, key_side, key_side[:, :, ::-1])
    minus = jnp.stack(three_parts(-key_side), axis=1).reshape(9, 8, 2, SPAN)
    key_gate = jnp.concatenate(
        [minus, jnp.ones((3, 8, 2, SPAN), BF16), jnp.zeros((52, 8, 2, SPAN), BF16)], axis=0
    )
    key_gate = jnp.transpose(key_gate, (2, 1, 3, 0))
    mine = lax.dynamic_index_in_dim(
        lax.dynamic_index_in_dim(gate, y, 2, keepdims=False), c, 2, keepdims=False
    )
    plus = jnp.stack(three_parts(mine), axis=0)
    plus = jnp.transpose(plus, (2, 0, 1, 3)).reshape(8, 3, 3 * SPAN)
    own_head = (
        (jnp.arange(9)[:, None] // 3) == (jnp.arange(3 * SPAN)[None, :] // SPAN)
    ).astype(BF16)
    query_gate = jnp.concatenate(
        [
            jnp.broadcast_to(own_head, (8, 9, 3 * SPAN)),
            plus,
            jnp.zeros((8, 52, 3 * SPAN), BF16),
        ],
        axis=1,
    )
    needed = (
        (key_z[None, :] < spans[:, None])
        | ((key_z[None, :] == spans[:, None]) & (spans[None, :] < y))
    ).reshape(64)
    slot = jnp.cumsum(needed.astype(jnp.int32)) - 1
    order = jnp.arange(64, dtype=jnp.int32)
    units = jnp.sum(
        jnp.where(needed[None, :] & (slot[None, :] == order[:, None]), order[None, :], 0), axis=1
    )
    plan = jnp.concatenate([units, jnp.stack([jnp.sum(needed.astype(jnp.int32)), z, y, c])])

    q_send, kv_send, local, lifted, state = pl.pallas_call(
        front_kernel,
        grid=(1,),
        in_specs=[
            VMEM,
            pl.BlockSpec((1024, 896), lambda i: (0, 0)),
            pl.BlockSpec((1024, 896), lambda i: (0, 0)),
            VMEM,
            VMEM,
            VMEM,
            VMEM,
        ],
        out_specs=[VMEM] * 5,
        out_shape=[
            jax.ShapeDtypeStruct((192, SPAN), BF16),
            jax.ShapeDtypeStruct((SPAN, 128), BF16),
            jax.ShapeDtypeStruct((SPAN, 192), F32),
            jax.ShapeDtypeStruct((SPAN, 192), BF16),
            jax.ShapeDtypeStruct((128, 128), BF16),
        ],
        scratch_shapes=[pltpu.VMEM((SPAN, 896), F32)],
        compiler_params=PARAMS,
        name="front",
    )(rows, w_own, w_oth, cosine, sine, decay, decay_row)

    states = lax.all_gather(state, SP, axis=0)
    kv_own = copies_from(kv_send, ("z", "y"), SKEW)
    kv_oth = swapped_cores(kv_own)
    queries = copies_from(q_send, "z")

    partial = pl.pallas_call(
        attend_kernel,
        in_specs=[SMEM, VMEM, VMEM, VMEM, VMEM, VMEM],
        out_specs=VMEM,
        out_shape=jax.ShapeDtypeStruct((8, 208, SPAN), BF16),
        scratch_shapes=[
            pltpu.VMEM((8, 2 * SPAN, 128), BF16),
            pltpu.VMEM((8, 80, 2 * SPAN), BF16),
            pltpu.VMEM((8, 128, 3 * SPAN), BF16),
            pltpu.VMEM((8, 80, 3 * SPAN), F32),
        ],
        compiler_params=PARAMS,
        name="attend",
    )(plan, queries, kv_own, kv_oth, key_gate, query_gate)
    parts = lax.all_to_all(partial, "z", 0, 0, tiled=True)

    ends = jnp.sum(states[:, HEAD : HEAD + 3, HEAD : HEAD + 3].astype(F32), axis=-1)
    index = jnp.arange(128, dtype=jnp.int32)
    between = (index[None, :] > index[:, None]) & (index[None, :] < here)
    span_log = jnp.sum(jnp.where(between[:, :, None], ends[None], 0.0), axis=1)
    factor = jnp.where((index < here)[:, None], jnp.exp(span_log), 0.0)
    above = jnp.repeat(factor[:, :2], HEAD, axis=1)
    below = jnp.pad(jnp.repeat(factor[:, 2:], HEAD, axis=1), ((0, 0), (0, HEAD)))
    incoming = pl.pallas_call(
        combine_kernel,
        in_specs=[VMEM] * 3,
        out_specs=VMEM,
        out_shape=jax.ShapeDtypeStruct((128, 128), BF16),
        compiler_params=PARAMS,
        name="combine",
    )(states, above, below)

    out_own = w_own[:, 896:].reshape(64, 16, 384)
    out_oth = w_oth[:, 896:].reshape(64, 16, 384)
    w_out = jnp.where(
        c == 0, jnp.stack([out_own, out_oth], axis=1), jnp.stack([out_oth, out_own], axis=1)
    ).reshape(2048, 384)
    share = pl.pallas_call(
        back_kernel,
        in_specs=[VMEM] * 5,
        out_specs=VMEM,
        out_shape=jax.ShapeDtypeStruct((SPAN, 2048), BF16),
        scratch_shapes=[pltpu.VMEM((SPAN, 384), BF16)],
        compiler_params=PARAMS,
        name="back",
    )(parts, local, lifted, incoming, w_out)
    shares = lax.all_to_all(share.reshape(4, 64, 2048), "tp", 0, 0, tiled=True)
    return jnp.sum(shares.astype(F32), axis=0).astype(BF16)


def solution(mesh):
    finer = Mesh(mesh.devices.reshape(8, 8, 2, mesh.shape["tp"]), ("z", "y", "c", "tp"))
    everyone = ("z", "y", "c", "tp")
    placed = (
        P(everyone, None),
        P(),
        P(SP, "tp"),
        P(SP, "tp"),
        P(SP, "tp"),
        P(SP, "tp"),
        P(SP, "tp"),
        P(SP, "tp"),
        P("tp", SP),
        P("tp", SP),
        P(SP, "tp"),
        P("tp", None),
    )
    return jax.shard_map(
        body, mesh=finer, in_specs=placed, out_specs=P(everyone, None), check_vma=False
    )
```

profile of v0, /device:TPU:16, one launch (start us, length us, event | category | flops | bytes accessed | tf_op | source)
XLA Modules:
  0.0 249.3 jit_solution(11980857057770099307)
XLA Ops:
  7.5 18.0 %all_to_all.30 = bf16[8,16,1280]{2,1,0:T(8,128)(2,1)} all-to-all(bf16[8,16,1280]{2,1,0:T(8,128)(2,1)S(1)} %broadcast_in_dim.110), channel_id=1, replica_groups=mesh['z'=8,'y'=8,'c'=2,'tp'=4] {'y'}, dimensions={0} | all-to-all | bytes 655360 | tf_op jit(solution)/shard_map/all_to_all | solution.py:28
  25.6 47.0 %all-gather.4.cloned.1.call-done.w_own = bf16[1024,1280]{1,0:T(8,128)(2,1)} async-done(((bf16[128,1280]{1,0:T(8,128)(2,1)}), bf16[1024,1280]{1,0:T(8,128)(2,1)}) %all-gather.4.cloned.1.call-update) | async-done | bytes 2621456 | tf_op jit(solution)/shard_map/all_gather | solution.py:220
  72.6 1.9 collective-permute-start
  78.8 4.2 %all-to-all-start = ((bf16[4,2,64,1024]{3,2,1,0:T(8,128)(2,1)}), bf16[4,2,64,1024]{3,2,1,0:T(8,128)(2,1)}, u32[]{:S(2)}, u32[]{:S(2)}) async-start(bf16[4,2,64,1024]{3,2,1,0:T(8,128)(2,1)} %broadcast_in_dim.109), calls=%async_computation | async-start | bytes 2097152 | tf_op jit(solution)/shard_map/all_to_all | solution.py:28
  87.2 12.0 %all-to-all-done.rows = bf16[4,2,64,1024]{3,2,1,0:T(8,128)(2,1)} async-done(((bf16[4,2,64,1024]{3,2,1,0:T(8,128)(2,1)}), bf16[4,2,64,1024]{3,2,1,0:T(8,128)(2,1)}, u32[]{:S(2)}, u32[]{:S(2)}) %all-to-all-start) | async-done | bytes 1048608 | tf_op jit(solution)/shard_map/all_to_all | solution.py:28
  99.2 1.5 copy-done
  100.7 5.5 %front.1 = (bf16[192,256]{1,0:T(8,128)(2,1)}, bf16[256,128]{1,0:T(8,128)(2,1)}, f32[256,192]{1,0:T(8,128)}, bf16[256,192]{1,0:T(8,128)(2,1)}, bf16[128,128]{1,0:T(8,128)(2,1)}) custom-call(bf16[4,2,64,1024]{3,2,1,0:T(8,128)(2,1)} %all-to-all-done.rows, bf16[1024,1280]{1,0:T(8,128)(2,1)} %all-gather.4.cloned.1.call-done.w_own, bf16[1024,1280]{1,0:T(8,128)(2,1)} %copy-done, ...), custom_call_target="tpu_custom_call" | custom-call | tf_op jit(solution)/shard_map/front/pallas_call | solution.py:277
  107.5 1.7 broadcast_in_dim.112
  109.2 10.9 %all-to-all-start.3 = ((bf16[8,256,128]{2,1,0:T(8,128)(2,1)}), bf16[8,256,128]{2,1,0:T(8,128)(2,1)S(1)}, u32[]{:S(2)}, u32[]{:S(2)}) async-start(bf16[8,256,128]{2,1,0:T(8,128)(2,1)} %broadcast_in_dim.112), calls=%async_computation.3 | async-start | bytes 1048576 | tf_op jit(solution)/shard_map/all_to_all | solution.py:28
  121.2 17.8 %all-to-all-done.3.kv_own = bf16[8,256,128]{2,1,0:T(8,128)(2,1)S(1)} async-done(((bf16[8,256,128]{2,1,0:T(8,128)(2,1)}), bf16[8,256,128]{2,1,0:T(8,128)(2,1)S(1)}, u32[]{:S(2)}, u32[]{:S(2)}) %all-to-all-start.3) | async-done | bytes 524320 | tf_op jit(solution)/shard_map/all_to_all | solution.py:28
  140.0 6.3 %all-to-all-start.2 = ((bf16[8,192,256]{2,1,0:T(8,128)(2,1)}), bf16[8,192,256]{2,1,0:T(8,128)(2,1)S(1)}, u32[]{:S(2)}, u32[]{:S(2)}) async-start(bf16[8,192,256]{2,1,0:T(8,128)(2,1)} %broadcast_in_dim.111), calls=%async_computation.2 | async-start | bytes 1572864 | tf_op jit(solution)/shard_map/all_to_all | solution.py:28
  146.6 1.9 collective-permute-start.1
  149.9 1.3 concatenate.12.plan
  152.2 1.3 maximum_bitcast_fusion.key_gate
  153.5 13.4 %all-to-all-done.2.query = bf16[8,192,256]{2,1,0:T(8,128)(2,1)S(1)} async-done(((bf16[8,192,256]{2,1,0:T(8,128)(2,1)}), bf16[8,192,256]{2,1,0:T(8,128)(2,1)S(1)}, u32[]{:S(2)}, u32[]{:S(2)}) %all-to-all-start.2) | async-done | bytes 786464 | tf_op jit(solution)/shard_map/all_to_all | solution.py:28
  168.6 20.7 %attend.1 = bf16[8,208,256]{2,1,0:T(8,128)(2,1)} custom-call(s32[68]{0:T(128)} %concatenate.12.plan, bf16[8,192,256]{2,1,0:T(8,128)(2,1)} %copy-done.2, bf16[8,256,128]{2,1,0:T(8,128)(2,1)} %copy-done.3, bf16[8,256,128]{2,1,0:T(8,128)(2,1)} %copy-done.4, bf16[2,8,256,64]{3,2,1,0:T(8,128)(2,1)} %maximum_bitcast_fusion.key_gate, ...), custom_call_target="tpu_custom_call" | custom-call | tf_op jit(solution)/shard_map/attend/pallas_call | solution.py:307
  189.2 3.5 %all-to-all-start.4 = ((bf16[8,208,256]{2,1,0:T(8,128)(2,1)}), bf16[8,208,256]{2,1,0:T(8,128)(2,1)S(1)}, u32[]{:S(2)}, u32[]{:S(2)}) async-start(bf16[8,208,256]{2,1,0:T(8,128)(2,1)} %attend.1), calls=%async_computation.4 | async-start | bytes 1703936 | tf_op jit(solution)/shard_map/all_to_all | solution.py:321
  192.8 1.3 slice.33
  194.3 1.4 maximum_select_fusion
  195.7 4.0 %all-gather.6.cloned.1.call-done = bf16[16384,128]{1,0:T(8,128)(2,1)} async-done(((bf16[128,128]{1,0:T(8,128)(2,1)}), bf16[16384,128]{1,0:T(8,128)(2,1)}) %all-gather.6.cloned.1.call-update) | async-done | bytes 4194320 | tf_op jit(solution)/shard_map/all_gather | solution.py:302
  202.6 4.2 %combine.1.state = bf16[128,128]{1,0:T(8,128)(2,1)} custom-call(bf16[128,128,128]{2,1,0:T(8,128)(2,1)} %bitcast.57, f32[128,128]{1,0:T(8,128)} %copy.112.above, f32[128,128]{1,0:T(8,128)} %pad.9.below), custom_call_target="tpu_custom_call" | custom-call | tf_op jit(solution)/shard_map/combine/pallas_call | solution.py:330
  206.9 8.1 %all-to-all-done.4.parts = bf16[8,208,256]{2,1,0:T(8,128)(2,1)S(1)} async-done(((bf16[8,208,256]{2,1,0:T(8,128)(2,1)}), bf16[8,208,256]{2,1,0:T(8,128)(2,1)S(1)}, u32[]{:S(2)}, u32[]{:S(2)}) %all-to-all-start.4) | async-done | bytes 852000 | tf_op jit(solution)/shard_map/all_to_all | solution.py:321
  215.9 4.9 %back.1 = bf16[256,2048]{1,0:T(8,128)(2,1)} custom-call(bf16[8,208,256]{2,1,0:T(8,128)(2,1)} %copy-done.1, f32[256,192]{1,0:T(8,128)} %get-tuple-element.12.local, bf16[256,192]{1,0:T(8,128)(2,1)} %get-tuple-element.13.lifted, bf16[128,128]{1,0:T(8,128)(2,1)} %combine.1.state, bf16[2048,384]{1,0:T(8,128)(2,1)} %bitcast.55), custom_call_target="tpu_custom_call" | custom-call | tf_op jit(solution)/shard_map/back/pallas_call | solution.py:344
  220.8 20.7 %all_to_all.31 = bf16[4,64,2048]{2,1,0:T(8,128)(2,1)S(1)} all-to-all(bf16[4,64,2048]{2,1,0:T(8,128)(2,1)} %bitcast.59), channel_id=1, replica_groups=mesh['z'=8,'y'=8,'c'=2,'tp'=4] {'tp'}, dimensions={0} | all-to-all | bytes 2097152 | tf_op jit(solution)/shard_map/all_to_all | solution.py:353
  (93 shorter events, 21.8 us)
Async XLA Ops:
  6.5 68.0 %copy-start.5 = (bf16[64,2048]{1,0:T(8,128)(2,1)S(1)}, bf16[64,2048]{1,0:T(8,128)(2,1)}, u32[]{:S(2)}) copy-start(bf16[64,2048]{1,0:T(8,128)(2,1)} %param.12) | copy-start | bytes 786436
  6.5 68.6 %copy-start.7 = (f32[2048]{0:T(1024)S(1)}, f32[2048]{0:T(1024)}, u32[]{:S(2)}) copy-start(f32[2048]{0:T(1024)} %param.13) | copy-start | bytes 24580
  6.5 66.1 %all-gather.4.cloned.1.call-start = ((), (), s32[]{:S(2)}) async-start(), calls=%async_computation.6 | async-start | bytes 2949120 | tf_op jit(solution)/shard_map/all_gather | solution.py:220
  72.6 26.6 %collective-permute-start = (bf16[1024,1280]{1,0:T(8,128)(2,1)}, bf16[1024,1280]{1,0:T(8,128)(2,1)S(1)}, u32[]{:S(2)}, u32[]{:S(2)}) collective-permute-start(bf16[1024,1280]{1,0:T(8,128)(2,1)} %all-gather.4.cloned.1.call-done.w_own), channel_id=1, source_target_pairs={{0,4},{4,0},{1,5},{5,1},{2,6},{6,2},{3,7},{7,3},{8,12},{12,8},{9,1... | collective-permute-start | bytes 7864328 | tf_op jit(solution)/shard_map/ppermute | solution.py:34
  77.6 5.5 %copy-start.8 = (f32[256,3]{0,1:T(4,128)S(1)}, f32[256,3]{0,1:T(4,128)}, u32[]{:S(2)}) copy-start(f32[256,3]{0,1:T(4,128)} %param.22) | copy-start | bytes 9220
  78.8 20.3 %all-to-all-start = ((bf16[4,2,64,1024]{3,2,1,0:T(8,128)(2,1)}), bf16[4,2,64,1024]{3,2,1,0:T(8,128)(2,1)}, u32[]{:S(2)}, u32[]{:S(2)}) async-start(bf16[4,2,64,1024]{3,2,1,0:T(8,128)(2,1)} %broadcast_in_dim.109), calls=%async_computation | async-start | bytes 2097152 | tf_op jit(solution)/shard_map/all_to_all | solution.py:28
  83.1 116.6 %all-gather.6.cloned.1.call-start = ((), (), s32[]{:S(2)}) async-start(), calls=%async_computation.7 | async-start | bytes 4227072 | tf_op jit(solution)/shard_map/all_gather | solution.py:302
  99.2 1.5 copy-start
  109.2 29.8 %copy-start.6 = (bf16[192,256]{1,0:T(8,128)(2,1)S(1)}, bf16[192,256]{1,0:T(8,128)(2,1)}, u32[]{:S(2)}) copy-start(bf16[192,256]{1,0:T(8,128)(2,1)} %get-tuple-element.10) | copy-start | bytes 294916
  109.2 29.8 %all-to-all-start.3 = ((bf16[8,256,128]{2,1,0:T(8,128)(2,1)}), bf16[8,256,128]{2,1,0:T(8,128)(2,1)S(1)}, u32[]{:S(2)}, u32[]{:S(2)}) async-start(bf16[8,256,128]{2,1,0:T(8,128)(2,1)} %broadcast_in_dim.112), calls=%async_computation.3 | async-start | bytes 1048576 | tf_op jit(solution)/shard_map/all_to_all | solution.py:28
  139.0 10.8 %copy-start.3 = (bf16[8,256,128]{2,1,0:T(8,128)(2,1)}, bf16[8,256,128]{2,1,0:T(8,128)(2,1)S(1)}, u32[]{:S(2)}) copy-start(bf16[8,256,128]{2,1,0:T(8,128)(2,1)S(1)} %all-to-all-done.3.kv_own) | copy-start | bytes 1572868
  140.0 26.9 %all-to-all-start.2 = ((bf16[8,192,256]{2,1,0:T(8,128)(2,1)}), bf16[8,192,256]{2,1,0:T(8,128)(2,1)S(1)}, u32[]{:S(2)}, u32[]{:S(2)}) async-start(bf16[8,192,256]{2,1,0:T(8,128)(2,1)} %broadcast_in_dim.111), calls=%async_computation.2 | async-start | bytes 1572864 | tf_op jit(solution)/shard_map/all_to_all | solution.py:28
  146.6 20.3 %collective-permute-start.1 = (bf16[8,256,128]{2,1,0:T(8,128)(2,1)S(1)}, bf16[8,256,128]{2,1,0:T(8,128)(2,1)S(1)}, u32[]{:S(2)}, u32[]{:S(2)}) collective-permute-start(bf16[8,256,128]{2,1,0:T(8,128)(2,1)S(1)} %all-to-all-done.3.kv_own), channel_id=1, source_target_pairs={{0,4},{4,0},{1,5},{5,1},{2,6},{6,2},{3,7},{7,3},{8,12},{12,8},{9,1... | collective-permute-start | bytes 1572872 | tf_op jit(solution)/shard_map/ppermute | solution.py:34
  166.9 0.9 copy-start.2
  167.8 0.8 copy-start.4
  189.2 25.7 %all-to-all-start.4 = ((bf16[8,208,256]{2,1,0:T(8,128)(2,1)}), bf16[8,208,256]{2,1,0:T(8,128)(2,1)S(1)}, u32[]{:S(2)}, u32[]{:S(2)}) async-start(bf16[8,208,256]{2,1,0:T(8,128)(2,1)} %attend.1), calls=%async_computation.4 | async-start | bytes 1703936 | tf_op jit(solution)/shard_map/all_to_all | solution.py:321
  192.8 1.5 slice-start
  214.9 0.9 copy-start.1
Sparse Core Ops, SparseCore 0:
  25.7 46.8 all-gather.3
  106.4 93.2 all-gather.5
where the time goes:
time: 250 us; the launch traced here: 249 us
  waiting for transfers between devices  102 us (41%)
  blocking collectives  38.8 us (16%)
  Pallas kernels  35.4 us (14%)
  starting transfers between devices  28.8 us (12%)
  local copies, waits for them, and re-layouts  17.8 us (7%)
  between operations  13.7 us (5%)
  other arithmetic  12.5 us (5%)
    all_gather x1, waiting for transfers between devices, body(): w_own = lax.all_gather(w_row, 'z', axis=0, tiled=True)  47 us
    all_to_all x3, waiting for transfers between devices, copies_from(): lax.all_to_all(copies, axis, split_axis=0, concat_axis=0, tiled=True, axi...  43.2 us
    all_to_all x3, starting transfers between devices, copies_from(): lax.all_to_all(copies, axis, split_axis=0, concat_axis=0, tiled=True, axi...  21.4 us
    all_to_all x1, blocking collectives, body(): shares = lax.all_to_all(share.reshape(4, 64, 2048), 'tp', 0, 0, tiled=True)  20.7 us
    pallas_call x1, Pallas kernels, body(): pl.pallas_call(attend_kernel, in_specs=[SMEM, VMEM, VMEM, VMEM, VMEM, VME...  20.7 us
    all_to_all x1, blocking collectives, copies_from(): lax.all_to_all(copies, axis, split_axis=0, concat_axis=0, tiled=True, axi...  18 us
    all_to_all x1, waiting for transfers between devices, body(): parts = lax.all_to_all(partial, 'z', 0, 0, tiled=True)  8.07 us
    pallas_call x1, Pallas kernels, body(): pl.pallas_call(front_kernel, grid=(1,), in_specs=[VMEM, pl.BlockSpec((102...  5.54 us
  transfers between devices with their start and end apart: 8, of which 6 were waited for; matrix products, arithmetic and copies ran while one was open for 10% of the time, Pallas kernels for 10%

commit v1 on v0

--- a/solution.py
+++ b/solution.py
@@ -99,8 +99,9 @@
 
 
 def attend_kernel(
-    plan, query, kv_own, kv_oth, key_gate, query_gate, out, keys, values, queries, total
+    plan, queries, kv_own, kv_oth, key_gate, out, keys, values, total
 ):
+    mine_z, mine_y, mine_c = (plan[65], plan[66], plan[67])
     extra = lax.broadcasted_iota(jnp.int32, (16, 2 * SPAN), 0)
     ones = jnp.where(extra == 0, 1.0, 0.0).astype(BF16)
     for y in range(8):
@@ -113,31 +114,48 @@
             values[y, :HEAD, at : at + 128] = held[y, 128:192]
             values[y, :HEAD, at + 128 : at + SPAN] = held[y, 192:]
         values[y, HEAD:, :] = ones
-    for z in range(8):
-        for h in range(3):
-            queries[z, :HEAD, h * SPAN : (h + 1) * SPAN] = query[z, h * HEAD : (h + 1) * HEAD]
-        queries[z, HEAD:, :] = query_gate[z]
     total[...] = jnp.zeros_like(total)
-    mine_z, mine_y, mine_c = (plan[65], plan[66], plan[67])
-
-    scores = jnp.dot(keys[mine_y], queries[mine_z], preferred_element_type=F32)
-    place = lax.broadcasted_iota(jnp.int32, (2 * SPAN, 3 * SPAN), 0)
-    wanted = lax.broadcasted_iota(jnp.int32, (2 * SPAN, 3 * SPAN), 1) % SPAN
-    limit = jnp.where(place < SPAN, wanted, mine_c * (4 * SPAN) - 1)
-    weights = jnp.where(place <= limit, jnp.exp2(scores), 0.0).astype(BF16)
-    total[mine_z] += jnp.dot(values[mine_y], weights, preferred_element_type=F32)
-
-    def unit(i, carry):
-        code = plan[i]
-        z = code // 8
-        y = code % 8
-        weights = jnp.exp2(
-            jnp.dot(keys[y], queries[z], preferred_element_type=F32)
-        ).astype(BF16)
-        total[z] += jnp.dot(values[y], weights, preferred_element_type=F32)
+
+    place = lax.broadcasted_iota(jnp.int32, (2 * SPAN, SPAN), 0)
+    wanted = lax.broadcasted_iota(jnp.int32, (2 * SPAN, SPAN), 1)
+    allowed = place <= jnp.where(place < SPAN, wanted, mine_c * (4 * SPAN) - 1)
+    for h in range(3):
+        scores = jnp.dot(keys[mine_y], queries[0, h], preferred_element_type=F32)
+        weights = jnp.where(allowed, jnp.exp2(scores), 0.0).astype(BF16)
+        total[mine_z, :, h * SPAN : (h + 1) * SPAN] += jnp.dot(
+            values[mine_y], weights, preferred_element_type=F32
+        )
+
+    def units(places):
+        at = []
+        for i in places:
+            code = plan[i]
+            at.append((code // 8, code % 8))
+        chunks = [(z, y, h) for z, y in at for h in range(3)]
+
+        def scored(z, y, h):
+            return jnp.dot(keys[y], queries[(mine_z + 8 - z) % 8, h], preferred_element_type=F32)
+
+        ready = scored(*chunks[0])
+        for n, (z, y, h) in enumerate(chunks):
+            ahead = scored(*chunks[n + 1]) if n + 1 < len(chunks) else None
+            weights = jnp.exp2(ready).astype(BF16)
+            total[z, :, h * SPAN : (h + 1) * SPAN] += jnp.dot(
+                values[y], weights, preferred_element_type=F32
+            )
+            ready = ahead
+
+    def pair(i, carry):
+        units((2 * i, 2 * i + 1))
         return carry
 
-    lax.fori_loop(0, plan[64], unit, 0)
+    count = plan[64]
+    lax.fori_loop(0, count // 2, pair, 0)
+
+    @pl.when(count % 2 == 1)
+    def _():
+        units((count - 1,))
+
     for z in range(8):
         rows = []
         for h in range(3):
@@ -225,8 +243,8 @@
         raw * lax.rsqrt(jnp.mean(raw * raw, axis=-1, keepdims=True) + EPS) * pre_gain
     ).astype(BF16)
     halves = jnp.transpose(normed.reshape(64, 64, 2, 16), (2, 0, 1, 3)).reshape(2, 64, 1024)
-    halves = jnp.where(c == 0, halves, halves[::-1])
     rows = copies_from(halves, "tp")
+    rows = jnp.where(c == 0, rows, rows[:, ::-1])
 
     here = z * 16 + y * 2 + c
     positions = (here * SPAN + jnp.arange(SPAN, dtype=jnp.int32)).astype(F32)
@@ -250,18 +268,19 @@
     mine = lax.dynamic_index_in_dim(
         lax.dynamic_index_in_dim(gate, y, 2, keepdims=False), c, 2, keepdims=False
     )
-    plus = jnp.stack(three_parts(mine), axis=0)
-    plus = jnp.transpose(plus, (2, 0, 1, 3)).reshape(8, 3, 3 * SPAN)
+    wanted = (spans[:, None] == ((z - spans) % 8)[None, :])[None, :, :, None]
+    mine = jnp.sum(jnp.where(wanted, mine[:, :, None, :], 0.0), axis=1)
+    plus = jnp.transpose(jnp.stack(three_parts(mine), axis=0), (2, 1, 0, 3))
     own_head = (
-        (jnp.arange(9)[:, None] // 3) == (jnp.arange(3 * SPAN)[None, :] // SPAN)
+        jnp.arange(9, dtype=jnp.int32)[None, :] // 3 == jnp.arange(3, dtype=jnp.int32)[:, None]
     ).astype(BF16)
     query_gate = jnp.concatenate(
         [
-            jnp.broadcast_to(own_head, (8, 9, 3 * SPAN)),
+            jnp.broadcast_to(own_head[None, :, :, None], (8, 3, 9, SPAN)),
             plus,
-            jnp.zeros((8, 52, 3 * SPAN), BF16),
-        ],
-        axis=1,
+            jnp.zeros((8, 3, 52, SPAN), BF16),
+        ],
+        axis=2,
     )
     needed = (
         (key_z[None, :] < spans[:, None])
@@ -302,22 +321,25 @@
     states = lax.all_gather(state, SP, axis=0)
     kv_own = copies_from(kv_send, ("z", "y"), SKEW)
     kv_oth = swapped_cores(kv_own)
-    queries = copies_from(q_send, "z")
+    queries = [q_send]
+    for k in range(1, 8):
+        queries.append(lax.ppermute(q_send, "z", [(i, (i + k) % 8) for i in range(8)]))
+    queries = jnp.stack([part.reshape(3, HEAD, SPAN) for part in queries])
+    queries = jnp.concatenate([queries, query_gate], axis=2)
 
     partial = pl.pallas_call(
         attend_kernel,
-        in_specs=[SMEM, VMEM, VMEM, VMEM, VMEM, VMEM],
+        in_specs=[SMEM] + [VMEM] * 4,
         out_specs=VMEM,
         out_shape=jax.ShapeDtypeStruct((8, 208, SPAN), BF16),
         scratch_shapes=[
             pltpu.VMEM((8, 2 * SPAN, 128), BF16),
             pltpu.VMEM((8, 80, 2 * SPAN), BF16),
-            pltpu.VMEM((8, 128, 3 * SPAN), BF16),
             pltpu.VMEM((8, 80, 3 * SPAN), F32),
         ],
         compiler_params=PARAMS,
         name="attend",
-    )(plan, queries, kv_own, kv_oth, key_gate, query_gate)
+    )(plan, queries, kv_own, kv_oth, key_gate)
     parts = lax.all_to_all(partial, "z", 0, 0, tiled=True)
 
     ends = jnp.sum(states[:, HEAD : HEAD + 3, HEAD : HEAD + 3].astype(F32), axis=-1)

time: 250 us -> 265 us (1.060)
  the two profiles are of different devices: /device:TPU:16 before, /device:TPU:8 now
where the time goes in v1:
time: 265 us; the launch traced here: 264 us
  waiting for transfers between devices  98.3 us (37%)
  starting transfers between devices  47.5 us (18%)
  blocking collectives  38.3 us (14%)
  Pallas kernels  35.8 us (14%)
  other arithmetic  15.6 us (6%)
  local copies, waits for them, and re-layouts  14.8 us (6%)
  between operations  13.9 us (5%)
    all_gather x1, waiting for transfers between devices, body(): w_own = lax.all_gather(w_row, 'z', axis=0, tiled=True)  45.9 us
    ppermute x7, starting transfers between devices, body(): lax.ppermute(q_send, 'z', [(i, (i + k) % 8) for i in range(8)])  25.2 us
    ppermute x7, waiting for transfers between devices, body(): lax.ppermute(q_send, 'z', [(i, (i + k) % 8) for i in range(8)])  24.8 us
    pallas_call x1, Pallas kernels, body(): pl.pallas_call(attend_kernel, in_specs=[SMEM] + [VMEM] * 4, out_specs=VME...  21.1 us
    all_to_all x1, blocking collectives, copies_from(): lax.all_to_all(copies, axis, split_axis=0, concat_axis=0, tiled=True, axi...  19.3 us
    all_to_all x1, blocking collectives, body(): shares = lax.all_to_all(share.reshape(4, 64, 2048), 'tp', 0, 0, tiled=True)  19.1 us
    all_to_all x1, waiting for transfers between devices, body(): parts = lax.all_to_all(partial, 'z', 0, 0, tiled=True)  15.3 us
    all_to_all x2, starting transfers between devices, copies_from(): lax.all_to_all(copies, axis, split_axis=0, concat_axis=0, tiled=True, axi...  14.4 us
  transfers between devices with their start and end apart: 14, of which 7 were waited for; matrix products, arithmetic and copies ran while one was open for 10% of the time, Pallas kernels for 10%

profile of v1, /device:TPU:8, one launch (start us, length us, event | category | flops | bytes accessed | tf_op | source)
XLA Modules:
  0.0 264.3 jit_solution(11609898335313779695)
XLA Ops:
  7.5 19.3 %all_to_all.25 = bf16[8,16,1280]{2,1,0:T(8,128)(2,1)} all-to-all(bf16[8,16,1280]{2,1,0:T(8,128)(2,1)S(1)} %broadcast_in_dim.136), channel_id=1, replica_groups=mesh['z'=8,'y'=8,'c'=2,'tp'=4] {'y'}, dimensions={0} | all-to-all | bytes 655360 | tf_op jit(solution)/shard_map/all_to_all | solution.py:28
  26.8 45.9 %all-gather.4.cloned.1.call-done.w_own = bf16[1024,1280]{1,0:T(8,128)(2,1)} async-done(((bf16[128,1280]{1,0:T(8,128)(2,1)}), bf16[1024,1280]{1,0:T(8,128)(2,1)}) %all-gather.4.cloned.1.call-update) | async-done | bytes 2621456 | tf_op jit(solution)/shard_map/all_gather | solution.py:238
  77.8 4.3 %all-to-all-start = ((bf16[4,2,64,1024]{3,2,1,0:T(8,128)(2,1)}), bf16[4,2,64,1024]{3,2,1,0:T(8,128)(2,1)}, u32[]{:S(2)}, u32[]{:S(2)}) async-start(bf16[4,2,64,1024]{3,2,1,0:T(8,128)(2,1)} %broadcast_in_dim.135), calls=%async_computation | async-start | bytes 2097152 | tf_op jit(solution)/shard_map/all_to_all | solution.py:28
  86.2 12.0 %all-to-all-done = bf16[4,2,64,1024]{3,2,1,0:T(8,128)(2,1)} async-done(((bf16[4,2,64,1024]{3,2,1,0:T(8,128)(2,1)}), bf16[4,2,64,1024]{3,2,1,0:T(8,128)(2,1)}, u32[]{:S(2)}, u32[]{:S(2)}) %all-to-all-start) | async-done | bytes 1048608 | tf_op jit(solution)/shard_map/all_to_all | solution.py:28
  98.2 3.1 %reverse_select_fusion.rows = bf16[4,2,64,1024]{3,2,1,0:T(8,128)(2,1)} fusion(bf16[4,2,64,1024]{3,2,1,0:T(8,128)(2,1)} %all-to-all-done, pred[]{:T(512)S(6)} %eq.96), kind=kLoop, calls=%fused_computation.2 | loop fusion | flops 524288 | bytes 2097153 | tf_op jit(solution)/shard_map/jit(_where)/select_n | solution.py:247
  102.8 5.5 %front.1 = (bf16[192,256]{1,0:T(8,128)(2,1)}, bf16[256,128]{1,0:T(8,128)(2,1)}, f32[256,192]{1,0:T(8,128)}, bf16[256,192]{1,0:T(8,128)(2,1)}, bf16[128,128]{1,0:T(8,128)(2,1)}) custom-call(bf16[4,2,64,1024]{3,2,1,0:T(8,128)(2,1)} %reverse_select_fusion.rows, bf16[1024,1280]{1,0:T(8,128)(2,1)} %all-gather.4.cloned.1.call-done.w_own, ...), custom_call_target="tpu_custom_call" | custom-call | tf_op jit(solution)/shard_map/front/pallas_call | solution.py:296
  114.7 10.1 %all-to-all-start.2 = ((bf16[8,256,128]{2,1,0:T(8,128)(2,1)}), bf16[8,256,128]{2,1,0:T(8,128)(2,1)S(1)}, u32[]{:S(2)}, u32[]{:S(2)}) async-start(bf16[8,256,128]{2,1,0:T(8,128)(2,1)} %broadcast_in_dim.143), calls=%async_computation.2 | async-start | bytes 1048576 | tf_op jit(solution)/shard_map/all_to_all | solution.py:28
  126.2 4.1 %collective-permute-start.7 = (bf16[192,256]{1,0:T(8,128)(2,1)S(1)}, bf16[192,256]{1,0:T(8,128)(2,1)S(1)}, u32[]{:S(2)}, u32[]{:S(2)}) collective-permute-start(bf16[192,256]{1,0:T(8,128)(2,1)S(1)} %copy-done.4), channel_id=1, source_target_pairs={{0,448},{64,0},{128,64},{192,128},{256,192},{320,256},{384,320},{4... | collective-permute-start | bytes 294920 | tf_op jit(solution)/shard_map/ppermute | solution.py:326
  130.4 2.7 %collective-permute-start.6 = (bf16[192,256]{1,0:T(8,128)(2,1)S(1)}, bf16[192,256]{1,0:T(8,128)(2,1)S(1)}, u32[]{:S(2)}, u32[]{:S(2)}) collective-permute-start(bf16[192,256]{1,0:T(8,128)(2,1)S(1)} %copy-done.4), channel_id=1, source_target_pairs={{0,384},{64,448},{128,0},{192,64},{256,128},{320,192},{384,256},{4... | collective-permute-start | bytes 294920 | tf_op jit(solution)/shard_map/ppermute | solution.py:326
  133.1 4.8 %collective-permute-start.5 = (bf16[192,256]{1,0:T(8,128)(2,1)S(1)}, bf16[192,256]{1,0:T(8,128)(2,1)S(1)}, u32[]{:S(2)}, u32[]{:S(2)}) collective-permute-start(bf16[192,256]{1,0:T(8,128)(2,1)S(1)} %copy-done.4), channel_id=1, source_target_pairs={{0,320},{64,384},{128,448},{192,0},{256,64},{320,128},{384,192},{4... | collective-permute-start | bytes 294920 | tf_op jit(solution)/shard_map/ppermute | solution.py:326
  138.0 5.1 %collective-permute-start.4 = (bf16[192,256]{1,0:T(8,128)(2,1)S(1)}, bf16[192,256]{1,0:T(8,128)(2,1)S(1)}, u32[]{:S(2)}, u32[]{:S(2)}) collective-permute-start(bf16[192,256]{1,0:T(8,128)(2,1)S(1)} %copy-done.4), channel_id=1, source_target_pairs={{0,256},{64,320},{128,384},{192,448},{256,0},{320,64},{384,128},{4... | collective-permute-start | bytes 294920 | tf_op jit(solution)/shard_map/ppermute | solution.py:326
  143.1 2.9 %collective-permute-start.1 = (bf16[192,256]{1,0:T(8,128)(2,1)S(1)}, bf16[192,256]{1,0:T(8,128)(2,1)S(1)}, u32[]{:S(2)}, u32[]{:S(2)}) collective-permute-start(bf16[192,256]{1,0:T(8,128)(2,1)S(1)} %copy-done.4), channel_id=1, source_target_pairs={{0,64},{64,128},{128,192},{192,256},{256,320},{320,384},{384,448},... | collective-permute-start | bytes 294920 | tf_op jit(solution)/shard_map/ppermute | solution.py:326
  146.0 7.2 %collective-permute-done.1 = bf16[192,256]{1,0:T(8,128)(2,1)S(1)} collective-permute-done((bf16[192,256]{1,0:T(8,128)(2,1)S(1)}, bf16[192,256]{1,0:T(8,128)(2,1)S(1)}, u32[]{:S(2)}, u32[]{:S(2)}) %collective-permute-start.1) | collective-permute-done | bytes 98336 | tf_op jit(solution)/shard_map/ppermute | solution.py:326
  153.2 3.3 %collective-permute-start.2 = (bf16[192,256]{1,0:T(8,128)(2,1)S(1)}, bf16[192,256]{1,0:T(8,128)(2,1)S(1)}, u32[]{:S(2)}, u32[]{:S(2)}) collective-permute-start(bf16[192,256]{1,0:T(8,128)(2,1)S(1)} %copy-done.4), channel_id=1, source_target_pairs={{0,128},{64,192},{128,256},{192,320},{256,384},{320,448},{384,0},{... | collective-permute-start | bytes 294920 | tf_op jit(solution)/shard_map/ppermute | solution.py:326
  156.5 6.9 %collective-permute-done.2 = bf16[192,256]{1,0:T(8,128)(2,1)S(1)} collective-permute-done((bf16[192,256]{1,0:T(8,128)(2,1)S(1)}, bf16[192,256]{1,0:T(8,128)(2,1)S(1)}, u32[]{:S(2)}, u32[]{:S(2)}) %collective-permute-start.2) | collective-permute-done | bytes 98336 | tf_op jit(solution)/shard_map/ppermute | solution.py:326
  163.4 2.2 collective-permute-start.3
  165.6 10.8 %collective-permute-done.3 = bf16[192,256]{1,0:T(8,128)(2,1)S(1)} collective-permute-done((bf16[192,256]{1,0:T(8,128)(2,1)S(1)}, bf16[192,256]{1,0:T(8,128)(2,1)S(1)}, u32[]{:S(2)}, u32[]{:S(2)}) %collective-permute-start.3) | collective-permute-done | bytes 98336 | tf_op jit(solution)/shard_map/ppermute | solution.py:326
  176.5 1.9 collective-permute-start.8
  181.3 21.1 %attend.1 = bf16[8,208,256]{2,1,0:T(8,128)(2,1)} custom-call(s32[68]{0:T(128)} %concatenate.12.plan, bf16[8,3,128,256]{3,2,1,0:T(8,128)(2,1)} %maximum_maximum_fusion.queries, bf16[8,256,128]{2,1,0:T(8,128)(2,1)} %copy-done.2, bf16[8,256,128]{2,1,0:T(8,128)(2,1)} %copy-done.3, bf16[2,8,256,64]{3,2,1,0:T(8,128)(2,1)} %maximum_bitcast_fusion.key_gate), custom_call_target="tpu_custom_call" | custom-call | tf_op jit(solution)/shard_map/attend/pallas_call | solution.py:330
  202.5 4.0 %all-to-all-start.3 = ((bf16[8,208,256]{2,1,0:T(8,128)(2,1)}), bf16[8,208,256]{2,1,0:T(8,128)(2,1)S(1)}, u32[]{:S(2)}, u32[]{:S(2)}) async-start(bf16[8,208,256]{2,1,0:T(8,128)(2,1)} %attend.1), calls=%async_computation.3 | async-start | bytes 1703936 | tf_op jit(solution)/shard_map/all_to_all | solution.py:343
  212.1 4.3 %combine.1.state = bf16[128,128]{1,0:T(8,128)(2,1)} custom-call(bf16[128,128,128]{2,1,0:T(8,128)(2,1)} %bitcast.64, f32[128,128]{1,0:T(8,128)} %copy.113.above, f32[128,128]{1,0:T(8,128)} %pad.9.below), custom_call_target="tpu_custom_call" | custom-call | tf_op jit(solution)/shard_map/combine/pallas_call | solution.py:352
  216.3 15.3 %all-to-all-done.3.parts = bf16[8,208,256]{2,1,0:T(8,128)(2,1)S(1)} async-done(((bf16[8,208,256]{2,1,0:T(8,128)(2,1)}), bf16[8,208,256]{2,1,0:T(8,128)(2,1)S(1)}, u32[]{:S(2)}, u32[]{:S(2)}) %all-to-all-start.3) | async-done | bytes 852000 | tf_op jit(solution)/shard_map/all_to_all | solution.py:343
  232.6 4.9 %back.1 = bf16[256,2048]{1,0:T(8,128)(2,1)} custom-call(bf16[8,208,256]{2,1,0:T(8,128)(2,1)} %copy-done.1, f32[256,192]{1,0:T(8,128)} %get-tuple-element.12.local, bf16[256,192]{1,0:T(8,128)(2,1)} %get-tuple-element.13.lifted, bf16[128,128]{1,0:T(8,128)(2,1)} %combine.1.state, bf16[2048,384]{1,0:T(8,128)(2,1)} %bitcast.62), custom_call_target="tpu_custom_call" | custom-call | tf_op jit(solution)/shard_map/back/pallas_call | solution.py:366
  237.5 19.1 %all_to_all.26 = bf16[4,64,2048]{2,1,0:T(8,128)(2,1)S(1)} all-to-all(bf16[4,64,2048]{2,1,0:T(8,128)(2,1)} %bitcast.66), channel_id=1, replica_groups=mesh['z'=8,'y'=8,'c'=2,'tp'=4] {'tp'}, dimensions={0} | all-to-all | bytes 2097152 | tf_op jit(solution)/shard_map/all_to_all | solution.py:375
  (116 shorter events, 29.6 us)
Async XLA Ops:
  6.5 69.6 %copy-start.6 = (f32[2048]{0:T(1024)S(1)}, f32[2048]{0:T(1024)}, u32[]{:S(2)}) copy-start(f32[2048]{0:T(1024)} %param.13) | copy-start | bytes 24580
  6.5 66.1 %all-gather.4.cloned.1.call-start = ((), (), s32[]{:S(2)}) async-start(), calls=%async_computation.5 | async-start | bytes 2949120 | tf_op jit(solution)/shard_map/all_gather | solution.py:238
  72.7 28.6 %collective-permute-start = (bf16[1024,1280]{1,0:T(8,128)(2,1)}, bf16[1024,1280]{1,0:T(8,128)(2,1)S(1)}, u32[]{:S(2)}, u32[]{:S(2)}) collective-permute-start(bf16[1024,1280]{1,0:T(8,128)(2,1)} %all-gather.4.cloned.1.call-done.w_own), channel_id=1, source_target_pairs={{0,4},{4,0},{1,5},{5,1},{2,6},{6,2},{3,7},{7,3},{8,12},{12,8},{9,1... | collective-permute-start | bytes 7864328 | tf_op jit(solution)/shard_map/ppermute | solution.py:34
  76.5 5.7 %copy-start.7 = (f32[256,3]{0,1:T(4,128)S(1)}, f32[256,3]{0,1:T(4,128)}, u32[]{:S(2)}) copy-start(f32[256,3]{0,1:T(4,128)} %param.22) | copy-start | bytes 9220
  77.8 20.4 %all-to-all-start = ((bf16[4,2,64,1024]{3,2,1,0:T(8,128)(2,1)}), bf16[4,2,64,1024]{3,2,1,0:T(8,128)(2,1)}, u32[]{:S(2)}, u32[]{:S(2)}) async-start(bf16[4,2,64,1024]{3,2,1,0:T(8,128)(2,1)} %broadcast_in_dim.135), calls=%async_computation | async-start | bytes 2097152 | tf_op jit(solution)/shard_map/all_to_all | solution.py:28
  82.1 127.0 %all-gather.6.cloned.1.call-start = ((), (), s32[]{:S(2)}) async-start(), calls=%async_computation.6 | async-start | bytes 4227072 | tf_op jit(solution)/shard_map/all_gather | solution.py:321
  101.3 1.5 copy-start
  108.4 5.4 %copy-start.5 = (bf16[256,128]{1,0:T(8,128)(2,1)S(1)}, bf16[256,128]{1,0:T(8,128)(2,1)}, u32[]{:S(2)}) copy-start(bf16[256,128]{1,0:T(8,128)(2,1)} %get-tuple-element.11) | copy-start | bytes 196612
  111.6 14.6 %copy-start.4 = (bf16[192,256]{1,0:T(8,128)(2,1)S(1)}, bf16[192,256]{1,0:T(8,128)(2,1)}, u32[]{:S(2)}) copy-start(bf16[192,256]{1,0:T(8,128)(2,1)} %get-tuple-element.10) | copy-start | bytes 294916
  114.7 61.7 %all-to-all-start.2 = ((bf16[8,256,128]{2,1,0:T(8,128)(2,1)}), bf16[8,256,128]{2,1,0:T(8,128)(2,1)S(1)}, u32[]{:S(2)}, u32[]{:S(2)}) async-start(bf16[8,256,128]{2,1,0:T(8,128)(2,1)} %broadcast_in_dim.143), calls=%async_computation.2 | async-start | bytes 1048576 | tf_op jit(solution)/shard_map/all_to_all | solution.py:28
  126.2 52.2 %collective-permute-start.7 = (bf16[192,256]{1,0:T(8,128)(2,1)S(1)}, bf16[192,256]{1,0:T(8,128)(2,1)S(1)}, u32[]{:S(2)}, u32[]{:S(2)}) collective-permute-start(bf16[192,256]{1,0:T(8,128)(2,1)S(1)} %copy-done.4), channel_id=1, source_target_pairs={{0,448},{64,0},{128,64},{192,128},{256,192},{320,256},{384,320},{4... | collective-permute-start | bytes 294920 | tf_op jit(solution)/shard_map/ppermute | solution.py:326
  130.4 48.0 %collective-permute-start.6 = (bf16[192,256]{1,0:T(8,128)(2,1)S(1)}, bf16[192,256]{1,0:T(8,128)(2,1)S(1)}, u32[]{:S(2)}, u32[]{:S(2)}) collective-permute-start(bf16[192,256]{1,0:T(8,128)(2,1)S(1)} %copy-done.4), channel_id=1, source_target_pairs={{0,384},{64,448},{128,0},{192,64},{256,128},{320,192},{384,256},{4... | collective-permute-start | bytes 294920 | tf_op jit(solution)/shard_map/ppermute | solution.py:326
  133.1 45.2 %collective-permute-start.5 = (bf16[192,256]{1,0:T(8,128)(2,1)S(1)}, bf16[192,256]{1,0:T(8,128)(2,1)S(1)}, u32[]{:S(2)}, u32[]{:S(2)}) collective-permute-start(bf16[192,256]{1,0:T(8,128)(2,1)S(1)} %copy-done.4), channel_id=1, source_target_pairs={{0,320},{64,384},{128,448},{192,0},{256,64},{320,128},{384,192},{4... | collective-permute-start | bytes 294920 | tf_op jit(solution)/shard_map/ppermute | solution.py:326
  138.0 38.4 %collective-permute-start.4 = (bf16[192,256]{1,0:T(8,128)(2,1)S(1)}, bf16[192,256]{1,0:T(8,128)(2,1)S(1)}, u32[]{:S(2)}, u32[]{:S(2)}) collective-permute-start(bf16[192,256]{1,0:T(8,128)(2,1)S(1)} %copy-done.4), channel_id=1, source_target_pairs={{0,256},{64,320},{128,384},{192,448},{256,0},{320,64},{384,128},{4... | collective-permute-start | bytes 294920 | tf_op jit(solution)/shard_map/ppermute | solution.py:326
  143.1 10.1 %collective-permute-start.1 = (bf16[192,256]{1,0:T(8,128)(2,1)S(1)}, bf16[192,256]{1,0:T(8,128)(2,1)S(1)}, u32[]{:S(2)}, u32[]{:S(2)}) collective-permute-start(bf16[192,256]{1,0:T(8,128)(2,1)S(1)} %copy-done.4), channel_id=1, source_target_pairs={{0,64},{64,128},{128,192},{192,256},{256,320},{320,384},{384,448},... | collective-permute-start | bytes 294920 | tf_op jit(solution)/shard_map/ppermute | solution.py:326
  153.2 10.2 %collective-permute-start.2 = (bf16[192,256]{1,0:T(8,128)(2,1)S(1)}, bf16[192,256]{1,0:T(8,128)(2,1)S(1)}, u32[]{:S(2)}, u32[]{:S(2)}) collective-permute-start(bf16[192,256]{1,0:T(8,128)(2,1)S(1)} %copy-done.4), channel_id=1, source_target_pairs={{0,128},{64,192},{128,256},{192,320},{256,384},{320,448},{384,0},{... | collective-permute-start | bytes 294920 | tf_op jit(solution)/shard_map/ppermute | solution.py:326
  163.4 13.0 %collective-permute-start.3 = (bf16[192,256]{1,0:T(8,128)(2,1)S(1)}, bf16[192,256]{1,0:T(8,128)(2,1)S(1)}, u32[]{:S(2)}, u32[]{:S(2)}) collective-permute-start(bf16[192,256]{1,0:T(8,128)(2,1)S(1)} %copy-done.4), channel_id=1, source_target_pairs={{0,192},{64,256},{128,320},{192,384},{256,448},{320,0},{384,64},{4... | collective-permute-start | bytes 294920 | tf_op jit(solution)/shard_map/ppermute | solution.py:326
  176.4 4.1 %copy-start.2 = (bf16[8,256,128]{2,1,0:T(8,128)(2,1)}, bf16[8,256,128]{2,1,0:T(8,128)(2,1)S(1)}, u32[]{:S(2)}) copy-start(bf16[8,256,128]{2,1,0:T(8,128)(2,1)S(1)} %all-to-all-done.2.kv_own) | copy-start | bytes 1572868
  176.5 4.1 %collective-permute-start.8 = (bf16[8,256,128]{2,1,0:T(8,128)(2,1)S(1)}, bf16[8,256,128]{2,1,0:T(8,128)(2,1)S(1)}, u32[]{:S(2)}, u32[]{:S(2)}) collective-permute-start(bf16[8,256,128]{2,1,0:T(8,128)(2,1)S(1)} %all-to-all-done.2.kv_own), channel_id=1, source_target_pairs={{0,4},{4,0},{1,5},{5,1},{2,6},{6,2},{3,7},{7,3},{8,12},{12,8},{9,1... | collective-permute-start | bytes 1572872 | tf_op jit(solution)/shard_map/ppermute | solution.py:34
  180.5 0.8 copy-start.3
  202.4 5.3 %slice-start = ((bf16[1024,1280]{1,0:T(8,128)(2,1)}), bf16[1024,384]{1,0:T(8,128)(2,1)S(1)}, s32[]{:S(2)}) async-start(bf16[1024,1280]{1,0:T(8,128)(2,1)} %copy-done), calls=%async_computation.7 | async-start | bytes 1572864 | tf_op jit(solution)/shard_map/slice | solution.py:362
  202.5 29.2 %all-to-all-start.3 = ((bf16[8,208,256]{2,1,0:T(8,128)(2,1)}), bf16[8,208,256]{2,1,0:T(8,128)(2,1)S(1)}, u32[]{:S(2)}, u32[]{:S(2)}) async-start(bf16[8,208,256]{2,1,0:T(8,128)(2,1)} %attend.1), calls=%async_computation.3 | async-start | bytes 1703936 | tf_op jit(solution)/shard_map/all_to_all | solution.py:343
  231.6 0.9 copy-start.1
Sparse Core Ops, SparseCore 0:
  26.9 45.7 all-gather.3
  108.5 90.5 all-gather.5

commit v2 on v1

--- a/solution.py
+++ b/solution.py
@@ -42,12 +42,16 @@
     return [part.astype(BF16) for part in (high, middle, low)]
 
 
+def project_kernel(rows, weights, own_out, oth_out):
+    product = jnp.dot(rows[...], weights[...], preferred_element_type=F32)
+    own_out[...] = product[:SPAN]
+    oth_out[...] = product[SPAN:]
+
+
 def front_kernel(
-    rows, w_own, w_oth, cosine, sine, decay, decay_row, q_out, kv_out, local_out, lifted_out, state_out, proj
+    first_part, second_part, cosine, sine, decay, decay_row, q_out, kv_out, local_out, lifted_out, proj
 ):
-    proj[...] = jnp.dot(
-        rows[:, 0].reshape(SPAN, -1), w_own[...], preferred_element_type=F32
-    ) + jnp.dot(rows[:, 1].reshape(SPAN, -1), w_oth[...], preferred_element_type=F32)
+    proj[...] = first_part[...] + second_part[...]
     cos = cosine[...]
     sin = sine[...]
     place = lax.broadcasted_iota(jnp.int32, (SPAN, SPAN), 0)
@@ -76,30 +80,23 @@
         )
         faded = (key.astype(F32) * jnp.exp(last - column)).astype(BF16)
         update = lax.dot_general(faded, value, TN, preferred_element_type=F32)
-        state_out[(h // 2) * HEAD : (h // 2 + 1) * HEAD, (h % 2) * HEAD : (h % 2 + 1) * HEAD] = (
-            update.astype(BF16)
+        update = update.astype(BF16)
+        kv_out[SPAN + 32 * h : SPAN + 32 * (h + 1)] = jnp.concatenate(
+            [update[:32], update[32:]], axis=1
         )
         lifted_out[:, h * HEAD : (h + 1) * HEAD] = (
             query.astype(F32) * jnp.exp(column)
         ).astype(BF16)
-    ends = decay_row[:, SPAN - 1 : SPAN]
-    high = ends.astype(BF16).astype(F32)
-    middle = (ends - high).astype(BF16).astype(F32)
-    low = ends - high - middle
-    lane = lax.broadcasted_iota(jnp.int32, (8, HEAD), 1)
-    tail = jnp.where(lane == 0, high, jnp.where(lane == 1, middle, jnp.where(lane == 2, low, 0.0)))
-    state_out[HEAD:, HEAD:] = jnp.concatenate(
-        [tail, jnp.zeros((HEAD - 8, HEAD), F32)], axis=0
-    ).astype(BF16)
-    q_out[...] = jnp.transpose(proj[:, 576:768] * (HEAD ** (-0.5) * LOG2E)).astype(BF16)
+    q_out[192:] = jnp.zeros((HEAD, SPAN), BF16)
+    q_out[:192] = jnp.transpose(proj[:, 576:768] * (HEAD ** (-0.5) * LOG2E)).astype(BF16)
     both = proj[:, 768:896]
     flipped = jnp.transpose(both)[HEAD:, :].astype(BF16)
     kv_out[:128] = jnp.concatenate([both[:128, :HEAD], both[128:, :HEAD]], axis=1).astype(BF16)
-    kv_out[128:] = jnp.concatenate([flipped[:, :128], flipped[:, 128:]], axis=0)
+    kv_out[128:SPAN] = jnp.concatenate([flipped[:, :128], flipped[:, 128:]], axis=0)
 
 
 def attend_kernel(
-    plan, queries, kv_own, kv_oth, key_gate, out, keys, values, total
+    plan, fade, received, query_gate, kv_own, kv_oth, key_gate, out, keys, values, queries, total
 ):
     mine_z, mine_y, mine_c = (plan[65], plan[66], plan[67])
     extra = lax.broadcasted_iota(jnp.int32, (16, 2 * SPAN), 0)
@@ -112,15 +109,19 @@
             keys[y, at + 128 : at + SPAN, :HEAD] = packed[:, HEAD:]
             keys[y, at : at + SPAN, HEAD:] = key_gate[side, y]
             values[y, :HEAD, at : at + 128] = held[y, 128:192]
-            values[y, :HEAD, at + 128 : at + SPAN] = held[y, 192:]
+            values[y, :HEAD, at + 128 : at + SPAN] = held[y, 192:SPAN]
         values[y, HEAD:, :] = ones
+    for z in range(8):
+        for h in range(3):
+            queries[z, h, :HEAD] = received[z, h * HEAD : (h + 1) * HEAD]
+            queries[z, h, HEAD:] = query_gate[z, h]
     total[...] = jnp.zeros_like(total)
 
     place = lax.broadcasted_iota(jnp.int32, (2 * SPAN, SPAN), 0)
     wanted = lax.broadcasted_iota(jnp.int32, (2 * SPAN, SPAN), 1)
     allowed = place <= jnp.where(place < SPAN, wanted, mine_c * (4 * SPAN) - 1)
     for h in range(3):
-        scores = jnp.dot(keys[mine_y], queries[0, h], preferred_element_type=F32)
+        scores = jnp.dot(keys[mine_y], queries[mine_z, h], preferred_element_type=F32)
         weights = jnp.where(allowed, jnp.exp2(scores), 0.0).astype(BF16)
         total[mine_z, :, h * SPAN : (h + 1) * SPAN] += jnp.dot(
             values[mine_y], weights, preferred_element_type=F32
@@ -134,7 +135,7 @@
         chunks = [(z, y, h) for z, y in at for h in range(3)]
 
         def scored(z, y, h):
-            return jnp.dot(keys[y], queries[(mine_z + 8 - z) % 8, h], preferred_element_type=F32)
+            return jnp.dot(keys[y], queries[z, h], preferred_element_type=F32)
 
         ready = scored(*chunks[0])
         for n, (z, y, h) in enumerate(chunks):
@@ -165,32 +166,33 @@
             rows.append(total[z, HEAD : HEAD + 1, h * SPAN : (h + 1) * SPAN])
         high = [row.astype(BF16).astype(F32) for row in rows]
         low = [row - big for row, big in zip(rows, high)]
-        out[z, 192:] = jnp.concatenate(high + low + [jnp.zeros((10, SPAN), F32)], axis=0).astype(
-            BF16
-        )
-
-
-def combine_kernel(states, above, below, out):
-    def add(j, carry):
-        upper, lower = carry
-        upper = upper + states[j, :HEAD].astype(F32) * above[pl.ds(j, 1), :]
-        lower = lower + states[j, HEAD:].astype(F32) * below[pl.ds(j, 1), :]
-        return (upper, lower)
-
-    zero = jnp.zeros((HEAD, 128), F32)
-    upper, lower = lax.fori_loop(0, states.shape[0], add, (zero, zero))
-    out[:HEAD] = upper.astype(BF16)
-    out[HEAD:] = lower.astype(BF16)
-
-
-def back_kernel(parts, local, lifted, state, w_out, out, mixed):
+        out[z, 192:208] = jnp.concatenate(
+            high + low + [jnp.zeros((10, SPAN), F32)], axis=0
+        ).astype(BF16)
+    for z in range(8):
+        sums = []
+        for h in range(3):
+            at = SPAN + 32 * h
+            state = jnp.zeros((32, 128), F32)
+            for side, held in enumerate((kv_own, kv_oth)):
+                for y in range(8):
+                    state = state + held[y, at : at + 32].astype(F32) * fade[
+                        ((z * 2 + side) * 8 + y) * 3 + h
+                    ]
+            sums.append(state)
+        sums = jnp.concatenate(sums, axis=0).astype(BF16)
+        out[z, 208:, :128] = sums[:48]
+        out[z, 208:, 128:] = sums[48:]
+
+
+def back_kernel(parts, local, lifted, w_out, out, mixed):
     total = parts[0].astype(F32)
     for z in range(1, 8):
         total = total + parts[z].astype(F32)
+    states = jnp.concatenate([total[208:, :128], total[208:, 128:]], axis=0)
     for h in range(3):
-        held = state[
-            (h // 2) * HEAD : (h // 2 + 1) * HEAD, (h % 2) * HEAD : (h % 2 + 1) * HEAD
-        ]
+        held = states[32 * h : 32 * (h + 1)]
+        held = jnp.concatenate([held[:, :HEAD], held[:, HEAD:]], axis=0).astype(BF16)
         raw = local[:, h * HEAD : (h + 1) * HEAD] + jnp.dot(
             lifted[:, h * HEAD : (h + 1) * HEAD], held, preferred_element_type=F32
         )
@@ -236,7 +238,6 @@
     width = shard.shape[1]
     w_row = copies_from(shard, "y").reshape(-1, width)
     w_own = lax.all_gather(w_row, "z", axis=0, tiled=True)
-    w_oth = swapped_cores(w_own)
 
     raw = tokens.astype(F32)
     normed = (
@@ -244,7 +245,10 @@
     ).astype(BF16)
     halves = jnp.transpose(normed.reshape(64, 64, 2, 16), (2, 0, 1, 3)).reshape(2, 64, 1024)
     rows = copies_from(halves, "tp")
-    rows = jnp.where(c == 0, rows, rows[:, ::-1])
+    kept = jnp.where(c == 0, rows[:, 0], rows[:, 1]).reshape(SPAN, 1024)
+    sent = jnp.where(c == 0, rows[:, 1], rows[:, 0]).reshape(SPAN, 1024)
+    came = swapped_cores(sent)
+    rows = jnp.concatenate([kept, came], axis=0)
 
     here = z * 16 + y * 2 + c
     positions = (here * SPAN + jnp.arange(SPAN, dtype=jnp.int32)).astype(F32)
@@ -253,6 +257,8 @@
     cosine, sine = (jnp.cos(angles), jnp.sin(angles))
     decay = jnp.cumsum(retain_log, axis=0)
     decay_row = jnp.pad(decay.T, ((0, 5), (0, 0)))
+    ends = lax.all_gather(decay[-1], "c")
+    ends = copies_from(copies_from(ends, "y"), "z").reshape(128, 3)
 
     gate = (forget_total * LOG2E).reshape(3, 8, 8, 2, SPAN)
     spans = jnp.arange(8, dtype=jnp.int32)
@@ -268,8 +274,6 @@
     mine = lax.dynamic_index_in_dim(
         lax.dynamic_index_in_dim(gate, y, 2, keepdims=False), c, 2, keepdims=False
     )
-    wanted = (spans[:, None] == ((z - spans) % 8)[None, :])[None, :, :, None]
-    mine = jnp.sum(jnp.where(wanted, mine[:, :, None, :], 0.0), axis=1)
     plus = jnp.transpose(jnp.stack(three_parts(mine), axis=0), (2, 1, 0, 3))
     own_head = (
         jnp.arange(9, dtype=jnp.int32)[None, :] // 3 == jnp.arange(3, dtype=jnp.int32)[:, None]
@@ -282,6 +286,14 @@
         ],
         axis=2,
     )
+    blocks = key_z * 16 + spans * 2
+    blocks = jnp.stack([blocks + c, blocks + 1 - c])
+    targets = spans * 16 + y * 2 + c
+    index = jnp.arange(128, dtype=jnp.int32)
+    between = (index > blocks[None, :, :, None]) & (index < targets[:, None, None, None])
+    fade = jnp.sum(jnp.where(between[..., None], ends, 0.0), axis=3)
+    earlier = blocks[None] < targets[:, None, None]
+    fade = jnp.where(earlier[..., None], jnp.exp(fade), 0.0).reshape(384)
     needed = (
         (key_z[None, :] < spans[:, None])
         | ((key_z[None, :] == spans[:, None]) & (spans[None, :] < y))
@@ -293,85 +305,65 @@
     )
     plan = jnp.concatenate([units, jnp.stack([jnp.sum(needed.astype(jnp.int32)), z, y, c])])
 
-    q_send, kv_send, local, lifted, state = pl.pallas_call(
+    own_part, oth_part = pl.pallas_call(
+        project_kernel,
+        grid=(1,),
+        in_specs=[VMEM, pl.BlockSpec((1024, 896), lambda i: (0, 0))],
+        out_specs=[VMEM] * 2,
+        out_shape=[jax.ShapeDtypeStruct((SPAN, 896), F32)] * 2,
+        compiler_params=PARAMS,
+        name="project",
+    )(rows, w_own)
+    q_send, kv_send, local, lifted = pl.pallas_call(
         front_kernel,
-        grid=(1,),
-        in_specs=[
-            VMEM,
-            pl.BlockSpec((1024, 896), lambda i: (0, 0)),
-            pl.BlockSpec((1024, 896), lambda i: (0, 0)),
-            VMEM,
-            VMEM,
-            VMEM,
-            VMEM,
-        ],
-        out_specs=[VMEM] * 5,
+        in_specs=[VMEM] * 6,
+        out_specs=[VMEM] * 4,
         out_shape=[
-            jax.ShapeDtypeStruct((192, SPAN), BF16),
-            jax.ShapeDtypeStruct((SPAN, 128), BF16),
+            jax.ShapeDtypeStruct((SPAN, SPAN), BF16),
+            jax.ShapeDtypeStruct((SPAN + 96, 128), BF16),
             jax.ShapeDtypeStruct((SPAN, 192), F32),
             jax.ShapeDtypeStruct((SPAN, 192), BF16),
-            jax.ShapeDtypeStruct((128, 128), BF16),
         ],
         scratch_shapes=[pltpu.VMEM((SPAN, 896), F32)],
         compiler_params=PARAMS,
         name="front",
-    )(rows, w_own, w_oth, cosine, sine, decay, decay_row)
-
-    states = lax.all_gather(state, SP, axis=0)
+    )(own_part, swapped_cores(oth_part), cosine, sine, decay, decay_row)
+
+    queries = lax.all_gather(q_send, "z", axis=0)
     kv_own = copies_from(kv_send, ("z", "y"), SKEW)
     kv_oth = swapped_cores(kv_own)
-    queries = [q_send]
-    for k in range(1, 8):
-        queries.append(lax.ppermute(q_send, "z", [(i, (i + k) % 8) for i in range(8)]))
-    queries = jnp.stack([part.reshape(3, HEAD, SPAN) for part in queries])
-    queries = jnp.concatenate([queries, query_gate], axis=2)
 
     partial = pl.pallas_call(
         attend_kernel,
-        in_specs=[SMEM] + [VMEM] * 4,
+        in_specs=[SMEM] * 2 + [VMEM] * 5,
         out_specs=VMEM,
-        out_shape=jax.ShapeDtypeStruct((8, 208, SPAN), BF16),
+        out_shape=jax.ShapeDtypeStruct((8, SPAN, SPAN), BF16),
         scratch_shapes=[
             pltpu.VMEM((8, 2 * SPAN, 128), BF16),
             pltpu.VMEM((8, 80, 2 * SPAN), BF16),
+            pltpu.VMEM((8, 3, 128, SPAN), BF16),
             pltpu.VMEM((8, 80, 3 * SPAN), F32),
         ],
         compiler_params=PARAMS,
         name="attend",
-    )(plan, queries, kv_own, kv_oth, key_gate)
+    )(plan, fade, queries, query_gate, kv_own, kv_oth, key_gate)
     parts = lax.all_to_all(partial, "z", 0, 0, tiled=True)
 
-    ends = jnp.sum(states[:, HEAD : HEAD + 3, HEAD : HEAD + 3].astype(F32), axis=-1)
-    index = jnp.arange(128, dtype=jnp.int32)
-    between = (index[None, :] > index[:, None]) & (index[None, :] < here)
-    span_log = jnp.sum(jnp.where(between[:, :, None], ends[None], 0.0), axis=1)
-    factor = jnp.where((index < here)[:, None], jnp.exp(span_log), 0.0)
-    above = jnp.repeat(factor[:, :2], HEAD, axis=1)
-    below = jnp.pad(jnp.repeat(factor[:, 2:], HEAD, axis=1), ((0, 0), (0, HEAD)))
-    incoming = pl.pallas_call(
-        combine_kernel,
-        in_specs=[VMEM] * 3,
-        out_specs=VMEM,
-        out_shape=jax.ShapeDtypeStruct((128, 128), BF16),
-        compiler_params=PARAMS,
-        name="combine",
-    )(states, above, below)
-
-    out_own = w_own[:, 896:].reshape(64, 16, 384)
-    out_oth = w_oth[:, 896:].reshape(64, 16, 384)
+    out_own = w_own[:, 896:]
+    out_oth = swapped_cores(out_own).reshape(64, 16, 384)
+    out_own = out_own.reshape(64, 16, 384)
     w_out = jnp.where(
         c == 0, jnp.stack([out_own, out_oth], axis=1), jnp.stack([out_oth, out_own], axis=1)
     ).reshape(2048, 384)
     share = pl.pallas_call(
         back_kernel,
-        in_specs=[VMEM] * 5,
+        in_specs=[VMEM] * 4,
         out_specs=VMEM,
         out_shape=jax.ShapeDtypeStruct((SPAN, 2048), BF16),
         scratch_shapes=[pltpu.VMEM((SPAN, 384), BF16)],
         compiler_params=PARAMS,
         name="back",
-    )(parts, local, lifted, incoming, w_out)
+    )(parts, local, lifted, w_out)
     shares = lax.all_to_all(share.reshape(4, 64, 2048), "tp", 0, 0, tiled=True)
     return jnp.sum(shares.astype(F32), axis=0).astype(BF16)
 

time: 265 us -> 257 us (0.970)
  the two profiles are of different devices: /device:TPU:8 before, /device:TPU:40 now
where the time goes in v2:
time: 257 us; the launch traced here: 256 us
  waiting for transfers between devices  96.8 us (38%)
  starting transfers between devices  56.3 us (22%)
  Pallas kernels  38.8 us (15%)
  blocking collectives  22.2 us (9%)
  local copies, waits for them, and re-layouts  17.2 us (7%)
  between operations  13.8 us (5%)
  other arithmetic  10.8 us (4%)
    all_to_all x5, starting transfers between devices, copies_from(): lax.all_to_all(copies, axis, split_axis=0, concat_axis=0, tiled=True, axi...  45 us
    all_to_all x5, waiting for transfers between devices, copies_from(): lax.all_to_all(copies, axis, split_axis=0, concat_axis=0, tiled=True, axi...  36.1 us
    all_gather x1, waiting for transfers between devices, body(): w_own = lax.all_gather(w_row, 'z', axis=0, tiled=True)  34.7 us
    pallas_call x1, Pallas kernels, body(): pl.pallas_call(attend_kernel, in_specs=[SMEM] * 2 + [VMEM] * 5, out_specs...  24.3 us
    all_to_all x1, waiting for transfers between devices, body(): parts = lax.all_to_all(partial, 'z', 0, 0, tiled=True)  20.6 us
    all_to_all x1, blocking collectives, body(): shares = lax.all_to_all(share.reshape(4, 64, 2048), 'tp', 0, 0, tiled=True)  19.5 us
    ppermute x4, starting transfers between devices, swapped_cores(): return lax.ppermute(value, 'c', [(0, 1), (1, 0)])  7.66 us
    pallas_call x1, Pallas kernels, body(): pl.pallas_call(front_kernel, in_specs=[VMEM] * 6, out_specs=[VMEM] * 4, o...  5.25 us
  transfers between devices with their start and end apart: 12, of which 9 were waited for; matrix products, arithmetic and copies ran while one was open for 8% of the time, Pallas kernels for 0%

profile of v2, /device:TPU:40, one launch (start us, length us, event | category | flops | bytes accessed | tf_op | source)
XLA Modules:
  0.0 255.7 jit_solution(13614686778676177190)
XLA Ops:
  8.2 8.7 %all-to-all-start.3 = ((bf16[8,16,1280]{2,1,0:T(8,128)(2,1)}), bf16[8,16,1280]{2,1,0:T(8,128)(2,1)S(1)}, u32[]{:S(2)}, u32[]{:S(2)}) async-start(bf16[8,16,1280]{2,1,0:T(8,128)(2,1)} %broadcast_in_dim.117), calls=%async_computation.3 | async-start | bytes 655360 | tf_op jit(solution)/shard_map/all_to_all | solution.py:28
  19.0 4.2 %all-to-all-done.3 = bf16[8,16,1280]{2,1,0:T(8,128)(2,1)S(1)} async-done(((bf16[8,16,1280]{2,1,0:T(8,128)(2,1)}), bf16[8,16,1280]{2,1,0:T(8,128)(2,1)S(1)}, u32[]{:S(2)}, u32[]{:S(2)}) %all-to-all-start.3) | async-done | bytes 327712 | tf_op jit(solution)/shard_map/all_to_all | solution.py:28
  24.4 5.3 %all-to-all-start.2 = ((bf16[4,2,64,1024]{3,2,1,0:T(8,128)(2,1)}), bf16[4,2,64,1024]{3,2,1,0:T(8,128)(2,1)S(1)}, u32[]{:S(2)}, u32[]{:S(2)}) async-start(bf16[4,2,64,1024]{3,2,1,0:T(8,128)(2,1)} %broadcast_in_dim.116), calls=%async_computation.2 | async-start | bytes 2097152 | tf_op jit(solution)/shard_map/all_to_all | solution.py:28
  33.0 9.4 %all-to-all-done.2 = bf16[4,2,64,1024]{3,2,1,0:T(8,128)(2,1)S(1)} async-done(((bf16[4,2,64,1024]{3,2,1,0:T(8,128)(2,1)}), bf16[4,2,64,1024]{3,2,1,0:T(8,128)(2,1)S(1)}, u32[]{:S(2)}, u32[]{:S(2)}) %all-to-all-start.2) | async-done | bytes 1048608 | tf_op jit(solution)/shard_map/all_to_all | solution.py:28
  42.4 1.9 collective-permute-start
  47.3 34.7 %all-gather.5.cloned.1.call-done.weights = bf16[1024,1280]{1,0:T(8,128)(2,1)} async-done(((bf16[128,1280]{1,0:T(8,128)(2,1)}), bf16[1024,1280]{1,0:T(8,128)(2,1)}) %all-gather.5.cloned.1.call-update) | async-done | bytes 2621456 | tf_op jit(solution)/shard_map/all_gather | solution.py:240
  81.9 4.3 %project.1 = (f32[256,896]{1,0:T(8,128)}, f32[256,896]{1,0:T(8,128)}) custom-call(bf16[512,1024]{1,0:T(8,128)(2,1)} %pad_maximum_fusion.rows, bf16[1024,1280]{1,0:T(8,128)(2,1)} %all-gather.5.cloned.1.call-done.weights), custom_call_target="tpu_custom_call" | custom-call | tf_op jit(solution)/shard_map/project/pallas_call | solution.py:308
  86.2 1.9 collective-permute-start.1
  88.1 2.6 %all-gather.1 = f32[2,1,3]{2,1,0:T(1,128)S(1)} all-gather(f32[1,1,3]{2,1,0:T(1,128)S(1)} %bitcast.81), channel_id=1, replica_groups=mesh['z'=8,'y'=8,'c'=2,'tp'=4] {'c'}, dimensions={0}, use_global_device_ids=true | all-gather | bytes 36 | tf_op jit(solution)/shard_map/all_gather | solution.py:260
  95.2 5.2 %front.1 = (bf16[256,256]{1,0:T(8,128)(2,1)}, bf16[352,128]{1,0:T(8,128)(2,1)}, f32[256,192]{1,0:T(8,128)}, bf16[256,192]{1,0:T(8,128)(2,1)}) custom-call(f32[256,896]{1,0:T(8,128)} %get-tuple-element.11.first_part, f32[256,896]{1,0:T(8,128)} %copy-done.3, f32[256,32]{1,0:T(8,128)} %get-tuple-element.29.cosine, f32[256,32]{1,0:T(8,128)} %get-tuple-element.28.sine, ...), custom_call_target="tpu_custom_call" | custom-call | tf_op jit(solution)/shard_map/front/pallas_call | solution.py:317
  100.5 1.8 broadcast_in_dim.120
  102.3 11.7 %all-to-all-start.4 = ((bf16[8,352,128]{2,1,0:T(8,128)(2,1)}), bf16[8,352,128]{2,1,0:T(8,128)(2,1)S(1)}, u32[]{:S(2)}, u32[]{:S(2)}) async-start(bf16[8,352,128]{2,1,0:T(8,128)(2,1)} %broadcast_in_dim.120), calls=%async_computation.4 | async-start | bytes 1441792 | tf_op jit(solution)/shard_map/all_to_all | solution.py:28
  117.4 15.7 %all-to-all-done.4.kv_own = bf16[8,352,128]{2,1,0:T(8,128)(2,1)S(1)} async-done(((bf16[8,352,128]{2,1,0:T(8,128)(2,1)}), bf16[8,352,128]{2,1,0:T(8,128)(2,1)S(1)}, u32[]{:S(2)}, u32[]{:S(2)}) %all-to-all-start.4) | async-done | bytes 720928 | tf_op jit(solution)/shard_map/all_to_all | solution.py:28
  133.7 11.1 %all-to-all-start = ((f32[8,2,3]{2,1,0:T(2,128)}), f32[8,2,3]{2,1,0:T(2,128)S(1)}, u32[]{:S(2)}, u32[]{:S(2)}) async-start(f32[8,2,3]{2,1,0:T(2,128)} %broadcast_in_dim.111), calls=%async_computation | async-start | bytes 16384 | tf_op jit(solution)/shard_map/all_to_all | solution.py:28
  144.8 1.9 collective-permute-start.2
  148.8 8.3 %all-to-all-start.1 = ((f32[8,8,2,3]{1,2,3,0:T(2,128)}), f32[8,8,2,3]{1,2,3,0:T(2,128)S(1)}, u32[]{:S(2)}, u32[]{:S(2)}) async-start(f32[8,8,2,3]{1,2,3,0:T(2,128)} %broadcast_in_dim.112), calls=%async_computation.1 | async-start | bytes 49152 | tf_op jit(solution)/shard_map/all_to_all | solution.py:28
  158.7 6.1 %all-to-all-done.1 = f32[8,8,2,3]{1,2,3,0:T(2,128)S(1)} async-done(((f32[8,8,2,3]{1,2,3,0:T(2,128)}), f32[8,8,2,3]{1,2,3,0:T(2,128)S(1)}, u32[]{:S(2)}, u32[]{:S(2)}) %all-to-all-start.1) | async-done | bytes 1568 | tf_op jit(solution)/shard_map/all_to_all | solution.py:28
  167.2 24.3 %attend.1 = bf16[8,256,256]{2,1,0:T(8,128)(2,1)} custom-call(s32[68]{0:T(128)} %concatenate.15.plan, f32[384]{0:T(512)} %select_n.110.fade, bf16[8,256,256]{2,1,0:T(8,128)(2,1)} %bitcast.68, bf16[8,3,64,256]{3,2,1,0:T(8,128)(2,1)} %maximum_maximum_fusion.query_gate, bf16[8,352,128]{2,1,0:T(8,128)(2,1)} %copy-done.1, bf16[8,352,128]{2,1,0:T(8,128)(2,1)} %copy-done.4, ...), custom_call_target="tpu_custom_call" | custom-call | tf_op jit(solution)/shard_map/attend/pallas_call | solution.py:336
  191.5 3.6 %all-to-all-start.5 = ((bf16[8,256,256]{2,1,0:T(8,128)(2,1)}), bf16[8,256,256]{2,1,0:T(8,128)(2,1)S(1)}, u32[]{:S(2)}, u32[]{:S(2)}) async-start(bf16[8,256,256]{2,1,0:T(8,128)(2,1)} %attend.1), calls=%async_computation.5 | async-start | bytes 2097152 | tf_op jit(solution)/shard_map/all_to_all | solution.py:350
  196.3 1.9 collective-permute-start.3
  198.2 2.3 collective-permute-done.3
  201.8 20.6 %all-to-all-done.5.parts = bf16[8,256,256]{2,1,0:T(8,128)(2,1)S(1)} async-done(((bf16[8,256,256]{2,1,0:T(8,128)(2,1)}), bf16[8,256,256]{2,1,0:T(8,128)(2,1)S(1)}, u32[]{:S(2)}, u32[]{:S(2)}) %all-to-all-start.5) | async-done | bytes 1048608 | tf_op jit(solution)/shard_map/all_to_all | solution.py:350
  223.4 5.0 %back.1 = bf16[256,2048]{1,0:T(8,128)(2,1)} custom-call(bf16[8,256,256]{2,1,0:T(8,128)(2,1)} %copy-done, f32[256,192]{1,0:T(8,128)} %get-tuple-element.15.local, bf16[256,192]{1,0:T(8,128)(2,1)} %get-tuple-element.16.lifted, bf16[2048,384]{1,0:T(8,128)(2,1)} %bitcast.61), custom_call_target="tpu_custom_call" | custom-call | tf_op jit(solution)/shard_map/back/pallas_call | solution.py:358
  228.4 19.5 %all_to_all.35 = bf16[4,64,2048]{2,1,0:T(8,128)(2,1)S(1)} all-to-all(bf16[4,64,2048]{2,1,0:T(8,128)(2,1)} %bitcast.62), channel_id=1, replica_groups=mesh['z'=8,'y'=8,'c'=2,'tp'=4] {'tp'}, dimensions={0} | all-to-all | bytes 2097152 | tf_op jit(solution)/shard_map/all_to_all | solution.py:367
  (104 shorter events, 30.0 us)
Async XLA Ops:
  6.5 11.9 %copy-start.6 = (f32[2048]{0:T(1024)S(1)}, f32[2048]{0:T(1024)}, u32[]{:S(2)}) copy-start(f32[2048]{0:T(1024)} %param.13) | copy-start | bytes 24580
  8.2 15.1 %all-to-all-start.3 = ((bf16[8,16,1280]{2,1,0:T(8,128)(2,1)}), bf16[8,16,1280]{2,1,0:T(8,128)(2,1)S(1)}, u32[]{:S(2)}, u32[]{:S(2)}) async-start(bf16[8,16,1280]{2,1,0:T(8,128)(2,1)} %broadcast_in_dim.117), calls=%async_computation.3 | async-start | bytes 655360 | tf_op jit(solution)/shard_map/all_to_all | solution.py:28
  19.0 11.4 %copy-start.5 = (f32[3,32768]{1,0:T(4,128)S(1)}, f32[3,32768]{1,0:T(4,128)}, u32[]{:S(2)}) copy-start(f32[3,32768]{1,0:T(4,128)} %param.23) | copy-start | bytes 1179652
  23.3 1.1 copy-start.2
  24.4 6.2 %copy-start.7 = (f32[256,3]{0,1:T(4,128)S(1)}, f32[256,3]{0,1:T(4,128)}, u32[]{:S(2)}) copy-start(f32[256,3]{0,1:T(4,128)} %param.22) | copy-start | bytes 9220
  24.4 17.9 %all-to-all-start.2 = ((bf16[4,2,64,1024]{3,2,1,0:T(8,128)(2,1)}), bf16[4,2,64,1024]{3,2,1,0:T(8,128)(2,1)S(1)}, u32[]{:S(2)}, u32[]{:S(2)}) async-start(bf16[4,2,64,1024]{3,2,1,0:T(8,128)(2,1)} %broadcast_in_dim.116), calls=%async_computation.2 | async-start | bytes 2097152 | tf_op jit(solution)/shard_map/all_to_all | solution.py:28
  29.7 52.3 %all-gather.5.cloned.1.call-start = ((), (), s32[]{:S(2)}) async-start(), calls=%async_computation.7 | async-start | bytes 2949120 | tf_op jit(solution)/shard_map/all_gather | solution.py:240
  42.4 3.8 %collective-permute-start = (bf16[256,1024]{1,0:T(8,128)(2,1)S(1)}, bf16[256,1024]{1,0:T(8,128)(2,1)S(1)}, u32[]{:S(2)}, u32[]{:S(2)}) collective-permute-start(bf16[256,1024]{1,0:T(8,128)(2,1)S(1)} %bitcast.70), channel_id=1, source_target_pairs={{0,4},{4,0},{1,5},{5,1},{2,6},{6,2},{3,7},{7,3},{8,12},{12,8},{9,1... | collective-permute-start | bytes 1572872 | tf_op jit(solution)/shard_map/ppermute | solution.py:34
  86.2 8.1 %collective-permute-start.1 = (f32[256,896]{1,0:T(8,128)}, f32[256,896]{1,0:T(8,128)S(1)}, u32[]{:S(2)}, u32[]{:S(2)}) collective-permute-start(f32[256,896]{1,0:T(8,128)} %get-tuple-element.12), channel_id=1, source_target_pairs={{0,4},{4,0},{1,5},{5,1},{2,6},{6,2},{3,7},{7,3},{8,12},{12,8},{9,1... | collective-permute-start | bytes 2752520 | tf_op jit(solution)/shard_map/ppermute | solution.py:34
  94.3 0.9 copy-start.3
  102.3 30.8 %all-to-all-start.4 = ((bf16[8,352,128]{2,1,0:T(8,128)(2,1)}), bf16[8,352,128]{2,1,0:T(8,128)(2,1)S(1)}, u32[]{:S(2)}, u32[]{:S(2)}) async-start(bf16[8,352,128]{2,1,0:T(8,128)(2,1)} %broadcast_in_dim.120), calls=%async_computation.4 | async-start | bytes 1441792 | tf_op jit(solution)/shard_map/all_to_all | solution.py:28
  114.1 52.3 %all-gather.7.cloned.1.call-start = ((), (), s32[]{:S(2)}) async-start(), calls=%async_computation.8 | async-start | bytes 1179648 | tf_op jit(solution)/shard_map/all_gather | solution.py:332
  133.1 33.3 %copy-start.1 = (bf16[8,352,128]{2,1,0:T(8,128)(2,1)}, bf16[8,352,128]{2,1,0:T(8,128)(2,1)S(1)}, u32[]{:S(2)}) copy-start(bf16[8,352,128]{2,1,0:T(8,128)(2,1)S(1)} %all-to-all-done.4.kv_own) | copy-start | bytes 2162692
  133.7 14.3 %all-to-all-start = ((f32[8,2,3]{2,1,0:T(2,128)}), f32[8,2,3]{2,1,0:T(2,128)S(1)}, u32[]{:S(2)}, u32[]{:S(2)}) async-start(f32[8,2,3]{2,1,0:T(2,128)} %broadcast_in_dim.111), calls=%async_computation | async-start | bytes 16384 | tf_op jit(solution)/shard_map/all_to_all | solution.py:28
  144.8 21.6 %collective-permute-start.2 = (bf16[8,352,128]{2,1,0:T(8,128)(2,1)S(1)}, bf16[8,352,128]{2,1,0:T(8,128)(2,1)S(1)}, u32[]{:S(2)}, u32[]{:S(2)}) collective-permute-start(bf16[8,352,128]{2,1,0:T(8,128)(2,1)S(1)} %all-to-all-done.4.kv_own), channel_id=1, source_target_pairs={{0,4},{4,0},{1,5},{5,1},{2,6},{6,2},{3,7},{7,3},{8,12},{12,8},{9,1... | collective-permute-start | bytes 2162696 | tf_op jit(solution)/shard_map/ppermute | solution.py:34
  148.8 16.1 %all-to-all-start.1 = ((f32[8,8,2,3]{1,2,3,0:T(2,128)}), f32[8,8,2,3]{1,2,3,0:T(2,128)S(1)}, u32[]{:S(2)}, u32[]{:S(2)}) async-start(f32[8,8,2,3]{1,2,3,0:T(2,128)} %broadcast_in_dim.112), calls=%async_computation.1 | async-start | bytes 49152 | tf_op jit(solution)/shard_map/all_to_all | solution.py:28
  166.3 0.9 copy-start.4
  191.5 30.9 %all-to-all-start.5 = ((bf16[8,256,256]{2,1,0:T(8,128)(2,1)}), bf16[8,256,256]{2,1,0:T(8,128)(2,1)S(1)}, u32[]{:S(2)}, u32[]{:S(2)}) async-start(bf16[8,256,256]{2,1,0:T(8,128)(2,1)} %attend.1), calls=%async_computation.5 | async-start | bytes 2097152 | tf_op jit(solution)/shard_map/all_to_all | solution.py:350
  196.3 4.2 %collective-permute-start.3 = (bf16[1024,384]{1,0:T(8,128)(2,1)S(1)}, bf16[1024,384]{1,0:T(8,128)(2,1)S(1)}, u32[]{:S(2)}, u32[]{:S(2)}) collective-permute-start(bf16[1024,384]{1,0:T(8,128)(2,1)S(1)} %slice.30), channel_id=1, source_target_pairs={{0,4},{4,0},{1,5},{5,1},{2,6},{6,2},{3,7},{7,3},{8,12},{12,8},{9,1... | collective-permute-start | bytes 2359304 | tf_op jit(solution)/shard_map/ppermute | solution.py:34
  222.4 1.0 copy-start
Sparse Core Ops, SparseCore 0:
  32.5 49.3 all-gather.4
  116.9 40.3 all-gather.6

commit v3 on v2

--- a/solution.py
+++ b/solution.py
@@ -48,51 +48,54 @@
     oth_out[...] = product[SPAN:]
 
 
-def front_kernel(
-    first_part, second_part, cosine, sine, decay, decay_row, q_out, kv_out, local_out, lifted_out, proj
-):
-    proj[...] = first_part[...] + second_part[...]
+def turned(proj, at, cos, sin):
+    first = proj[:, at : at + 32]
+    second = proj[:, at + 32 : at + 64]
+    return jnp.concatenate([first * cos - second * sin, first * sin + second * cos], axis=1)
+
+
+def front_kernel(first_part, second_part, cosine, sine, decay, q_out, kv_out, proj_out):
+    proj_out[...] = first_part[...] + second_part[...]
+    cos = cosine[...]
+    sin = sine[...]
+    for h in range(3):
+        key = turned(proj_out, 192 + h * HEAD, cos, sin).astype(BF16)
+        value = proj_out[:, 384 + h * HEAD : 384 + (h + 1) * HEAD].astype(BF16)
+        column = decay[:, h : h + 1]
+        last = decay[SPAN - 1 : SPAN, h : h + 1]
+        faded = (key.astype(F32) * jnp.exp(last - column)).astype(BF16)
+        update = lax.dot_general(faded, value, TN, preferred_element_type=F32).astype(BF16)
+        kv_out[SPAN + 32 * h : SPAN + 32 * (h + 1)] = jnp.concatenate(
+            [update[:32], update[32:]], axis=1
+        )
+    q_out[192:] = jnp.zeros((HEAD, SPAN), BF16)
+    q_out[:192] = jnp.transpose(proj_out[:, 576:768] * (HEAD ** (-0.5) * LOG2E)).astype(BF16)
+    both = proj_out[:, 768:896]
+    flipped = jnp.transpose(both)[HEAD:, :].astype(BF16)
+    kv_out[:128] = jnp.concatenate([both[:128, :HEAD], both[128:, :HEAD]], axis=1).astype(BF16)
+    kv_out[128:SPAN] = jnp.concatenate([flipped[:, :128], flipped[:, 128:]], axis=0)
+
+
+def local_kernel(proj, cosine, sine, decay, decay_row, local_out, lifted_out):
     cos = cosine[...]
     sin = sine[...]
     place = lax.broadcasted_iota(jnp.int32, (SPAN, SPAN), 0)
     other = lax.broadcasted_iota(jnp.int32, (SPAN, SPAN), 1)
     causal = place >= other
-
-    def turned(at):
-        first = proj[:, at : at + 32]
-        second = proj[:, at + 32 : at + 64]
-        return jnp.concatenate(
-            [first * cos - second * sin, first * sin + second * cos], axis=1
-        )
-
     for h in range(3):
-        query = (turned(h * HEAD) * HEAD ** (-0.5)).astype(BF16)
-        key = turned(192 + h * HEAD).astype(BF16)
+        query = (turned(proj, h * HEAD, cos, sin) * HEAD ** (-0.5)).astype(BF16)
+        key = turned(proj, 192 + h * HEAD, cos, sin).astype(BF16)
         value = proj[:, 384 + h * HEAD : 384 + (h + 1) * HEAD].astype(BF16)
         column = decay[:, h : h + 1]
-        row = decay_row[h : h + 1, :]
-        last = decay[SPAN - 1 : SPAN, h : h + 1]
         scores = lax.dot_general(query, key, NT, preferred_element_type=F32)
-        gap = jnp.where(causal, column - row, 0.0)
+        gap = jnp.where(causal, column - decay_row[h : h + 1, :], 0.0)
         weights = jnp.where(causal, scores * jnp.exp(gap), 0.0).astype(BF16)
         local_out[:, h * HEAD : (h + 1) * HEAD] = jnp.dot(
             weights, value, preferred_element_type=F32
         )
-        faded = (key.astype(F32) * jnp.exp(last - column)).astype(BF16)
-        update = lax.dot_general(faded, value, TN, preferred_element_type=F32)
-        update = update.astype(BF16)
-        kv_out[SPAN + 32 * h : SPAN + 32 * (h + 1)] = jnp.concatenate(
-            [update[:32], update[32:]], axis=1
-        )
         lifted_out[:, h * HEAD : (h + 1) * HEAD] = (
             query.astype(F32) * jnp.exp(column)
         ).astype(BF16)
-    q_out[192:] = jnp.zeros((HEAD, SPAN), BF16)
-    q_out[:192] = jnp.transpose(proj[:, 576:768] * (HEAD ** (-0.5) * LOG2E)).astype(BF16)
-    both = proj[:, 768:896]
-    flipped = jnp.transpose(both)[HEAD:, :].astype(BF16)
-    kv_out[:128] = jnp.concatenate([both[:128, :HEAD], both[128:, :HEAD]], axis=1).astype(BF16)
-    kv_out[128:SPAN] = jnp.concatenate([flipped[:, :128], flipped[:, 128:]], axis=0)
 
 
 def attend_kernel(
@@ -222,6 +225,8 @@
     forget_total,
 ):
     z, y, c = (lax.axis_index("z"), lax.axis_index("y"), lax.axis_index("c"))
+    decay = jnp.cumsum(retain_log, axis=0)
+    ends = jnp.concatenate(three_parts(decay[-1]))
     shard = jnp.concatenate(
         [
             w_query_ret,
@@ -232,11 +237,13 @@
             w_value_att,
             w_out_ret.T,
             w_out_att.T,
+            jnp.pad(ends[None, :], ((0, 15), (0, 119))),
         ],
         axis=1,
     )
-    width = shard.shape[1]
-    w_row = copies_from(shard, "y").reshape(-1, width)
+    w_row = copies_from(shard, "y")
+    line_ends = jnp.sum(w_row[:, 0, 1280:1289].reshape(8, 3, 3).astype(F32), axis=1)
+    w_row = w_row[:, :, :1280].reshape(128, 1280)
     w_own = lax.all_gather(w_row, "z", axis=0, tiled=True)
 
     raw = tokens.astype(F32)
@@ -255,10 +262,14 @@
     inverse = THETA ** (-jnp.arange(32, dtype=F32) / 32)
     angles = positions[:, None] * inverse[None, :]
     cosine, sine = (jnp.cos(angles), jnp.sin(angles))
-    decay = jnp.cumsum(retain_log, axis=0)
     decay_row = jnp.pad(decay.T, ((0, 5), (0, 0)))
-    ends = lax.all_gather(decay[-1], "c")
-    ends = copies_from(copies_from(ends, "y"), "z").reshape(128, 3)
+    ends_own = copies_from(line_ends, "z")
+    ends_oth = swapped_cores(ends_own)
+    ends = jnp.where(
+        c == 0,
+        jnp.stack([ends_own, ends_oth], axis=2),
+        jnp.stack([ends_oth, ends_own], axis=2),
+    ).reshape(128, 3)
 
     gate = (forget_total * LOG2E).reshape(3, 8, 8, 2, SPAN)
     spans = jnp.arange(8, dtype=jnp.int32)
@@ -314,24 +325,36 @@
         compiler_params=PARAMS,
         name="project",
     )(rows, w_own)
-    q_send, kv_send, local, lifted = pl.pallas_call(
+    q_send, kv_send, proj = pl.pallas_call(
         front_kernel,
-        in_specs=[VMEM] * 6,
-        out_specs=[VMEM] * 4,
+        in_specs=[VMEM] * 5,
+        out_specs=[VMEM] * 3,
         out_shape=[
             jax.ShapeDtypeStruct((SPAN, SPAN), BF16),
             jax.ShapeDtypeStruct((SPAN + 96, 128), BF16),
-            jax.ShapeDtypeStruct((SPAN, 192), F32),
-            jax.ShapeDtypeStruct((SPAN, 192), BF16),
+            jax.ShapeDtypeStruct((SPAN, 896), F32),
         ],
-        scratch_shapes=[pltpu.VMEM((SPAN, 896), F32)],
         compiler_params=PARAMS,
         name="front",
-    )(own_part, swapped_cores(oth_part), cosine, sine, decay, decay_row)
+    )(own_part, swapped_cores(oth_part), cosine, sine, decay)
 
     queries = lax.all_gather(q_send, "z", axis=0)
     kv_own = copies_from(kv_send, ("z", "y"), SKEW)
     kv_oth = swapped_cores(kv_own)
+    local, lifted = pl.pallas_call(
+        local_kernel,
+        in_specs=[VMEM] * 5,
+        out_specs=[VMEM] * 2,
+        out_shape=[jax.ShapeDtypeStruct((SPAN, 192), F32), jax.ShapeDtypeStruct((SPAN, 192), BF16)],
+        compiler_params=PARAMS,
+        name="local",
+    )(proj, cosine, sine, decay, decay_row)
+    out_own = w_own[:, 896:]
+    out_oth = swapped_cores(out_own).reshape(64, 16, 384)
+    out_own = out_own.reshape(64, 16, 384)
+    w_out = jnp.where(
+        c == 0, jnp.stack([out_own, out_oth], axis=1), jnp.stack([out_oth, out_own], axis=1)
+    ).reshape(2048, 384)
 
     partial = pl.pallas_call(
         attend_kernel,
@@ -349,12 +372,6 @@
     )(plan, fade, queries, query_gate, kv_own, kv_oth, key_gate)
     parts = lax.all_to_all(partial, "z", 0, 0, tiled=True)
 
-    out_own = w_own[:, 896:]
-    out_oth = swapped_cores(out_own).reshape(64, 16, 384)
-    out_own = out_own.reshape(64, 16, 384)
-    w_out = jnp.where(
-        c == 0, jnp.stack([out_own, out_oth], axis=1), jnp.stack([out_oth, out_own], axis=1)
-    ).reshape(2048, 384)
     share = pl.pallas_call(
         back_kernel,
         in_specs=[VMEM] * 4,

time: 257 us -> 256 us (level)
  the two profiles are of different devices: /device:TPU:40 before, /device:TPU:48 now
where the time goes in v3:
time: 256 us; the launch traced here: 255 us
  waiting for transfers between devices  105 us (41%)
  starting transfers between devices  45.5 us (18%)
  Pallas kernels  42.4 us (17%)
  blocking collectives  19.4 us (8%)
  local copies, waits for them, and re-layouts  18.1 us (7%)
  between operations  13.8 us (5%)
  other arithmetic  11 us (4%)
    all_to_all x4, waiting for transfers between devices, copies_from(): lax.all_to_all(copies, axis, split_axis=0, concat_axis=0, tiled=True, axi...  51.4 us
    all_gather x1, waiting for transfers between devices, body(): w_own = lax.all_gather(w_row, 'z', axis=0, tiled=True)  32.1 us
    all_to_all x4, starting transfers between devices, copies_from(): lax.all_to_all(copies, axis, split_axis=0, concat_axis=0, tiled=True, axi...  30.8 us
    pallas_call x1, Pallas kernels, body(): pl.pallas_call(attend_kernel, in_specs=[SMEM] * 2 + [VMEM] * 5, out_specs...  24.7 us
    all_to_all x1, blocking collectives, body(): shares = lax.all_to_all(share.reshape(4, 64, 2048), 'tp', 0, 0, tiled=True)  19.4 us
    all_to_all x1, waiting for transfers between devices, body(): parts = lax.all_to_all(partial, 'z', 0, 0, tiled=True)  16.8 us
    ppermute x5, starting transfers between devices, swapped_cores(): return lax.ppermute(value, 'c', [(0, 1), (1, 0)])  9.57 us
    all_to_all x1, starting transfers between devices, body(): parts = lax.all_to_all(partial, 'z', 0, 0, tiled=True)  5.18 us
  transfers between devices with their start and end apart: 12, of which 9 were waited for; matrix products, arithmetic and copies ran while one was open for 7% of the time, Pallas kernels for 2%

profile of v3, /device:TPU:48, one launch (start us, length us, event | category | flops | bytes accessed | tf_op | source)
XLA Modules:
  0.0 255.0 jit_solution(12570957259672969630)
XLA Ops:
  10.5 8.6 %all-to-all-start = ((bf16[8,16,1408]{2,1,0:T(8,128)(2,1)}), bf16[8,16,1408]{2,1,0:T(8,128)(2,1)S(1)}, u32[]{:S(2)}, u32[]{:S(2)}) async-start(bf16[8,16,1408]{2,1,0:T(8,128)(2,1)} %broadcast_in_dim.112), calls=%async_computation | async-start | bytes 720896 | tf_op jit(solution)/shard_map/all_to_all | solution.py:28
  21.2 6.4 %all-to-all-done = bf16[8,16,1408]{2,1,0:T(8,128)(2,1)S(1)} async-done(((bf16[8,16,1408]{2,1,0:T(8,128)(2,1)}), bf16[8,16,1408]{2,1,0:T(8,128)(2,1)S(1)}, u32[]{:S(2)}, u32[]{:S(2)}) %all-to-all-start) | async-done | bytes 360480 | tf_op jit(solution)/shard_map/all_to_all | solution.py:28
  28.8 4.4 %all-to-all-start.2 = ((bf16[4,2,64,1024]{3,2,1,0:T(8,128)(2,1)}), bf16[4,2,64,1024]{3,2,1,0:T(8,128)(2,1)S(1)}, u32[]{:S(2)}, u32[]{:S(2)}) async-start(bf16[4,2,64,1024]{3,2,1,0:T(8,128)(2,1)} %broadcast_in_dim.117), calls=%async_computation.2 | async-start | bytes 2097152 | tf_op jit(solution)/shard_map/all_to_all | solution.py:28
  35.0 12.7 %all-to-all-done.2 = bf16[4,2,64,1024]{3,2,1,0:T(8,128)(2,1)S(1)} async-done(((bf16[4,2,64,1024]{3,2,1,0:T(8,128)(2,1)}), bf16[4,2,64,1024]{3,2,1,0:T(8,128)(2,1)S(1)}, u32[]{:S(2)}, u32[]{:S(2)}) %all-to-all-start.2) | async-done | bytes 1048608 | tf_op jit(solution)/shard_map/all_to_all | solution.py:28
  47.9 1.9 collective-permute-start.1
  49.9 1.8 collective-permute-done.1
  52.7 32.1 %all-gather.4.cloned.1.call-done.weights = bf16[1024,1280]{1,0:T(8,128)(2,1)} async-done(((bf16[128,1280]{1,0:T(8,128)(2,1)}), bf16[1024,1280]{1,0:T(8,128)(2,1)}) %all-gather.4.cloned.1.call-update) | async-done | bytes 2621456 | tf_op jit(solution)/shard_map/all_gather | solution.py:247
  84.8 4.3 %project.1 = (f32[256,896]{1,0:T(8,128)}, f32[256,896]{1,0:T(8,128)}) custom-call(bf16[512,1024]{1,0:T(8,128)(2,1)} %pad_maximum_fusion.rows, bf16[1024,1280]{1,0:T(8,128)(2,1)} %all-gather.4.cloned.1.call-done.weights), custom_call_target="tpu_custom_call" | custom-call | tf_op jit(solution)/shard_map/project/pallas_call | solution.py:319
  89.1 1.9 collective-permute-start.2
  95.4 4.4 %front.1 = (bf16[256,256]{1,0:T(8,128)(2,1)}, bf16[352,128]{1,0:T(8,128)(2,1)}, f32[256,896]{1,0:T(8,128)}) custom-call(f32[256,896]{1,0:T(8,128)} %get-tuple-element.12.first_part, f32[256,896]{1,0:T(8,128)} %copy-done.2, f32[256,32]{1,0:T(8,128)} %get-tuple-element.31.cosine, f32[256,32]{1,0:T(8,128)} %get-tuple-element.30.sine, f32[256,3]{1,0:T(8,128)} %copy.148.decay), custom_call_target="tpu_custom_call" | custom-call | tf_op jit(solution)/shard_map/front/pallas_call | solution.py:328
  99.7 1.9 broadcast_in_dim.120
  101.6 11.1 %all-to-all-start.3 = ((bf16[8,352,128]{2,1,0:T(8,128)(2,1)}), bf16[8,352,128]{2,1,0:T(8,128)(2,1)S(1)}, u32[]{:S(2)}, u32[]{:S(2)}) async-start(bf16[8,352,128]{2,1,0:T(8,128)(2,1)} %broadcast_in_dim.120), calls=%async_computation.3 | async-start | bytes 1441792 | tf_op jit(solution)/shard_map/all_to_all | solution.py:28
  116.0 24.4 %all-to-all-done.3.kv_own = bf16[8,352,128]{2,1,0:T(8,128)(2,1)S(1)} async-done(((bf16[8,352,128]{2,1,0:T(8,128)(2,1)}), bf16[8,352,128]{2,1,0:T(8,128)(2,1)S(1)}, u32[]{:S(2)}, u32[]{:S(2)}) %all-to-all-start.3) | async-done | bytes 720928 | tf_op jit(solution)/shard_map/all_to_all | solution.py:28
  140.5 1.9 collective-permute-start.3
  143.1 6.7 %all-to-all-start.1 = ((f32[8,8,3]{1,2,0:T(4,128)}), f32[8,8,3]{1,2,0:T(4,128)S(1)}, u32[]{:S(2)}, u32[]{:S(2)}) async-start(f32[8,8,3]{1,2,0:T(4,128)} %broadcast_in_dim.113), calls=%async_computation.1 | async-start | bytes 32768 | tf_op jit(solution)/shard_map/all_to_all | solution.py:28
  149.9 7.8 %all-to-all-done.1 = f32[8,8,3]{1,2,0:T(4,128)S(1)} async-done(((f32[8,8,3]{1,2,0:T(4,128)}), f32[8,8,3]{1,2,0:T(4,128)S(1)}, u32[]{:S(2)}, u32[]{:S(2)}) %all-to-all-start.1) | async-done | bytes 800 | tf_op jit(solution)/shard_map/all_to_all | solution.py:28
  157.7 1.9 collective-permute-start
  164.3 24.7 %attend.1 = bf16[8,256,256]{2,1,0:T(8,128)(2,1)} custom-call(s32[68]{0:T(128)} %concatenate.18.plan, f32[384]{0:T(512)} %select_n.125.fade, bf16[8,256,256]{2,1,0:T(8,128)(2,1)} %bitcast.72, bf16[8,3,64,256]{3,2,1,0:T(8,128)(2,1)} %maximum_maximum_fusion.query_gate, bf16[8,352,128]{2,1,0:T(8,128)(2,1)} %copy-done.1, bf16[8,352,128]{2,1,0:T(8,128)(2,1)} %copy-done.3, ...), custom_call_target="tpu_custom_call" | custom-call | tf_op jit(solution)/shard_map/attend/pallas_call | solution.py:359
  189.0 5.2 %all-to-all-start.4 = ((bf16[8,256,256]{2,1,0:T(8,128)(2,1)}), bf16[8,256,256]{2,1,0:T(8,128)(2,1)S(1)}, u32[]{:S(2)}, u32[]{:S(2)}) async-start(bf16[8,256,256]{2,1,0:T(8,128)(2,1)} %attend.1), calls=%async_computation.4 | async-start | bytes 2097152 | tf_op jit(solution)/shard_map/all_to_all | solution.py:373
  195.4 1.9 collective-permute-start.4
  200.9 4.0 %local.1 = (f32[256,192]{1,0:T(8,128)}, bf16[256,192]{1,0:T(8,128)(2,1)}) custom-call(f32[256,896]{1,0:T(8,128)} %get-tuple-element.16.proj, f32[256,32]{1,0:T(8,128)} %get-tuple-element.31.cosine, f32[256,32]{1,0:T(8,128)} %get-tuple-element.30.sine, f32[256,3]{1,0:T(8,128)} %copy.148.decay, f32[8,256]{1,0:T(8,128)} %pad.9.decay_row), custom_call_target="tpu_custom_call" | custom-call | tf_op jit(solution)/shard_map/local/pallas_call | solution.py:344
  205.0 16.8 %all-to-all-done.4.parts = bf16[8,256,256]{2,1,0:T(8,128)(2,1)S(1)} async-done(((bf16[8,256,256]{2,1,0:T(8,128)(2,1)}), bf16[8,256,256]{2,1,0:T(8,128)(2,1)S(1)}, u32[]{:S(2)}, u32[]{:S(2)}) %all-to-all-start.4) | async-done | bytes 1048608 | tf_op jit(solution)/shard_map/all_to_all | solution.py:373
  222.8 5.0 %back.1 = bf16[256,2048]{1,0:T(8,128)(2,1)} custom-call(bf16[8,256,256]{2,1,0:T(8,128)(2,1)} %copy-done, f32[256,192]{1,0:T(8,128)} %get-tuple-element.17.local, bf16[256,192]{1,0:T(8,128)(2,1)} %get-tuple-element.18.lifted, bf16[2048,384]{1,0:T(8,128)(2,1)} %bitcast.65), custom_call_target="tpu_custom_call" | custom-call | tf_op jit(solution)/shard_map/back/pallas_call | solution.py:375
  227.8 19.4 %all_to_all.30 = bf16[4,64,2048]{2,1,0:T(8,128)(2,1)S(1)} all-to-all(bf16[4,64,2048]{2,1,0:T(8,128)(2,1)} %bitcast.66), channel_id=1, replica_groups=mesh['z'=8,'y'=8,'c'=2,'tp'=4] {'tp'}, dimensions={0} | all-to-all | bytes 2097152 | tf_op jit(solution)/shard_map/all_to_all | solution.py:384
  (110 shorter events, 29.9 us)
Async XLA Ops:
  6.5 14.1 %copy-start.5 = (f32[2048]{0:T(1024)S(1)}, f32[2048]{0:T(1024)}, u32[]{:S(2)}) copy-start(f32[2048]{0:T(1024)} %param.13) | copy-start | bytes 24580
  10.5 17.1 %all-to-all-start = ((bf16[8,16,1408]{2,1,0:T(8,128)(2,1)}), bf16[8,16,1408]{2,1,0:T(8,128)(2,1)S(1)}, u32[]{:S(2)}, u32[]{:S(2)}) async-start(bf16[8,16,1408]{2,1,0:T(8,128)(2,1)} %broadcast_in_dim.112), calls=%async_computation | async-start | bytes 720896 | tf_op jit(solution)/shard_map/all_to_all | solution.py:28
  28.8 5.2 %copy-start.4 = (f32[3,32768]{1,0:T(4,128)S(1)}, f32[3,32768]{1,0:T(4,128)}, u32[]{:S(2)}) copy-start(f32[3,32768]{1,0:T(4,128)} %param.23) | copy-start | bytes 1179652
  28.8 19.0 %all-to-all-start.2 = ((bf16[4,2,64,1024]{3,2,1,0:T(8,128)(2,1)}), bf16[4,2,64,1024]{3,2,1,0:T(8,128)(2,1)S(1)}, u32[]{:S(2)}, u32[]{:S(2)}) async-start(bf16[4,2,64,1024]{3,2,1,0:T(8,128)(2,1)} %broadcast_in_dim.117), calls=%async_computation.2 | async-start | bytes 2097152 | tf_op jit(solution)/shard_map/all_to_all | solution.py:28
  33.2 51.7 %all-gather.4.cloned.1.call-start = ((), (), s32[]{:S(2)}) async-start(), calls=%async_computation.6 | async-start | bytes 2949120 | tf_op jit(solution)/shard_map/all_gather | solution.py:247
  47.9 3.8 %collective-permute-start.1 = (bf16[256,1024]{1,0:T(8,128)(2,1)S(1)}, bf16[256,1024]{1,0:T(8,128)(2,1)S(1)}, u32[]{:S(2)}, u32[]{:S(2)}) collective-permute-start(bf16[256,1024]{1,0:T(8,128)(2,1)S(1)} %bitcast.74), channel_id=1, source_target_pairs={{0,4},{4,0},{1,5},{5,1},{2,6},{6,2},{3,7},{7,3},{8,12},{12,8},{9,1... | collective-permute-start | bytes 1572872 | tf_op jit(solution)/shard_map/ppermute | solution.py:34
  89.1 5.3 %collective-permute-start.2 = (f32[256,896]{1,0:T(8,128)}, f32[256,896]{1,0:T(8,128)S(1)}, u32[]{:S(2)}, u32[]{:S(2)}) collective-permute-start(f32[256,896]{1,0:T(8,128)} %get-tuple-element.13), channel_id=1, source_target_pairs={{0,4},{4,0},{1,5},{5,1},{2,6},{6,2},{3,7},{7,3},{8,12},{12,8},{9,1... | collective-permute-start | bytes 2752520 | tf_op jit(solution)/shard_map/ppermute | solution.py:34
  94.4 0.9 copy-start.2
  101.6 38.9 %all-to-all-start.3 = ((bf16[8,352,128]{2,1,0:T(8,128)(2,1)}), bf16[8,352,128]{2,1,0:T(8,128)(2,1)S(1)}, u32[]{:S(2)}, u32[]{:S(2)}) async-start(bf16[8,352,128]{2,1,0:T(8,128)(2,1)} %broadcast_in_dim.120), calls=%async_computation.3 | async-start | bytes 1441792 | tf_op jit(solution)/shard_map/all_to_all | solution.py:28
  112.7 50.6 %all-gather.6.cloned.1.call-start = ((), (), s32[]{:S(2)}) async-start(), calls=%async_computation.7 | async-start | bytes 1179648 | tf_op jit(solution)/shard_map/all_gather | solution.py:341
  140.5 22.9 %copy-start.1 = (bf16[8,352,128]{2,1,0:T(8,128)(2,1)}, bf16[8,352,128]{2,1,0:T(8,128)(2,1)S(1)}, u32[]{:S(2)}) copy-start(bf16[8,352,128]{2,1,0:T(8,128)(2,1)S(1)} %all-to-all-done.3.kv_own) | copy-start | bytes 2162692
  140.5 22.8 %collective-permute-start.3 = (bf16[8,352,128]{2,1,0:T(8,128)(2,1)S(1)}, bf16[8,352,128]{2,1,0:T(8,128)(2,1)S(1)}, u32[]{:S(2)}, u32[]{:S(2)}) collective-permute-start(bf16[8,352,128]{2,1,0:T(8,128)(2,1)S(1)} %all-to-all-done.3.kv_own), channel_id=1, source_target_pairs={{0,4},{4,0},{1,5},{5,1},{2,6},{6,2},{3,7},{7,3},{8,12},{12,8},{9,1... | collective-permute-start | bytes 2162696 | tf_op jit(solution)/shard_map/ppermute | solution.py:34
  143.1 14.6 %all-to-all-start.1 = ((f32[8,8,3]{1,2,0:T(4,128)}), f32[8,8,3]{1,2,0:T(4,128)S(1)}, u32[]{:S(2)}, u32[]{:S(2)}) async-start(f32[8,8,3]{1,2,0:T(4,128)} %broadcast_in_dim.113), calls=%async_computation.1 | async-start | bytes 32768 | tf_op jit(solution)/shard_map/all_to_all | solution.py:28
  157.7 3.7 %collective-permute-start = (f32[8,8,3]{1,2,0:T(4,128)S(1)}, f32[8,8,3]{1,2,0:T(4,128)S(1)}, u32[]{:S(2)}, u32[]{:S(2)}) collective-permute-start(f32[8,8,3]{1,2,0:T(4,128)S(1)} %all-to-all-done.1), channel_id=1, source_target_pairs={{0,4},{4,0},{1,5},{5,1},{2,6},{6,2},{3,7},{7,3},{8,12},{12,8},{9,1... | collective-permute-start | bytes 2312 | tf_op jit(solution)/shard_map/ppermute | solution.py:34
  163.3 0.9 copy-start.3
  189.0 32.8 %all-to-all-start.4 = ((bf16[8,256,256]{2,1,0:T(8,128)(2,1)}), bf16[8,256,256]{2,1,0:T(8,128)(2,1)S(1)}, u32[]{:S(2)}, u32[]{:S(2)}) async-start(bf16[8,256,256]{2,1,0:T(8,128)(2,1)} %attend.1), calls=%async_computation.4 | async-start | bytes 2097152 | tf_op jit(solution)/shard_map/all_to_all | solution.py:373
  195.4 4.2 %collective-permute-start.4 = (bf16[1024,384]{1,0:T(8,128)(2,1)S(1)}, bf16[1024,384]{1,0:T(8,128)(2,1)S(1)}, u32[]{:S(2)}, u32[]{:S(2)}) collective-permute-start(bf16[1024,384]{1,0:T(8,128)(2,1)S(1)} %slice.40), channel_id=1, source_target_pairs={{0,4},{4,0},{1,5},{5,1},{2,6},{6,2},{3,7},{7,3},{8,12},{12,8},{9,1... | collective-permute-start | bytes 2359304 | tf_op jit(solution)/shard_map/ppermute | solution.py:34
  221.8 1.0 copy-start
Sparse Core Ops, SparseCore 0:
  36.1 48.7 all-gather.3
  115.6 47.7 all-gather.5

commit v4 on v3

--- a/solution.py
+++ b/solution.py
@@ -14,7 +14,7 @@
 LOG2E = 1.4426950408889634
 F32 = jnp.float32
 BF16 = jnp.bfloat16
-SKEW = [[((m - y) % 8) * 8 + y for y in range(8)] for m in range(8)]
+ROTATION = [(z * 8 + y, ((z + y) % 8) * 8 + y) for z in range(8) for y in range(8)]
 NT = (((1,), (1,)), ((), ()))
 TN = (((0,), (0,)), ((), ()))
 VMEM = pl.BlockSpec(memory_space=pltpu.VMEM)
@@ -22,12 +22,9 @@
 PARAMS = pltpu.CompilerParams(vmem_limit_bytes=56 * 1024 * 1024)
 
 
-def copies_from(shard, axis, groups=None):
-    count = len(groups[0]) if groups else lax.axis_size(axis)
-    copies = jnp.broadcast_to(shard, (count, *shard.shape))
-    return lax.all_to_all(
-        copies, axis, split_axis=0, concat_axis=0, tiled=True, axis_index_groups=groups
-    )
+def copies_from(shard, axis):
+    copies = jnp.broadcast_to(shard, (lax.axis_size(axis), *shard.shape))
+    return lax.all_to_all(copies, axis, split_axis=0, concat_axis=0, tiled=True)
 
 
 def swapped_cores(value):
@@ -99,9 +96,21 @@
 
 
 def attend_kernel(
-    plan, fade, received, query_gate, kv_own, kv_oth, key_gate, out, keys, values, queries, total
+    plan,
+    fade,
+    received,
+    query_gate,
+    kv_own,
+    kv_oth,
+    key_gate,
+    out,
+    keys,
+    values,
+    queries,
+    total,
+    even,
+    odd,
 ):
-    mine_z, mine_y, mine_c = (plan[65], plan[66], plan[67])
     extra = lax.broadcasted_iota(jnp.int32, (16, 2 * SPAN), 0)
     ones = jnp.where(extra == 0, 1.0, 0.0).astype(BF16)
     for y in range(8):
@@ -122,43 +131,44 @@
 
     place = lax.broadcasted_iota(jnp.int32, (2 * SPAN, SPAN), 0)
     wanted = lax.broadcasted_iota(jnp.int32, (2 * SPAN, SPAN), 1)
-    allowed = place <= jnp.where(place < SPAN, wanted, mine_c * (4 * SPAN) - 1)
+    allowed = place <= jnp.where(place < SPAN, wanted, plan[66] * (4 * SPAN) - 1)
+
+    def weigh(i, held, h):
+        z, y = (plan[i] // 8, plan[i] % 8)
+        at = h * SPAN
+        total[z, :, at : at + SPAN] += jnp.dot(
+            values[y], held[:, at : at + SPAN], preferred_element_type=F32
+        )
+
+    def score(i, held, h, mask=None):
+        z, y = (plan[i] // 8, plan[i] % 8)
+        for at in (0, SPAN):
+            weights = jnp.exp2(
+                jnp.dot(keys[y, at : at + SPAN], queries[z, h], preferred_element_type=F32)
+            )
+            if mask is not None:
+                weights = jnp.where(mask[at : at + SPAN], weights, 0.0)
+            held[at : at + SPAN, h * SPAN : (h + 1) * SPAN] = weights.astype(BF16)
+
     for h in range(3):
-        scores = jnp.dot(keys[mine_y], queries[mine_z, h], preferred_element_type=F32)
-        weights = jnp.where(allowed, jnp.exp2(scores), 0.0).astype(BF16)
-        total[mine_z, :, h * SPAN : (h + 1) * SPAN] += jnp.dot(
-            values[mine_y], weights, preferred_element_type=F32
-        )
-
-    def units(places):
-        at = []
-        for i in places:
-            code = plan[i]
-            at.append((code // 8, code % 8))
-        chunks = [(z, y, h) for z, y in at for h in range(3)]
-
-        def scored(z, y, h):
-            return jnp.dot(keys[y], queries[z, h], preferred_element_type=F32)
-
-        ready = scored(*chunks[0])
-        for n, (z, y, h) in enumerate(chunks):
-            ahead = scored(*chunks[n + 1]) if n + 1 < len(chunks) else None
-            weights = jnp.exp2(ready).astype(BF16)
-            total[z, :, h * SPAN : (h + 1) * SPAN] += jnp.dot(
-                values[y], weights, preferred_element_type=F32
-            )
-            ready = ahead
+        score(0, even, h, allowed)
 
     def pair(i, carry):
-        units((2 * i, 2 * i + 1))
+        for h in range(3):
+            score(2 * i + 1, odd, h)
+            weigh(2 * i, even, h)
+        for h in range(3):
+            score(2 * i + 2, even, h)
+            weigh(2 * i + 1, odd, h)
         return carry
 
-    count = plan[64]
+    count = plan[65]
     lax.fori_loop(0, count // 2, pair, 0)
 
     @pl.when(count % 2 == 1)
     def _():
-        units((count - 1,))
+        for h in range(3):
+            weigh(count - 1, even, h)
 
     for z in range(8):
         rows = []
@@ -273,7 +283,7 @@
 
     gate = (forget_total * LOG2E).reshape(3, 8, 8, 2, SPAN)
     spans = jnp.arange(8, dtype=jnp.int32)
-    key_z = (z + y - spans) % 8
+    key_z = (z - spans) % 8
     chosen = (spans[:, None] == key_z[None, :])[None, :, :, None, None]
     key_side = jnp.sum(jnp.where(chosen, gate, 0.0), axis=1)
     key_side = jnp.where(c == 0, key_side, key_side[:, :, ::-1])
@@ -314,7 +324,8 @@
     units = jnp.sum(
         jnp.where(needed[None, :] & (slot[None, :] == order[:, None]), order[None, :], 0), axis=1
     )
-    plan = jnp.concatenate([units, jnp.stack([jnp.sum(needed.astype(jnp.int32)), z, y, c])])
+    own = jnp.stack([(z - y) % 8 * 8 + y])
+    plan = jnp.concatenate([own, units, jnp.stack([jnp.sum(needed.astype(jnp.int32)) + 1, c])])
 
     own_part, oth_part = pl.pallas_call(
         project_kernel,
@@ -339,7 +350,7 @@
     )(own_part, swapped_cores(oth_part), cosine, sine, decay)
 
     queries = lax.all_gather(q_send, "z", axis=0)
-    kv_own = copies_from(kv_send, ("z", "y"), SKEW)
+    kv_own = copies_from(lax.ppermute(kv_send, ("z", "y"), ROTATION), "y")
     kv_oth = swapped_cores(kv_own)
     local, lifted = pl.pallas_call(
         local_kernel,
@@ -366,6 +377,8 @@
             pltpu.VMEM((8, 80, 2 * SPAN), BF16),
             pltpu.VMEM((8, 3, 128, SPAN), BF16),
             pltpu.VMEM((8, 80, 3 * SPAN), F32),
+            pltpu.VMEM((2 * SPAN, 3 * SPAN), BF16),
+            pltpu.VMEM((2 * SPAN, 3 * SPAN), BF16),
         ],
         compiler_params=PARAMS,
         name="attend",

time: 256 us -> 242 us (0.945)
  the two profiles are of different devices: /device:TPU:48 before, /device:TPU:2 now
where the time goes in v4:
time: 242 us; the launch traced here: 241 us
  waiting for transfers between devices  99.7 us (41%)
  starting transfers between devices  49.5 us (20%)
  Pallas kernels  33.8 us (14%)
  blocking collectives  16.1 us (7%)
  local copies, waits for them, and re-layouts  16 us (7%)
  between operations  14.3 us (6%)
  other arithmetic  11.6 us (5%)
    all_to_all x4, waiting for transfers between devices, copies_from(): return lax.all_to_all(copies, axis, split_axis=0, concat_axis=0, tiled=True)  47.3 us
    all_to_all x4, starting transfers between devices, copies_from(): return lax.all_to_all(copies, axis, split_axis=0, concat_axis=0, tiled=True)  34.2 us
    all_gather x1, waiting for transfers between devices, body(): w_own = lax.all_gather(w_row, 'z', axis=0, tiled=True)  29.9 us
    pallas_call x1, Pallas kernels, body(): pl.pallas_call(attend_kernel, in_specs=[SMEM] * 2 + [VMEM] * 5, out_specs...  16.1 us
    all_to_all x1, blocking collectives, body(): shares = lax.all_to_all(share.reshape(4, 64, 2048), 'tp', 0, 0, tiled=True)  16.1 us
    all_to_all x1, waiting for transfers between devices, body(): parts = lax.all_to_all(partial, 'z', 0, 0, tiled=True)  15.6 us
    ppermute x5, starting transfers between devices, swapped_cores(): return lax.ppermute(value, 'c', [(0, 1), (1, 0)])  9.75 us
    pallas_call x1, Pallas kernels, body(): pl.pallas_call(back_kernel, in_specs=[VMEM] * 4, out_specs=VMEM, out_shap...  5.02 us
  transfers between devices with their start and end apart: 13, of which 10 were waited for; matrix products, arithmetic and copies ran while one was open for 7% of the time, Pallas kernels for 2%

profile of v4, /device:TPU:2, one launch (start us, length us, event | category | flops | bytes accessed | tf_op | source)
XLA Modules:
  0.0 241.0 jit_solution(2431234421273560720)
XLA Ops:
  10.5 7.1 %all-to-all-start = ((bf16[8,16,1408]{2,1,0:T(8,128)(2,1)}), bf16[8,16,1408]{2,1,0:T(8,128)(2,1)S(1)}, u32[]{:S(2)}, u32[]{:S(2)}) async-start(bf16[8,16,1408]{2,1,0:T(8,128)(2,1)} %broadcast_in_dim.112), calls=%async_computation | async-start | bytes 720896 | tf_op jit(solution)/shard_map/all_to_all | solution.py:27
  19.7 11.9 %all-to-all-done = bf16[8,16,1408]{2,1,0:T(8,128)(2,1)S(1)} async-done(((bf16[8,16,1408]{2,1,0:T(8,128)(2,1)}), bf16[8,16,1408]{2,1,0:T(8,128)(2,1)S(1)}, u32[]{:S(2)}, u32[]{:S(2)}) %all-to-all-start) | async-done | bytes 360480 | tf_op jit(solution)/shard_map/all_to_all | solution.py:27
  32.7 5.0 %all-to-all-start.2 = ((bf16[4,2,64,1024]{3,2,1,0:T(8,128)(2,1)}), bf16[4,2,64,1024]{3,2,1,0:T(8,128)(2,1)S(1)}, u32[]{:S(2)}, u32[]{:S(2)}) async-start(bf16[4,2,64,1024]{3,2,1,0:T(8,128)(2,1)} %broadcast_in_dim.117), calls=%async_computation.2 | async-start | bytes 2097152 | tf_op jit(solution)/shard_map/all_to_all | solution.py:27
  39.5 11.0 %all-to-all-done.2 = bf16[4,2,64,1024]{3,2,1,0:T(8,128)(2,1)S(1)} async-done(((bf16[4,2,64,1024]{3,2,1,0:T(8,128)(2,1)}), bf16[4,2,64,1024]{3,2,1,0:T(8,128)(2,1)S(1)}, u32[]{:S(2)}, u32[]{:S(2)}) %all-to-all-start.2) | async-done | bytes 1048608 | tf_op jit(solution)/shard_map/all_to_all | solution.py:27
  50.6 1.9 collective-permute-start.1
  52.6 1.8 collective-permute-done.1
  55.4 29.9 %all-gather.4.cloned.1.call-done.weights = bf16[1024,1280]{1,0:T(8,128)(2,1)} async-done(((bf16[128,1280]{1,0:T(8,128)(2,1)}), bf16[1024,1280]{1,0:T(8,128)(2,1)}) %all-gather.4.cloned.1.call-update) | async-done | bytes 2621456 | tf_op jit(solution)/shard_map/all_gather | solution.py:257
  85.4 4.2 %project.1 = (f32[256,896]{1,0:T(8,128)}, f32[256,896]{1,0:T(8,128)}) custom-call(bf16[512,1024]{1,0:T(8,128)(2,1)} %pad_maximum_fusion.rows, bf16[1024,1280]{1,0:T(8,128)(2,1)} %all-gather.4.cloned.1.call-done.weights), custom_call_target="tpu_custom_call" | custom-call | tf_op jit(solution)/shard_map/project/pallas_call | solution.py:330
  89.6 1.9 collective-permute-start.2
  95.9 4.4 %front.1 = (bf16[256,256]{1,0:T(8,128)(2,1)}, bf16[352,128]{1,0:T(8,128)(2,1)}, f32[256,896]{1,0:T(8,128)}) custom-call(f32[256,896]{1,0:T(8,128)} %get-tuple-element.12.first_part, f32[256,896]{1,0:T(8,128)} %copy-done.2, f32[256,32]{1,0:T(8,128)} %get-tuple-element.31.cosine, f32[256,32]{1,0:T(8,128)} %get-tuple-element.30.sine, f32[256,3]{1,0:T(8,128)} %copy.148.decay), custom_call_target="tpu_custom_call" | custom-call | tf_op jit(solution)/shard_map/front/pallas_call | solution.py:339
  102.9 17.1 %all-to-all-start.3 = ((bf16[8,352,128]{2,1,0:T(8,128)(2,1)}), bf16[8,352,128]{2,1,0:T(8,128)(2,1)S(1)}, u32[]{:S(2)}, u32[]{:S(2)}) async-start(bf16[8,352,128]{2,1,0:T(8,128)(2,1)} %broadcast_in_dim.120), calls=%async_computation.3 | async-start | bytes 1441792 | tf_op jit(solution)/shard_map/all_to_all | solution.py:27
  123.3 17.8 %all-to-all-done.3.kv_own = bf16[8,352,128]{2,1,0:T(8,128)(2,1)S(1)} async-done(((bf16[8,352,128]{2,1,0:T(8,128)(2,1)}), bf16[8,352,128]{2,1,0:T(8,128)(2,1)S(1)}, u32[]{:S(2)}, u32[]{:S(2)}) %all-to-all-start.3) | async-done | bytes 720928 | tf_op jit(solution)/shard_map/all_to_all | solution.py:27
  141.1 1.9 collective-permute-start.4
  143.8 5.0 %all-to-all-start.1 = ((f32[8,8,3]{1,2,0:T(4,128)}), f32[8,8,3]{1,2,0:T(4,128)S(1)}, u32[]{:S(2)}, u32[]{:S(2)}) async-start(f32[8,8,3]{1,2,0:T(4,128)} %broadcast_in_dim.113), calls=%async_computation.1 | async-start | bytes 32768 | tf_op jit(solution)/shard_map/all_to_all | solution.py:27
  150.0 6.7 %all-to-all-done.1 = f32[8,8,3]{1,2,0:T(4,128)S(1)} async-done(((f32[8,8,3]{1,2,0:T(4,128)}), f32[8,8,3]{1,2,0:T(4,128)S(1)}, u32[]{:S(2)}, u32[]{:S(2)}) %all-to-all-start.1) | async-done | bytes 800 | tf_op jit(solution)/shard_map/all_to_all | solution.py:27
  156.7 1.9 collective-permute-start
  161.3 2.5 %all-gather.6.cloned.1.call-done = bf16[2048,256]{1,0:T(8,128)(2,1)} async-done(((bf16[256,256]{1,0:T(8,128)(2,1)}), bf16[2048,256]{1,0:T(8,128)(2,1)}) %all-gather.6.cloned.1.call-update) | async-done | bytes 1048592 | tf_op jit(solution)/shard_map/all_gather | solution.py:352
  164.7 16.1 %attend.1 = bf16[8,256,256]{2,1,0:T(8,128)(2,1)} custom-call(s32[67]{0:T(128)} %pad_add_fusion.1.plan, f32[384]{0:T(512)} %select_n.132.fade, bf16[8,256,256]{2,1,0:T(8,128)(2,1)} %bitcast.71, bf16[8,3,64,256]{3,2,1,0:T(8,128)(2,1)} %maximum_maximum_fusion.query_gate, bf16[8,352,128]{2,1,0:T(8,128)(2,1)} %copy-done.1, bf16[8,352,128]{2,1,0:T(8,128)(2,1)} %copy-done.3, ...), custom_call_target="tpu_custom_call" | custom-call | tf_op jit(solution)/shard_map/attend/pallas_call | solution.py:370
  180.8 4.0 %all-to-all-start.4 = ((bf16[8,256,256]{2,1,0:T(8,128)(2,1)}), bf16[8,256,256]{2,1,0:T(8,128)(2,1)S(1)}, u32[]{:S(2)}, u32[]{:S(2)}) async-start(bf16[8,256,256]{2,1,0:T(8,128)(2,1)} %attend.1), calls=%async_computation.4 | async-start | bytes 2097152 | tf_op jit(solution)/shard_map/all_to_all | solution.py:386
  186.0 2.1 collective-permute-start.5
  191.6 4.0 %local.1 = (f32[256,192]{1,0:T(8,128)}, bf16[256,192]{1,0:T(8,128)(2,1)}) custom-call(f32[256,896]{1,0:T(8,128)} %get-tuple-element.16.proj, f32[256,32]{1,0:T(8,128)} %get-tuple-element.31.cosine, f32[256,32]{1,0:T(8,128)} %get-tuple-element.30.sine, f32[256,3]{1,0:T(8,128)} %copy.148.decay, f32[8,256]{1,0:T(8,128)} %pad.9.decay_row), custom_call_target="tpu_custom_call" | custom-call | tf_op jit(solution)/shard_map/local/pallas_call | solution.py:355
  195.6 15.6 %all-to-all-done.4.parts = bf16[8,256,256]{2,1,0:T(8,128)(2,1)S(1)} async-done(((bf16[8,256,256]{2,1,0:T(8,128)(2,1)}), bf16[8,256,256]{2,1,0:T(8,128)(2,1)S(1)}, u32[]{:S(2)}, u32[]{:S(2)}) %all-to-all-start.4) | async-done | bytes 1048608 | tf_op jit(solution)/shard_map/all_to_all | solution.py:386
  212.1 5.0 %back.1 = bf16[256,2048]{1,0:T(8,128)(2,1)} custom-call(bf16[8,256,256]{2,1,0:T(8,128)(2,1)} %copy-done, f32[256,192]{1,0:T(8,128)} %get-tuple-element.17.local, bf16[256,192]{1,0:T(8,128)(2,1)} %get-tuple-element.18.lifted, bf16[2048,384]{1,0:T(8,128)(2,1)} %bitcast.64), custom_call_target="tpu_custom_call" | custom-call | tf_op jit(solution)/shard_map/back/pallas_call | solution.py:388
  217.2 16.1 %all_to_all.30 = bf16[4,64,2048]{2,1,0:T(8,128)(2,1)S(1)} all-to-all(bf16[4,64,2048]{2,1,0:T(8,128)(2,1)} %bitcast.65), channel_id=1, replica_groups=mesh['z'=8,'y'=8,'c'=2,'tp'=4] {'tp'}, dimensions={0} | all-to-all | bytes 2097152 | tf_op jit(solution)/shard_map/all_to_all | solution.py:397
  (112 shorter events, 31.8 us)
Async XLA Ops:
  6.5 12.6 %copy-start.5 = (f32[2048]{0:T(1024)S(1)}, f32[2048]{0:T(1024)}, u32[]{:S(2)}) copy-start(f32[2048]{0:T(1024)} %param.13) | copy-start | bytes 24580
  10.5 21.1 %all-to-all-start = ((bf16[8,16,1408]{2,1,0:T(8,128)(2,1)}), bf16[8,16,1408]{2,1,0:T(8,128)(2,1)S(1)}, u32[]{:S(2)}, u32[]{:S(2)}) async-start(bf16[8,16,1408]{2,1,0:T(8,128)(2,1)} %broadcast_in_dim.112), calls=%async_computation | async-start | bytes 720896 | tf_op jit(solution)/shard_map/all_to_all | solution.py:27
  32.7 5.7 %copy-start.4 = (f32[3,32768]{1,0:T(4,128)S(1)}, f32[3,32768]{1,0:T(4,128)}, u32[]{:S(2)}) copy-start(f32[3,32768]{1,0:T(4,128)} %param.23) | copy-start | bytes 1179652
  32.7 17.8 %all-to-all-start.2 = ((bf16[4,2,64,1024]{3,2,1,0:T(8,128)(2,1)}), bf16[4,2,64,1024]{3,2,1,0:T(8,128)(2,1)S(1)}, u32[]{:S(2)}, u32[]{:S(2)}) async-start(bf16[4,2,64,1024]{3,2,1,0:T(8,128)(2,1)} %broadcast_in_dim.117), calls=%async_computation.2 | async-start | bytes 2097152 | tf_op jit(solution)/shard_map/all_to_all | solution.py:27
  37.7 47.7 %all-gather.4.cloned.1.call-start = ((), (), s32[]{:S(2)}) async-start(), calls=%async_computation.6 | async-start | bytes 2949120 | tf_op jit(solution)/shard_map/all_gather | solution.py:257
  50.6 3.8 %collective-permute-start.1 = (bf16[256,1024]{1,0:T(8,128)(2,1)S(1)}, bf16[256,1024]{1,0:T(8,128)(2,1)S(1)}, u32[]{:S(2)}, u32[]{:S(2)}) collective-permute-start(bf16[256,1024]{1,0:T(8,128)(2,1)S(1)} %bitcast.73), channel_id=1, source_target_pairs={{0,4},{4,0},{1,5},{5,1},{2,6},{6,2},{3,7},{7,3},{8,12},{12,8},{9,1... | collective-permute-start | bytes 1572872 | tf_op jit(solution)/shard_map/ppermute | solution.py:31
  89.6 5.3 %collective-permute-start.2 = (f32[256,896]{1,0:T(8,128)}, f32[256,896]{1,0:T(8,128)S(1)}, u32[]{:S(2)}, u32[]{:S(2)}) collective-permute-start(f32[256,896]{1,0:T(8,128)} %get-tuple-element.13), channel_id=1, source_target_pairs={{0,4},{4,0},{1,5},{5,1},{2,6},{6,2},{3,7},{7,3},{8,12},{12,8},{9,1... | collective-permute-start | bytes 2752520 | tf_op jit(solution)/shard_map/ppermute | solution.py:31
  94.9 1.0 copy-start.2
  100.3 1.6 collective-permute-start.3
  102.9 38.2 %all-to-all-start.3 = ((bf16[8,352,128]{2,1,0:T(8,128)(2,1)}), bf16[8,352,128]{2,1,0:T(8,128)(2,1)S(1)}, u32[]{:S(2)}, u32[]{:S(2)}) async-start(bf16[8,352,128]{2,1,0:T(8,128)(2,1)} %broadcast_in_dim.120), calls=%async_computation.3 | async-start | bytes 1441792 | tf_op jit(solution)/shard_map/all_to_all | solution.py:27
  120.0 43.8 %all-gather.6.cloned.1.call-start = ((), (), s32[]{:S(2)}) async-start(), calls=%async_computation.7 | async-start | bytes 1179648 | tf_op jit(solution)/shard_map/all_gather | solution.py:352
  141.1 22.7 %copy-start.1 = (bf16[8,352,128]{2,1,0:T(8,128)(2,1)}, bf16[8,352,128]{2,1,0:T(8,128)(2,1)S(1)}, u32[]{:S(2)}) copy-start(bf16[8,352,128]{2,1,0:T(8,128)(2,1)S(1)} %all-to-all-done.3.kv_own) | copy-start | bytes 2162692
  141.1 22.7 %collective-permute-start.4 = (bf16[8,352,128]{2,1,0:T(8,128)(2,1)S(1)}, bf16[8,352,128]{2,1,0:T(8,128)(2,1)S(1)}, u32[]{:S(2)}, u32[]{:S(2)}) collective-permute-start(bf16[8,352,128]{2,1,0:T(8,128)(2,1)S(1)} %all-to-all-done.3.kv_own), channel_id=1, source_target_pairs={{0,4},{4,0},{1,5},{5,1},{2,6},{6,2},{3,7},{7,3},{8,12},{12,8},{9,1... | collective-permute-start | bytes 2162696 | tf_op jit(solution)/shard_map/ppermute | solution.py:31
  143.8 12.9 %all-to-all-start.1 = ((f32[8,8,3]{1,2,0:T(4,128)}), f32[8,8,3]{1,2,0:T(4,128)S(1)}, u32[]{:S(2)}, u32[]{:S(2)}) async-start(f32[8,8,3]{1,2,0:T(4,128)} %broadcast_in_dim.113), calls=%async_computation.1 | async-start | bytes 32768 | tf_op jit(solution)/shard_map/all_to_all | solution.py:27
  156.7 3.1 %collective-permute-start = (f32[8,8,3]{1,2,0:T(4,128)S(1)}, f32[8,8,3]{1,2,0:T(4,128)S(1)}, u32[]{:S(2)}, u32[]{:S(2)}) collective-permute-start(f32[8,8,3]{1,2,0:T(4,128)S(1)} %all-to-all-done.1), channel_id=1, source_target_pairs={{0,4},{4,0},{1,5},{5,1},{2,6},{6,2},{3,7},{7,3},{8,12},{12,8},{9,1... | collective-permute-start | bytes 2312 | tf_op jit(solution)/shard_map/ppermute | solution.py:31
  163.8 0.9 copy-start.3
  180.8 30.4 %all-to-all-start.4 = ((bf16[8,256,256]{2,1,0:T(8,128)(2,1)}), bf16[8,256,256]{2,1,0:T(8,128)(2,1)S(1)}, u32[]{:S(2)}, u32[]{:S(2)}) async-start(bf16[8,256,256]{2,1,0:T(8,128)(2,1)} %attend.1), calls=%async_computation.4 | async-start | bytes 2097152 | tf_op jit(solution)/shard_map/all_to_all | solution.py:386
  186.0 4.2 %collective-permute-start.5 = (bf16[1024,384]{1,0:T(8,128)(2,1)S(1)}, bf16[1024,384]{1,0:T(8,128)(2,1)S(1)}, u32[]{:S(2)}, u32[]{:S(2)}) collective-permute-start(bf16[1024,384]{1,0:T(8,128)(2,1)S(1)} %slice.40), channel_id=1, source_target_pairs={{0,4},{4,0},{1,5},{5,1},{2,6},{6,2},{3,7},{7,3},{8,12},{12,8},{9,1... | collective-permute-start | bytes 2359304 | tf_op jit(solution)/shard_map/ppermute | solution.py:31
  211.2 1.0 copy-start
Sparse Core Ops, SparseCore 0:
  40.6 44.7 all-gather.3
  122.9 40.8 all-gather.5

commit v5 on v4

--- a/solution.py
+++ b/solution.py
@@ -95,22 +95,7 @@
         ).astype(BF16)
 
 
-def attend_kernel(
-    plan,
-    fade,
-    received,
-    query_gate,
-    kv_own,
-    kv_oth,
-    key_gate,
-    out,
-    keys,
-    values,
-    queries,
-    total,
-    even,
-    odd,
-):
+def prepare_kernel(fade, kv_own, kv_oth, key_gate, keys, values, states):
     extra = lax.broadcasted_iota(jnp.int32, (16, 2 * SPAN), 0)
     ones = jnp.where(extra == 0, 1.0, 0.0).astype(BF16)
     for y in range(8):
@@ -124,6 +109,25 @@
             values[y, :HEAD, at + 128 : at + SPAN] = held[y, 192:SPAN]
         values[y, HEAD:, :] = ones
     for z in range(8):
+        sums = []
+        for h in range(3):
+            at = SPAN + 32 * h
+            state = jnp.zeros((32, 128), F32)
+            for side, held in enumerate((kv_own, kv_oth)):
+                for y in range(8):
+                    state = state + held[y, at : at + 32].astype(F32) * fade[
+                        ((z * 2 + side) * 8 + y) * 3 + h
+                    ]
+            sums.append(state)
+        sums = jnp.concatenate(sums, axis=0).astype(BF16)
+        states[z, :, :128] = sums[:48]
+        states[z, :, 128:] = sums[48:]
+
+
+def attend_kernel(
+    plan, received, query_gate, keys, values, states, out, queries, total, even, odd
+):
+    for z in range(8):
         for h in range(3):
             queries[z, h, :HEAD] = received[z, h * HEAD : (h + 1) * HEAD]
             queries[z, h, HEAD:] = query_gate[z, h]
@@ -182,20 +186,7 @@
         out[z, 192:208] = jnp.concatenate(
             high + low + [jnp.zeros((10, SPAN), F32)], axis=0
         ).astype(BF16)
-    for z in range(8):
-        sums = []
-        for h in range(3):
-            at = SPAN + 32 * h
-            state = jnp.zeros((32, 128), F32)
-            for side, held in enumerate((kv_own, kv_oth)):
-                for y in range(8):
-                    state = state + held[y, at : at + 32].astype(F32) * fade[
-                        ((z * 2 + side) * 8 + y) * 3 + h
-                    ]
-            sums.append(state)
-        sums = jnp.concatenate(sums, axis=0).astype(BF16)
-        out[z, 208:, :128] = sums[:48]
-        out[z, 208:, 128:] = sums[48:]
+        out[z, 208:] = states[z]
 
 
 def back_kernel(parts, local, lifted, w_out, out, mixed):
@@ -235,8 +226,7 @@
     forget_total,
 ):
     z, y, c = (lax.axis_index("z"), lax.axis_index("y"), lax.axis_index("c"))
-    decay = jnp.cumsum(retain_log, axis=0)
-    ends = jnp.concatenate(three_parts(decay[-1]))
+    ends = jnp.concatenate(three_parts(jnp.sum(retain_log, axis=0)))
     shard = jnp.concatenate(
         [
             w_query_ret,
@@ -272,6 +262,7 @@
     inverse = THETA ** (-jnp.arange(32, dtype=F32) / 32)
     angles = positions[:, None] * inverse[None, :]
     cosine, sine = (jnp.cos(angles), jnp.sin(angles))
+    decay = jnp.cumsum(retain_log, axis=0)
     decay_row = jnp.pad(decay.T, ((0, 5), (0, 0)))
     ends_own = copies_from(line_ends, "z")
     ends_oth = swapped_cores(ends_own)
@@ -350,7 +341,8 @@
     )(own_part, swapped_cores(oth_part), cosine, sine, decay)
 
     queries = lax.all_gather(q_send, "z", axis=0)
-    kv_own = copies_from(lax.ppermute(kv_send, ("z", "y"), ROTATION), "y")
+    kv_send = lax.ppermute(kv_send, ("z", "y"), ROTATION)
+    kv_own = copies_from(kv_send, "y")
     kv_oth = swapped_cores(kv_own)
     local, lifted = pl.pallas_call(
         local_kernel,
@@ -367,14 +359,24 @@
         c == 0, jnp.stack([out_own, out_oth], axis=1), jnp.stack([out_oth, out_own], axis=1)
     ).reshape(2048, 384)
 
+    keys, values, states = pl.pallas_call(
+        prepare_kernel,
+        in_specs=[SMEM] + [VMEM] * 3,
+        out_specs=[VMEM] * 3,
+        out_shape=[
+            jax.ShapeDtypeStruct((8, 2 * SPAN, 128), BF16),
+            jax.ShapeDtypeStruct((8, 80, 2 * SPAN), BF16),
+            jax.ShapeDtypeStruct((8, 48, SPAN), BF16),
+        ],
+        compiler_params=PARAMS,
+        name="prepare",
+    )(fade, kv_own, kv_oth, key_gate)
     partial = pl.pallas_call(
         attend_kernel,
-        in_specs=[SMEM] * 2 + [VMEM] * 5,
+        in_specs=[SMEM] + [VMEM] * 5,
         out_specs=VMEM,
         out_shape=jax.ShapeDtypeStruct((8, SPAN, SPAN), BF16),
         scratch_shapes=[
-            pltpu.VMEM((8, 2 * SPAN, 128), BF16),
-            pltpu.VMEM((8, 80, 2 * SPAN), BF16),
             pltpu.VMEM((8, 3, 128, SPAN), BF16),
             pltpu.VMEM((8, 80, 3 * SPAN), F32),
             pltpu.VMEM((2 * SPAN, 3 * SPAN), BF16),
@@ -382,7 +384,7 @@
         ],
         compiler_params=PARAMS,
         name="attend",
-    )(plan, fade, queries, query_gate, kv_own, kv_oth, key_gate)
+    )(plan, queries, query_gate, keys, values, states)
     parts = lax.all_to_all(partial, "z", 0, 0, tiled=True)
 
     share = pl.pallas_call(

time: 242 us -> 246 us (1.017)
  the two profiles are of different devices: /device:TPU:2 before, /device:TPU:1 now
where the time goes in v5:
time: 246 us; the launch traced here: 245 us
  waiting for transfers between devices  89.3 us (36%)
  starting transfers between devices  59.5 us (24%)
  Pallas kernels  35.9 us (15%)
  blocking collectives  18.1 us (7%)
  local copies, waits for them, and re-layouts  15.2 us (6%)
  between operations  14.4 us (6%)
  other arithmetic  12.4 us (5%)
    all_to_all x4, waiting for transfers between devices, copies_from(): return lax.all_to_all(copies, axis, split_axis=0, concat_axis=0, tiled=True)  42 us
    all_to_all x4, starting transfers between devices, copies_from(): return lax.all_to_all(copies, axis, split_axis=0, concat_axis=0, tiled=True)  34.9 us
    all_gather x1, waiting for transfers between devices, body(): w_own = lax.all_gather(w_row, 'z', axis=0, tiled=True)  25.6 us
    ppermute x5, starting transfers between devices, swapped_cores(): return lax.ppermute(value, 'c', [(0, 1), (1, 0)])  19.5 us
    all_to_all x1, waiting for transfers between devices, body(): parts = lax.all_to_all(partial, 'z', 0, 0, tiled=True)  18.4 us
    all_to_all x1, blocking collectives, body(): shares = lax.all_to_all(share.reshape(4, 64, 2048), 'tp', 0, 0, tiled=True)  18.1 us
    pallas_call x1, Pallas kernels, body(): pl.pallas_call(attend_kernel, in_specs=[SMEM] + [VMEM] * 5, out_specs=VME...  14.3 us
    pallas_call x1, Pallas kernels, body(): pl.pallas_call(back_kernel, in_specs=[VMEM] * 4, out_specs=VMEM, out_shap...  5.03 us
  transfers between devices with their start and end apart: 13, of which 9 were waited for; matrix products, arithmetic and copies ran while one was open for 8% of the time, Pallas kernels for 3%

profile of v5, /device:TPU:1, one launch (start us, length us, event | category | flops | bytes accessed | tf_op | source)
XLA Modules:
  0.0 244.8 jit_solution(1650778594745937788)
XLA Ops:
  9.1 7.6 %all-to-all-start.1 = ((bf16[8,16,1408]{2,1,0:T(8,128)(2,1)}), bf16[8,16,1408]{2,1,0:T(8,128)(2,1)S(1)}, u32[]{:S(2)}, u32[]{:S(2)}) async-start(bf16[8,16,1408]{2,1,0:T(8,128)(2,1)} %broadcast_in_dim.111), calls=%async_computation.1 | async-start | bytes 720896 | tf_op jit(solution)/shard_map/all_to_all | solution.py:27
  18.9 8.5 %all-to-all-done.1 = bf16[8,16,1408]{2,1,0:T(8,128)(2,1)S(1)} async-done(((bf16[8,16,1408]{2,1,0:T(8,128)(2,1)}), bf16[8,16,1408]{2,1,0:T(8,128)(2,1)S(1)}, u32[]{:S(2)}, u32[]{:S(2)}) %all-to-all-start.1) | async-done | bytes 360480 | tf_op jit(solution)/shard_map/all_to_all | solution.py:27
  28.5 6.9 %all-to-all-start = ((bf16[4,2,64,1024]{3,2,1,0:T(8,128)(2,1)}), bf16[4,2,64,1024]{3,2,1,0:T(8,128)(2,1)S(1)}, u32[]{:S(2)}, u32[]{:S(2)}) async-start(bf16[4,2,64,1024]{3,2,1,0:T(8,128)(2,1)} %broadcast_in_dim.109), calls=%async_computation | async-start | bytes 2097152 | tf_op jit(solution)/shard_map/all_to_all | solution.py:27
  38.7 10.2 %all-to-all-done = bf16[4,2,64,1024]{3,2,1,0:T(8,128)(2,1)S(1)} async-done(((bf16[4,2,64,1024]{3,2,1,0:T(8,128)(2,1)}), bf16[4,2,64,1024]{3,2,1,0:T(8,128)(2,1)S(1)}, u32[]{:S(2)}, u32[]{:S(2)}) %all-to-all-start) | async-done | bytes 1048608 | tf_op jit(solution)/shard_map/all_to_all | solution.py:27
  49.0 4.6 %collective-permute-start = (bf16[256,1024]{1,0:T(8,128)(2,1)S(1)}, bf16[256,1024]{1,0:T(8,128)(2,1)S(1)}, u32[]{:S(2)}, u32[]{:S(2)}) collective-permute-start(bf16[256,1024]{1,0:T(8,128)(2,1)S(1)} %bitcast.73), channel_id=1, source_target_pairs={{0,4},{4,0},{1,5},{5,1},{2,6},{6,2},{3,7},{7,3},{8,12},{12,8},{9,1... | collective-permute-start | bytes 1572872 | tf_op jit(solution)/shard_map/ppermute | solution.py:31
  56.1 25.6 %all-gather.4.cloned.1.call-done.weights = bf16[1024,1280]{1,0:T(8,128)(2,1)} async-done(((bf16[128,1280]{1,0:T(8,128)(2,1)}), bf16[1024,1280]{1,0:T(8,128)(2,1)}) %all-gather.4.cloned.1.call-update) | async-done | bytes 2621456 | tf_op jit(solution)/shard_map/all_gather | solution.py:247
  81.7 4.3 %project.1 = (f32[256,896]{1,0:T(8,128)}, f32[256,896]{1,0:T(8,128)}) custom-call(bf16[512,1024]{1,0:T(8,128)(2,1)} %pad_maximum_fusion.rows, bf16[1024,1280]{1,0:T(8,128)(2,1)} %all-gather.4.cloned.1.call-done.weights), custom_call_target="tpu_custom_call" | custom-call | tf_op jit(solution)/shard_map/project/pallas_call | solution.py:321
  86.0 5.7 %collective-permute-start.1 = (f32[256,896]{1,0:T(8,128)}, f32[256,896]{1,0:T(8,128)S(1)}, u32[]{:S(2)}, u32[]{:S(2)}) collective-permute-start(f32[256,896]{1,0:T(8,128)} %get-tuple-element.16), channel_id=1, source_target_pairs={{0,4},{4,0},{1,5},{5,1},{2,6},{6,2},{3,7},{7,3},{8,12},{12,8},{9,1... | collective-permute-start | bytes 2752520 | tf_op jit(solution)/shard_map/ppermute | solution.py:31
  96.0 4.4 %front.1 = (bf16[256,256]{1,0:T(8,128)(2,1)}, bf16[352,128]{1,0:T(8,128)(2,1)}, f32[256,896]{1,0:T(8,128)}) custom-call(f32[256,896]{1,0:T(8,128)} %get-tuple-element.15.first_part, f32[256,896]{1,0:T(8,128)} %copy-done.2, f32[256,32]{1,0:T(8,128)} %get-tuple-element.37.cosine, f32[256,32]{1,0:T(8,128)} %get-tuple-element.36.sine, f32[256,3]{1,0:T(8,128)} %copy.140.decay), custom_call_target="tpu_custom_call" | custom-call | tf_op jit(solution)/shard_map/front/pallas_call | solution.py:330
  100.4 1.5 collective-permute-start.3
  103.0 15.5 %all-to-all-start.3 = ((bf16[8,352,128]{2,1,0:T(8,128)(2,1)}), bf16[8,352,128]{2,1,0:T(8,128)(2,1)S(1)}, u32[]{:S(2)}, u32[]{:S(2)}) async-start(bf16[8,352,128]{2,1,0:T(8,128)(2,1)} %broadcast_in_dim.120), calls=%async_computation.3 | async-start | bytes 1441792 | tf_op jit(solution)/shard_map/all_to_all | solution.py:27
  121.8 17.8 %all-to-all-done.3.kv_own = bf16[8,352,128]{2,1,0:T(8,128)(2,1)S(1)} async-done(((bf16[8,352,128]{2,1,0:T(8,128)(2,1)}), bf16[8,352,128]{2,1,0:T(8,128)(2,1)S(1)}, u32[]{:S(2)}, u32[]{:S(2)}) %all-to-all-start.3) | async-done | bytes 720928 | tf_op jit(solution)/shard_map/all_to_all | solution.py:27
  139.6 3.5 %collective-permute-start.4 = (bf16[8,352,128]{2,1,0:T(8,128)(2,1)S(1)}, bf16[8,352,128]{2,1,0:T(8,128)(2,1)S(1)}, u32[]{:S(2)}, u32[]{:S(2)}) collective-permute-start(bf16[8,352,128]{2,1,0:T(8,128)(2,1)S(1)} %all-to-all-done.3.kv_own), channel_id=1, source_target_pairs={{0,4},{4,0},{1,5},{5,1},{2,6},{6,2},{3,7},{7,3},{8,12},{12,8},{9,1... | collective-permute-start | bytes 2162696 | tf_op jit(solution)/shard_map/ppermute | solution.py:31
  143.8 4.9 %all-to-all-start.2 = ((f32[8,8,3]{1,2,0:T(4,128)}), f32[8,8,3]{1,2,0:T(4,128)S(1)}, u32[]{:S(2)}, u32[]{:S(2)}) async-start(f32[8,8,3]{1,2,0:T(4,128)} %broadcast_in_dim.116), calls=%async_computation.2 | async-start | bytes 32768 | tf_op jit(solution)/shard_map/all_to_all | solution.py:27
  149.9 5.5 %all-to-all-done.2 = f32[8,8,3]{1,2,0:T(4,128)S(1)} async-done(((f32[8,8,3]{1,2,0:T(4,128)}), f32[8,8,3]{1,2,0:T(4,128)S(1)}, u32[]{:S(2)}, u32[]{:S(2)}) %all-to-all-start.2) | async-done | bytes 800 | tf_op jit(solution)/shard_map/all_to_all | solution.py:27
  155.3 3.3 %collective-permute-start.2 = (f32[8,8,3]{1,2,0:T(4,128)S(1)}, f32[8,8,3]{1,2,0:T(4,128)S(1)}, u32[]{:S(2)}, u32[]{:S(2)}) collective-permute-start(f32[8,8,3]{1,2,0:T(4,128)S(1)} %all-to-all-done.2), channel_id=1, source_target_pairs={{0,4},{4,0},{1,5},{5,1},{2,6},{6,2},{3,7},{7,3},{8,12},{12,8},{9,1... | collective-permute-start | bytes 2312 | tf_op jit(solution)/shard_map/ppermute | solution.py:31
  162.0 3.9 %prepare.1 = (bf16[8,512,128]{2,1,0:T(8,128)(2,1)}, bf16[8,80,512]{2,1,0:T(8,128)(2,1)}, bf16[8,48,256]{2,1,0:T(8,128)(2,1)}) custom-call(f32[384]{0:T(512)} %select_n.142.fade, bf16[8,352,128]{2,1,0:T(8,128)(2,1)} %copy-done.1, bf16[8,352,128]{2,1,0:T(8,128)(2,1)} %copy-done.3, bf16[2,8,256,64]{3,2,1,0:T(8,128)(2,1)} %maximum_bitcast_fusion.key_gate), custom_call_target="tpu_custom_call" | custom-call | tf_op jit(solution)/shard_map/prepare/pallas_call | solution.py:362
  165.8 14.3 %attend.1 = bf16[8,256,256]{2,1,0:T(8,128)(2,1)} custom-call(s32[67]{0:T(128)} %pad_add_fusion.1.plan, bf16[8,256,256]{2,1,0:T(8,128)(2,1)} %bitcast.71, bf16[8,3,64,256]{3,2,1,0:T(8,128)(2,1)} %maximum_maximum_fusion.query_gate, bf16[8,512,128]{2,1,0:T(8,128)(2,1)} %get-tuple-element.19.keys, bf16[8,80,512]{2,1,0:T(8,128)(2,1)} %get-tuple-element.20.values, ...), custom_call_target="tpu_custom_call" | custom-call | tf_op jit(solution)/shard_map/attend/pallas_call | solution.py:374
  180.2 3.6 %all-to-all-start.4 = ((bf16[8,256,256]{2,1,0:T(8,128)(2,1)}), bf16[8,256,256]{2,1,0:T(8,128)(2,1)S(1)}, u32[]{:S(2)}, u32[]{:S(2)}) async-start(bf16[8,256,256]{2,1,0:T(8,128)(2,1)} %attend.1), calls=%async_computation.4 | async-start | bytes 2097152 | tf_op jit(solution)/shard_map/all_to_all | solution.py:388
  185.0 2.4 collective-permute-start.5
  190.5 4.0 %local.1 = (f32[256,192]{1,0:T(8,128)}, bf16[256,192]{1,0:T(8,128)(2,1)}) custom-call(f32[256,896]{1,0:T(8,128)} %get-tuple-element.22.proj, f32[256,32]{1,0:T(8,128)} %get-tuple-element.37.cosine, f32[256,32]{1,0:T(8,128)} %get-tuple-element.36.sine, f32[256,3]{1,0:T(8,128)} %copy.140.decay, f32[8,256]{1,0:T(8,128)} %pad.9.decay_row), custom_call_target="tpu_custom_call" | custom-call | tf_op jit(solution)/shard_map/local/pallas_call | solution.py:347
  194.5 18.4 %all-to-all-done.4.parts = bf16[8,256,256]{2,1,0:T(8,128)(2,1)S(1)} async-done(((bf16[8,256,256]{2,1,0:T(8,128)(2,1)}), bf16[8,256,256]{2,1,0:T(8,128)(2,1)S(1)}, u32[]{:S(2)}, u32[]{:S(2)}) %all-to-all-start.4) | async-done | bytes 1048608 | tf_op jit(solution)/shard_map/all_to_all | solution.py:388
  213.9 5.0 %back.1 = bf16[256,2048]{1,0:T(8,128)(2,1)} custom-call(bf16[8,256,256]{2,1,0:T(8,128)(2,1)} %copy-done, f32[256,192]{1,0:T(8,128)} %get-tuple-element.23.local, bf16[256,192]{1,0:T(8,128)(2,1)} %get-tuple-element.24.lifted, bf16[2048,384]{1,0:T(8,128)(2,1)} %bitcast.64), custom_call_target="tpu_custom_call" | custom-call | tf_op jit(solution)/shard_map/back/pallas_call | solution.py:390
  218.9 18.1 %all_to_all.30 = bf16[4,64,2048]{2,1,0:T(8,128)(2,1)S(1)} all-to-all(bf16[4,64,2048]{2,1,0:T(8,128)(2,1)} %bitcast.65), channel_id=1, replica_groups=mesh['z'=8,'y'=8,'c'=2,'tp'=4] {'tp'}, dimensions={0} | all-to-all | bytes 2097152 | tf_op jit(solution)/shard_map/all_to_all | solution.py:399
  (115 shorter events, 30.9 us)
Async XLA Ops:
  6.5 11.8 %copy-start.6 = (f32[2048]{0:T(1024)S(1)}, f32[2048]{0:T(1024)}, u32[]{:S(2)}) copy-start(f32[2048]{0:T(1024)} %param.13) | copy-start | bytes 24580
  9.1 18.3 %all-to-all-start.1 = ((bf16[8,16,1408]{2,1,0:T(8,128)(2,1)}), bf16[8,16,1408]{2,1,0:T(8,128)(2,1)S(1)}, u32[]{:S(2)}, u32[]{:S(2)}) async-start(bf16[8,16,1408]{2,1,0:T(8,128)(2,1)} %broadcast_in_dim.111), calls=%async_computation.1 | async-start | bytes 720896 | tf_op jit(solution)/shard_map/all_to_all | solution.py:27
  28.5 7.7 %copy-start.4 = (f32[3,32768]{1,0:T(4,128)S(1)}, f32[3,32768]{1,0:T(4,128)}, u32[]{:S(2)}) copy-start(f32[3,32768]{1,0:T(4,128)} %param.23) | copy-start | bytes 1179652
  28.5 7.9 %copy-start.5 = (f32[256,3]{0,1:T(4,128)S(1)}, f32[256,3]{0,1:T(4,128)}, u32[]{:S(2)}) copy-start(f32[256,3]{0,1:T(4,128)} %param.22) | copy-start | bytes 9220
  28.5 20.3 %all-to-all-start = ((bf16[4,2,64,1024]{3,2,1,0:T(8,128)(2,1)}), bf16[4,2,64,1024]{3,2,1,0:T(8,128)(2,1)S(1)}, u32[]{:S(2)}, u32[]{:S(2)}) async-start(bf16[4,2,64,1024]{3,2,1,0:T(8,128)(2,1)} %broadcast_in_dim.109), calls=%async_computation | async-start | bytes 2097152 | tf_op jit(solution)/shard_map/all_to_all | solution.py:27
  35.5 46.2 %all-gather.4.cloned.1.call-start = ((), (), s32[]{:S(2)}) async-start(), calls=%async_computation.6 | async-start | bytes 2949120 | tf_op jit(solution)/shard_map/all_gather | solution.py:247
  49.0 6.1 %collective-permute-start = (bf16[256,1024]{1,0:T(8,128)(2,1)S(1)}, bf16[256,1024]{1,0:T(8,128)(2,1)S(1)}, u32[]{:S(2)}, u32[]{:S(2)}) collective-permute-start(bf16[256,1024]{1,0:T(8,128)(2,1)S(1)} %bitcast.73), channel_id=1, source_target_pairs={{0,4},{4,0},{1,5},{5,1},{2,6},{6,2},{3,7},{7,3},{8,12},{12,8},{9,1... | collective-permute-start | bytes 1572872 | tf_op jit(solution)/shard_map/ppermute | solution.py:31
  86.0 9.1 %collective-permute-start.1 = (f32[256,896]{1,0:T(8,128)}, f32[256,896]{1,0:T(8,128)S(1)}, u32[]{:S(2)}, u32[]{:S(2)}) collective-permute-start(f32[256,896]{1,0:T(8,128)} %get-tuple-element.16), channel_id=1, source_target_pairs={{0,4},{4,0},{1,5},{5,1},{2,6},{6,2},{3,7},{7,3},{8,12},{12,8},{9,1... | collective-permute-start | bytes 2752520 | tf_op jit(solution)/shard_map/ppermute | solution.py:31
  95.1 0.9 copy-start.2
  100.4 1.7 collective-permute-start.3
  103.0 36.5 %all-to-all-start.3 = ((bf16[8,352,128]{2,1,0:T(8,128)(2,1)}), bf16[8,352,128]{2,1,0:T(8,128)(2,1)S(1)}, u32[]{:S(2)}, u32[]{:S(2)}) async-start(bf16[8,352,128]{2,1,0:T(8,128)(2,1)} %broadcast_in_dim.120), calls=%async_computation.3 | async-start | bytes 1441792 | tf_op jit(solution)/shard_map/all_to_all | solution.py:27
  118.5 47.4 %all-gather.6.cloned.1.call-start = ((), (), s32[]{:S(2)}) async-start(), calls=%async_computation.7 | async-start | bytes 1179648 | tf_op jit(solution)/shard_map/all_gather | solution.py:343
  139.6 21.5 %copy-start.1 = (bf16[8,352,128]{2,1,0:T(8,128)(2,1)}, bf16[8,352,128]{2,1,0:T(8,128)(2,1)S(1)}, u32[]{:S(2)}) copy-start(bf16[8,352,128]{2,1,0:T(8,128)(2,1)S(1)} %all-to-all-done.3.kv_own) | copy-start | bytes 2162692
  139.6 21.5 %collective-permute-start.4 = (bf16[8,352,128]{2,1,0:T(8,128)(2,1)S(1)}, bf16[8,352,128]{2,1,0:T(8,128)(2,1)S(1)}, u32[]{:S(2)}, u32[]{:S(2)}) collective-permute-start(bf16[8,352,128]{2,1,0:T(8,128)(2,1)S(1)} %all-to-all-done.3.kv_own), channel_id=1, source_target_pairs={{0,4},{4,0},{1,5},{5,1},{2,6},{6,2},{3,7},{7,3},{8,12},{12,8},{9,1... | collective-permute-start | bytes 2162696 | tf_op jit(solution)/shard_map/ppermute | solution.py:31
  143.8 11.6 %all-to-all-start.2 = ((f32[8,8,3]{1,2,0:T(4,128)}), f32[8,8,3]{1,2,0:T(4,128)S(1)}, u32[]{:S(2)}, u32[]{:S(2)}) async-start(f32[8,8,3]{1,2,0:T(4,128)} %broadcast_in_dim.116), calls=%async_computation.2 | async-start | bytes 32768 | tf_op jit(solution)/shard_map/all_to_all | solution.py:27
  155.3 4.2 %collective-permute-start.2 = (f32[8,8,3]{1,2,0:T(4,128)S(1)}, f32[8,8,3]{1,2,0:T(4,128)S(1)}, u32[]{:S(2)}, u32[]{:S(2)}) collective-permute-start(f32[8,8,3]{1,2,0:T(4,128)S(1)} %all-to-all-done.2), channel_id=1, source_target_pairs={{0,4},{4,0},{1,5},{5,1},{2,6},{6,2},{3,7},{7,3},{8,12},{12,8},{9,1... | collective-permute-start | bytes 2312 | tf_op jit(solution)/shard_map/ppermute | solution.py:31
  161.0 0.9 copy-start.3
  180.2 32.8 %all-to-all-start.4 = ((bf16[8,256,256]{2,1,0:T(8,128)(2,1)}), bf16[8,256,256]{2,1,0:T(8,128)(2,1)S(1)}, u32[]{:S(2)}, u32[]{:S(2)}) async-start(bf16[8,256,256]{2,1,0:T(8,128)(2,1)} %attend.1), calls=%async_computation.4 | async-start | bytes 2097152 | tf_op jit(solution)/shard_map/all_to_all | solution.py:388
  185.0 4.2 %collective-permute-start.5 = (bf16[1024,384]{1,0:T(8,128)(2,1)S(1)}, bf16[1024,384]{1,0:T(8,128)(2,1)S(1)}, u32[]{:S(2)}, u32[]{:S(2)}) collective-permute-start(bf16[1024,384]{1,0:T(8,128)(2,1)S(1)} %slice.35), channel_id=1, source_target_pairs={{0,4},{4,0},{1,5},{5,1},{2,6},{6,2},{3,7},{7,3},{8,12},{12,8},{9,1... | collective-permute-start | bytes 2359304 | tf_op jit(solution)/shard_map/ppermute | solution.py:31
  212.9 1.0 copy-start
Sparse Core Ops, SparseCore 0:
  38.4 43.3 all-gather.3
  121.4 36.5 all-gather.5

commit v6 on v5

--- a/solution.py
+++ b/solution.py
@@ -1,3 +1,5 @@
+import functools
+
 import jax
 import jax.numpy as jnp
 from jax import lax
@@ -39,10 +41,22 @@
     return [part.astype(BF16) for part in (high, middle, low)]
 
 
-def project_kernel(rows, weights, own_out, oth_out):
-    product = jnp.dot(rows[...], weights[...], preferred_element_type=F32)
-    own_out[...] = product[:SPAN]
-    oth_out[...] = product[SPAN:]
+def project_kernel(rows, weights, own_out, oth_out, product):
+    step = pl.program_id(0)
+    part = jnp.dot(rows[...], weights[...], preferred_element_type=F32)
+
+    @pl.when(step == 0)
+    def _():
+        product[...] = part
+
+    @pl.when(step > 0)
+    def _():
+        product[...] += part
+
+    @pl.when(step == pl.num_programs(0) - 1)
+    def _():
+        own_out[...] = product[:SPAN]
+        oth_out[...] = product[SPAN:].astype(BF16)
 
 
 def turned(proj, at, cos, sin):
@@ -52,7 +66,7 @@
 
 
 def front_kernel(first_part, second_part, cosine, sine, decay, q_out, kv_out, proj_out):
-    proj_out[...] = first_part[...] + second_part[...]
+    proj_out[...] = first_part[...] + second_part[...].astype(F32)
     cos = cosine[...]
     sin = sine[...]
     for h in range(3):
@@ -95,37 +109,43 @@
         ).astype(BF16)
 
 
-def prepare_kernel(fade, kv_own, kv_oth, key_gate, keys, values, states):
-    extra = lax.broadcasted_iota(jnp.int32, (16, 2 * SPAN), 0)
+def prepare_kernel(side, fade, held, key_gate, keys, values, states):
+    extra = lax.broadcasted_iota(jnp.int32, (16, SPAN), 0)
     ones = jnp.where(extra == 0, 1.0, 0.0).astype(BF16)
     for y in range(8):
-        for side, held in enumerate((kv_own, kv_oth)):
-            packed = held[y, :128]
-            at = side * SPAN
-            keys[y, at : at + 128, :HEAD] = packed[:, :HEAD]
-            keys[y, at + 128 : at + SPAN, :HEAD] = packed[:, HEAD:]
-            keys[y, at : at + SPAN, HEAD:] = key_gate[side, y]
-            values[y, :HEAD, at : at + 128] = held[y, 128:192]
-            values[y, :HEAD, at + 128 : at + SPAN] = held[y, 192:SPAN]
+        packed = held[y, :128]
+        keys[y, :128, :HEAD] = packed[:, :HEAD]
+        keys[y, 128:, :HEAD] = packed[:, HEAD:]
+        keys[y, :, HEAD:] = key_gate[side, y]
+        values[y, :HEAD, :128] = held[y, 128:192]
+        values[y, :HEAD, 128:] = held[y, 192:SPAN]
         values[y, HEAD:, :] = ones
     for z in range(8):
-        sums = []
         for h in range(3):
             at = SPAN + 32 * h
             state = jnp.zeros((32, 128), F32)
-            for side, held in enumerate((kv_own, kv_oth)):
-                for y in range(8):
-                    state = state + held[y, at : at + 32].astype(F32) * fade[
-                        ((z * 2 + side) * 8 + y) * 3 + h
-                    ]
-            sums.append(state)
-        sums = jnp.concatenate(sums, axis=0).astype(BF16)
-        states[z, :, :128] = sums[:48]
-        states[z, :, 128:] = sums[48:]
+            for y in range(8):
+                state = state + held[y, at : at + 32].astype(F32) * fade[
+                    ((z * 2 + side) * 8 + y) * 3 + h
+                ]
+            states[z, 32 * h : 32 * (h + 1)] = state
 
 
 def attend_kernel(
-    plan, received, query_gate, keys, values, states, out, queries, total, even, odd
+    plan,
+    received,
+    query_gate,
+    keys_own,
+    keys_oth,
+    values_own,
+    values_oth,
+    states_own,
+    states_oth,
+    out,
+    queries,
+    total,
+    even,
+    odd,
 ):
     for z in range(8):
         for h in range(3):
@@ -141,15 +161,13 @@
         z, y = (plan[i] // 8, plan[i] % 8)
         at = h * SPAN
         total[z, :, at : at + SPAN] += jnp.dot(
-            values[y], held[:, at : at + SPAN], preferred_element_type=F32
-        )
+            values_own[y], held[:SPAN, at : at + SPAN], preferred_element_type=F32
+        ) + jnp.dot(values_oth[y], held[SPAN:, at : at + SPAN], preferred_element_type=F32)
 
     def score(i, held, h, mask=None):
         z, y = (plan[i] // 8, plan[i] % 8)
-        for at in (0, SPAN):
-            weights = jnp.exp2(
-                jnp.dot(keys[y, at : at + SPAN], queries[z, h], preferred_element_type=F32)
-            )
+        for at, keys in ((0, keys_own), (SPAN, keys_oth)):
+            weights = jnp.exp2(jnp.dot(keys[y], queries[z, h], preferred_element_type=F32))
             if mask is not None:
                 weights = jnp.where(mask[at : at + SPAN], weights, 0.0)
             held[at : at + SPAN, h * SPAN : (h + 1) * SPAN] = weights.astype(BF16)
@@ -186,7 +204,9 @@
         out[z, 192:208] = jnp.concatenate(
             high + low + [jnp.zeros((10, SPAN), F32)], axis=0
         ).astype(BF16)
-        out[z, 208:] = states[z]
+        sums = (states_own[z] + states_oth[z]).astype(BF16)
+        out[z, 208:, :128] = sums[:48]
+        out[z, 208:, 128:] = sums[48:]
 
 
 def back_kernel(parts, local, lifted, w_out, out, mixed):
@@ -241,9 +261,7 @@
         ],
         axis=1,
     )
-    w_row = copies_from(shard, "y")
-    line_ends = jnp.sum(w_row[:, 0, 1280:1289].reshape(8, 3, 3).astype(F32), axis=1)
-    w_row = w_row[:, :, :1280].reshape(128, 1280)
+    w_row = copies_from(shard, "y").reshape(128, 1408)
     w_own = lax.all_gather(w_row, "z", axis=0, tiled=True)
 
     raw = tokens.astype(F32)
@@ -264,14 +282,6 @@
     cosine, sine = (jnp.cos(angles), jnp.sin(angles))
     decay = jnp.cumsum(retain_log, axis=0)
     decay_row = jnp.pad(decay.T, ((0, 5), (0, 0)))
-    ends_own = copies_from(line_ends, "z")
-    ends_oth = swapped_cores(ends_own)
-    ends = jnp.where(
-        c == 0,
-        jnp.stack([ends_own, ends_oth], axis=2),
-        jnp.stack([ends_oth, ends_own], axis=2),
-    ).reshape(128, 3)
-
     gate = (forget_total * LOG2E).reshape(3, 8, 8, 2, SPAN)
     spans = jnp.arange(8, dtype=jnp.int32)
     key_z = (z - spans) % 8
@@ -298,14 +308,6 @@
         ],
         axis=2,
     )
-    blocks = key_z * 16 + spans * 2
-    blocks = jnp.stack([blocks + c, blocks + 1 - c])
-    targets = spans * 16 + y * 2 + c
-    index = jnp.arange(128, dtype=jnp.int32)
-    between = (index > blocks[None, :, :, None]) & (index < targets[:, None, None, None])
-    fade = jnp.sum(jnp.where(between[..., None], ends, 0.0), axis=3)
-    earlier = blocks[None] < targets[:, None, None]
-    fade = jnp.where(earlier[..., None], jnp.exp(fade), 0.0).reshape(384)
     needed = (
         (key_z[None, :] < spans[:, None])
         | ((key_z[None, :] == spans[:, None]) & (spans[None, :] < y))
@@ -320,10 +322,17 @@
 
     own_part, oth_part = pl.pallas_call(
         project_kernel,
-        grid=(1,),
-        in_specs=[VMEM, pl.BlockSpec((1024, 896), lambda i: (0, 0))],
-        out_specs=[VMEM] * 2,
-        out_shape=[jax.ShapeDtypeStruct((SPAN, 896), F32)] * 2,
+        grid=(2,),
+        in_specs=[
+            pl.BlockSpec((2 * SPAN, 512), lambda i: (0, i)),
+            pl.BlockSpec((512, 896), lambda i: (i, 0)),
+        ],
+        out_specs=[pl.BlockSpec((SPAN, 896), lambda i: (0, 0))] * 2,
+        out_shape=[
+            jax.ShapeDtypeStruct((SPAN, 896), F32),
+            jax.ShapeDtypeStruct((SPAN, 896), BF16),
+        ],
+        scratch_shapes=[pltpu.VMEM((2 * SPAN, 896), F32)],
         compiler_params=PARAMS,
         name="project",
     )(rows, w_own)
@@ -344,6 +353,22 @@
     kv_send = lax.ppermute(kv_send, ("z", "y"), ROTATION)
     kv_own = copies_from(kv_send, "y")
     kv_oth = swapped_cores(kv_own)
+    ends_own = w_own[:, 1280:1289].reshape(8, 8, 16, 9)[:, :, 0].astype(F32)
+    ends_own = jnp.sum(ends_own.reshape(8, 8, 3, 3), axis=2)
+    ends_oth = swapped_cores(ends_own)
+    ends = jnp.where(
+        c == 0,
+        jnp.stack([ends_own, ends_oth], axis=2),
+        jnp.stack([ends_oth, ends_own], axis=2),
+    ).reshape(128, 3)
+    blocks = key_z * 16 + spans * 2
+    blocks = jnp.stack([blocks + c, blocks + 1 - c])
+    targets = spans * 16 + y * 2 + c
+    index = jnp.arange(128, dtype=jnp.int32)
+    between = (index > blocks[None, :, :, None]) & (index < targets[:, None, None, None])
+    fade = jnp.sum(jnp.where(between[..., None], ends, 0.0), axis=3)
+    earlier = blocks[None] < targets[:, None, None]
+    fade = jnp.where(earlier[..., None], jnp.exp(fade), 0.0).reshape(384)
     local, lifted = pl.pallas_call(
         local_kernel,
         in_specs=[VMEM] * 5,
@@ -352,28 +377,32 @@
         compiler_params=PARAMS,
         name="local",
     )(proj, cosine, sine, decay, decay_row)
-    out_own = w_own[:, 896:]
+    out_own = w_own[:, 896:1280]
     out_oth = swapped_cores(out_own).reshape(64, 16, 384)
     out_own = out_own.reshape(64, 16, 384)
     w_out = jnp.where(
         c == 0, jnp.stack([out_own, out_oth], axis=1), jnp.stack([out_oth, out_own], axis=1)
     ).reshape(2048, 384)
 
-    keys, values, states = pl.pallas_call(
-        prepare_kernel,
-        in_specs=[SMEM] + [VMEM] * 3,
-        out_specs=[VMEM] * 3,
-        out_shape=[
-            jax.ShapeDtypeStruct((8, 2 * SPAN, 128), BF16),
-            jax.ShapeDtypeStruct((8, 80, 2 * SPAN), BF16),
-            jax.ShapeDtypeStruct((8, 48, SPAN), BF16),
-        ],
-        compiler_params=PARAMS,
-        name="prepare",
-    )(fade, kv_own, kv_oth, key_gate)
+    def prepared(side, held):
+        return pl.pallas_call(
+            functools.partial(prepare_kernel, side),
+            in_specs=[SMEM] + [VMEM] * 2,
+            out_specs=[VMEM] * 3,
+            out_shape=[
+                jax.ShapeDtypeStruct((8, SPAN, 128), BF16),
+                jax.ShapeDtypeStruct((8, 80, SPAN), BF16),
+                jax.ShapeDtypeStruct((8, 96, 128), F32),
+            ],
+            compiler_params=PARAMS,
+            name="prepare",
+        )(fade, held, key_gate)
+
+    keys_own, values_own, states_own = prepared(0, kv_own)
+    keys_oth, values_oth, states_oth = prepared(1, kv_oth)
     partial = pl.pallas_call(
         attend_kernel,
-        in_specs=[SMEM] + [VMEM] * 5,
+        in_specs=[SMEM] + [VMEM] * 8,
         out_specs=VMEM,
         out_shape=jax.ShapeDtypeStruct((8, SPAN, SPAN), BF16),
         scratch_shapes=[
@@ -384,7 +413,17 @@
         ],
         compiler_params=PARAMS,
         name="attend",
-    )(plan, queries, query_gate, keys, values, states)
+    )(
+        plan,
+        queries,
+        query_gate,
+        keys_own,
+        keys_oth,
+        values_own,
+        values_oth,
+        states_own,
+        states_oth,
+    )
     parts = lax.all_to_all(partial, "z", 0, 0, tiled=True)
 
     share = pl.pallas_call(

time: 246 us -> 238 us (0.967)
  the two profiles are of different devices: /device:TPU:1 before, /device:TPU:56 now
where the time goes in v6:
time: 238 us; the launch traced here: 237 us
  waiting for transfers between devices  99.4 us (42%)
  starting transfers between devices  42.7 us (18%)
  Pallas kernels  41 us (17%)
  blocking collectives  15.4 us (6%)
  between operations  14.5 us (6%)
  other arithmetic  12.4 us (5%)
  local copies, waits for them, and re-layouts  11.4 us (5%)
    all_gather x1, waiting for transfers between devices, body(): w_own = lax.all_gather(w_row, 'z', axis=0, tiled=True)  36.6 us
    all_to_all x3, waiting for transfers between devices, copies_from(): return lax.all_to_all(copies, axis, split_axis=0, concat_axis=0, tiled=True)  29 us
    all_to_all x3, starting transfers between devices, copies_from(): return lax.all_to_all(copies, axis, split_axis=0, concat_axis=0, tiled=True)  24.1 us
    pallas_call x1, Pallas kernels, body(): pl.pallas_call(attend_kernel, in_specs=[SMEM] + [VMEM] * 8, out_specs=VME...  17.5 us
    all_to_all x1, waiting for transfers between devices, body(): parts = lax.all_to_all(partial, 'z', 0, 0, tiled=True)  16.4 us
    all_to_all x1, blocking collectives, body(): shares = lax.all_to_all(share.reshape(4, 64, 2048), 'tp', 0, 0, tiled=True)  15.4 us
    all_gather x1, waiting for transfers between devices, body(): queries = lax.all_gather(q_send, 'z', axis=0)  11 us
    ppermute x5, starting transfers between devices, swapped_cores(): return lax.ppermute(value, 'c', [(0, 1), (1, 0)])  10.2 us
  transfers between devices with their start and end apart: 12, of which 9 were waited for; matrix products, arithmetic and copies ran while one was open for 7% of the time, Pallas kernels for 4%

profile of v6, /device:TPU:56, one launch (start us, length us, event | category | flops | bytes accessed | tf_op | source)
XLA Modules:
  0.0 236.8 jit_solution(16965869763034391512)
XLA Ops:
  9.1 8.5 %all-to-all-start.1 = ((bf16[8,16,1408]{2,1,0:T(8,128)(2,1)}), bf16[8,16,1408]{2,1,0:T(8,128)(2,1)S(1)}, u32[]{:S(2)}, u32[]{:S(2)}) async-start(bf16[8,16,1408]{2,1,0:T(8,128)(2,1)} %broadcast_in_dim.108), calls=%async_computation.1 | async-start | bytes 720896 | tf_op jit(solution)/shard_map/all_to_all | solution.py:29
  19.8 6.9 %all-to-all-done.1 = bf16[8,16,1408]{2,1,0:T(8,128)(2,1)S(1)} async-done(((bf16[8,16,1408]{2,1,0:T(8,128)(2,1)}), bf16[8,16,1408]{2,1,0:T(8,128)(2,1)S(1)}, u32[]{:S(2)}, u32[]{:S(2)}) %all-to-all-start.1) | async-done | bytes 360480 | tf_op jit(solution)/shard_map/all_to_all | solution.py:29
  27.7 3.6 %all-to-all-start = ((bf16[4,2,64,1024]{3,2,1,0:T(8,128)(2,1)}), bf16[4,2,64,1024]{3,2,1,0:T(8,128)(2,1)S(1)}, u32[]{:S(2)}, u32[]{:S(2)}) async-start(bf16[4,2,64,1024]{3,2,1,0:T(8,128)(2,1)} %broadcast_in_dim.106), calls=%async_computation | async-start | bytes 2097152 | tf_op jit(solution)/shard_map/all_to_all | solution.py:29
  35.0 8.2 %all-to-all-done = bf16[4,2,64,1024]{3,2,1,0:T(8,128)(2,1)S(1)} async-done(((bf16[4,2,64,1024]{3,2,1,0:T(8,128)(2,1)}), bf16[4,2,64,1024]{3,2,1,0:T(8,128)(2,1)S(1)}, u32[]{:S(2)}, u32[]{:S(2)}) %all-to-all-start) | async-done | bytes 1048608 | tf_op jit(solution)/shard_map/all_to_all | solution.py:29
  43.2 1.9 collective-permute-start
  48.1 36.6 %all-gather.4.cloned.1.call-done.weights = bf16[1024,1408]{1,0:T(8,128)(2,1)} async-done(((bf16[128,1408]{1,0:T(8,128)(2,1)}), bf16[1024,1408]{1,0:T(8,128)(2,1)}) %all-gather.4.cloned.1.call-update) | async-done | bytes 2883600 | tf_op jit(solution)/shard_map/all_gather | solution.py:265
  84.7 4.2 %project.1 = (f32[256,896]{1,0:T(8,128)}, bf16[256,896]{1,0:T(8,128)(2,1)}) custom-call(bf16[512,1024]{1,0:T(8,128)(2,1)} %pad_maximum_fusion.rows, bf16[1024,1408]{1,0:T(8,128)(2,1)} %all-gather.4.cloned.1.call-done.weights), custom_call_target="tpu_custom_call" | custom-call | tf_op jit(solution)/shard_map/project/pallas_call | solution.py:323
  94.5 4.3 %front.1 = (bf16[256,256]{1,0:T(8,128)(2,1)}, bf16[352,128]{1,0:T(8,128)(2,1)}, f32[256,896]{1,0:T(8,128)}) custom-call(f32[256,896]{1,0:T(8,128)} %get-tuple-element.18.first_part, bf16[256,896]{1,0:T(8,128)(2,1)} %copy-done.5, f32[256,32]{1,0:T(8,128)} %get-tuple-element.43.cosine, f32[256,32]{1,0:T(8,128)} %get-tuple-element.42.sine, f32[256,3]{1,0:T(8,128)} %copy.127.decay), custom_call_target="tpu_custom_call" | custom-call | tf_op jit(solution)/shard_map/front/pallas_call | solution.py:339
  98.8 4.1 %collective-permute-start.3 = (bf16[352,128]{1,0:T(8,128)(2,1)}, bf16[352,128]{1,0:T(8,128)(2,1)S(1)}, u32[]{:S(2)}, u32[]{:S(2)}) collective-permute-start(bf16[352,128]{1,0:T(8,128)(2,1)} %get-tuple-element.21), channel_id=1, source_target_pairs={{0,0},{8,72},{16,144},{24,216},{32,288},{40,360},{48,432},{56,504}... | collective-permute-start | bytes 270344 | tf_op jit(solution)/shard_map/ppermute | solution.py:353
  102.9 3.0 %collective-permute-done.3 = bf16[352,128]{1,0:T(8,128)(2,1)S(1)} collective-permute-done((bf16[352,128]{1,0:T(8,128)(2,1)}, bf16[352,128]{1,0:T(8,128)(2,1)S(1)}, u32[]{:S(2)}, u32[]{:S(2)}) %collective-permute-start.3) | collective-permute-done | bytes 90144 | tf_op jit(solution)/shard_map/ppermute | solution.py:353
  106.9 12.0 %all-to-all-start.2 = ((bf16[8,352,128]{2,1,0:T(8,128)(2,1)}), bf16[8,352,128]{2,1,0:T(8,128)(2,1)S(1)}, u32[]{:S(2)}, u32[]{:S(2)}) async-start(bf16[8,352,128]{2,1,0:T(8,128)(2,1)} %broadcast_in_dim.116), calls=%async_computation.2 | async-start | bytes 1441792 | tf_op jit(solution)/shard_map/all_to_all | solution.py:29
  122.3 13.9 %all-to-all-done.2.held = bf16[8,352,128]{2,1,0:T(8,128)(2,1)S(1)} async-done(((bf16[8,352,128]{2,1,0:T(8,128)(2,1)}), bf16[8,352,128]{2,1,0:T(8,128)(2,1)S(1)}, u32[]{:S(2)}, u32[]{:S(2)}) %all-to-all-start.2) | async-done | bytes 720928 | tf_op jit(solution)/shard_map/all_to_all | solution.py:29
  136.2 1.9 collective-permute-start.4
  139.7 2.4 %collective-permute-start.2 = (f32[8,8,3]{1,0,2:T(8,128)S(1)}, f32[8,8,3]{1,0,2:T(8,128)S(1)}, u32[]{:S(2)}, u32[]{:S(2)}) collective-permute-start(f32[8,8,3]{1,0,2:T(8,128)S(1)} %convert_reduce_fusion), channel_id=1, source_target_pairs={{0,4},{4,0},{1,5},{5,1},{2,6},{6,2},{3,7},{7,3},{8,12},{12,8},{9,1... | collective-permute-start | bytes 2312 | tf_op jit(solution)/shard_map/ppermute | solution.py:33
  144.4 2.9 %prepare.2 = (bf16[8,256,128]{2,1,0:T(8,128)(2,1)}, bf16[8,80,256]{2,1,0:T(8,128)(2,1)}, f32[8,96,128]{2,1,0:T(8,128)}) custom-call(f32[384]{0:T(512)} %select_n.142.fade, bf16[8,352,128]{2,1,0:T(8,128)(2,1)} %copy-done.1, bf16[2,8,256,64]{3,2,1,0:T(8,128)(2,1)} %maximum_bitcast_fusion.key_gate), custom_call_target="tpu_custom_call" | custom-call | tf_op jit(solution)/shard_map/prepare/pallas_call | solution.py:388
  148.2 3.0 %prepare.3 = (bf16[8,256,128]{2,1,0:T(8,128)(2,1)}, bf16[8,80,256]{2,1,0:T(8,128)(2,1)}, f32[8,96,128]{2,1,0:T(8,128)}) custom-call(f32[384]{0:T(512)} %select_n.142.fade, bf16[8,352,128]{2,1,0:T(8,128)(2,1)} %copy-done.3, bf16[2,8,256,64]{3,2,1,0:T(8,128)(2,1)} %maximum_bitcast_fusion.key_gate), custom_call_target="tpu_custom_call" | custom-call | tf_op jit(solution)/shard_map/prepare/pallas_call | solution.py:388
  151.2 11.0 %all-gather.6.cloned.1.call-done = bf16[2048,256]{1,0:T(8,128)(2,1)} async-done(((bf16[256,256]{1,0:T(8,128)(2,1)}), bf16[2048,256]{1,0:T(8,128)(2,1)}) %all-gather.6.cloned.1.call-update) | async-done | bytes 1048592 | tf_op jit(solution)/shard_map/all_gather | solution.py:352
  162.3 17.5 %attend.1 = bf16[8,256,256]{2,1,0:T(8,128)(2,1)} custom-call(s32[67]{0:T(128)} %pad_add_fusion.1.plan, bf16[8,256,256]{2,1,0:T(8,128)(2,1)} %bitcast.73, bf16[8,3,64,256]{3,2,1,0:T(8,128)(2,1)} %maximum_maximum_fusion.query_gate, bf16[8,256,128]{2,1,0:T(8,128)(2,1)} %get-tuple-element.22.keys_own, bf16[8,256,128]{2,1,0:T(8,128)(2,1)} %get-tuple-element.23.keys_oth, ...), custom_call_target="tpu_custom_call" | custom-call | tf_op jit(solution)/shard_map/attend/pallas_call | solution.py:403
  179.8 4.2 %all-to-all-start.3 = ((bf16[8,256,256]{2,1,0:T(8,128)(2,1)}), bf16[8,256,256]{2,1,0:T(8,128)(2,1)}, u32[]{:S(2)}, u32[]{:S(2)}) async-start(bf16[8,256,256]{2,1,0:T(8,128)(2,1)} %attend.1), calls=%async_computation.3 | async-start | bytes 2097152 | tf_op jit(solution)/shard_map/all_to_all | solution.py:427
  184.1 2.1 collective-permute-start.5
  186.9 4.0 %local.1 = (f32[256,192]{1,0:T(8,128)}, bf16[256,192]{1,0:T(8,128)(2,1)}) custom-call(f32[256,896]{1,0:T(8,128)} %get-tuple-element.28.proj, f32[256,32]{1,0:T(8,128)} %get-tuple-element.43.cosine, f32[256,32]{1,0:T(8,128)} %get-tuple-element.42.sine, f32[256,3]{1,0:T(8,128)} %copy.127.decay, f32[8,256]{1,0:T(8,128)} %pad.9.decay_row), custom_call_target="tpu_custom_call" | custom-call | tf_op jit(solution)/shard_map/local/pallas_call | solution.py:372
  192.2 16.4 %all-to-all-done.3.parts = bf16[8,256,256]{2,1,0:T(8,128)(2,1)} async-done(((bf16[8,256,256]{2,1,0:T(8,128)(2,1)}), bf16[8,256,256]{2,1,0:T(8,128)(2,1)}, u32[]{:S(2)}, u32[]{:S(2)}) %all-to-all-start.3) | async-done | bytes 1048608 | tf_op jit(solution)/shard_map/all_to_all | solution.py:427
  208.7 5.0 %back.1 = bf16[256,2048]{1,0:T(8,128)(2,1)} custom-call(bf16[8,256,256]{2,1,0:T(8,128)(2,1)} %all-to-all-done.3.parts, f32[256,192]{1,0:T(8,128)} %get-tuple-element.29.local, bf16[256,192]{1,0:T(8,128)(2,1)} %get-tuple-element.30.lifted, bf16[2048,384]{1,0:T(8,128)(2,1)} %bitcast.65), custom_call_target="tpu_custom_call" | custom-call | tf_op jit(solution)/shard_map/back/pallas_call | solution.py:429
  213.7 15.4 %all_to_all.25 = bf16[4,64,2048]{2,1,0:T(8,128)(2,1)S(1)} all-to-all(bf16[4,64,2048]{2,1,0:T(8,128)(2,1)} %bitcast.67), channel_id=1, replica_groups=mesh['z'=8,'y'=8,'c'=2,'tp'=4] {'tp'}, dimensions={0} | all-to-all | bytes 2097152 | tf_op jit(solution)/shard_map/all_to_all | solution.py:438
  (112 shorter events, 29.1 us)
Async XLA Ops:
  6.5 12.6 %copy-start.7 = (f32[2048]{0:T(1024)S(1)}, f32[2048]{0:T(1024)}, u32[]{:S(2)}) copy-start(f32[2048]{0:T(1024)} %param.13) | copy-start | bytes 24580
  9.1 17.5 %all-to-all-start.1 = ((bf16[8,16,1408]{2,1,0:T(8,128)(2,1)}), bf16[8,16,1408]{2,1,0:T(8,128)(2,1)S(1)}, u32[]{:S(2)}, u32[]{:S(2)}) async-start(bf16[8,16,1408]{2,1,0:T(8,128)(2,1)} %broadcast_in_dim.108), calls=%async_computation.1 | async-start | bytes 720896 | tf_op jit(solution)/shard_map/all_to_all | solution.py:29
  19.7 12.4 %copy-start.4 = (f32[3,32768]{1,0:T(4,128)S(1)}, f32[3,32768]{1,0:T(4,128)}, u32[]{:S(2)}) copy-start(f32[3,32768]{1,0:T(4,128)} %param.23) | copy-start | bytes 1179652
  26.6 1.1 copy-start.2
  27.7 4.6 %copy-start.6 = (f32[256,3]{0,1:T(4,128)S(1)}, f32[256,3]{0,1:T(4,128)}, u32[]{:S(2)}) copy-start(f32[256,3]{0,1:T(4,128)} %param.22) | copy-start | bytes 9220
  27.7 15.4 %all-to-all-start = ((bf16[4,2,64,1024]{3,2,1,0:T(8,128)(2,1)}), bf16[4,2,64,1024]{3,2,1,0:T(8,128)(2,1)S(1)}, u32[]{:S(2)}, u32[]{:S(2)}) async-start(bf16[4,2,64,1024]{3,2,1,0:T(8,128)(2,1)} %broadcast_in_dim.106), calls=%async_computation | async-start | bytes 2097152 | tf_op jit(solution)/shard_map/all_to_all | solution.py:29
  31.4 53.3 %all-gather.4.cloned.1.call-start = ((), (), s32[]{:S(2)}) async-start(), calls=%async_computation.5 | async-start | bytes 3244032 | tf_op jit(solution)/shard_map/all_gather | solution.py:265
  43.2 3.8 %collective-permute-start = (bf16[256,1024]{1,0:T(8,128)(2,1)S(1)}, bf16[256,1024]{1,0:T(8,128)(2,1)S(1)}, u32[]{:S(2)}, u32[]{:S(2)}) collective-permute-start(bf16[256,1024]{1,0:T(8,128)(2,1)S(1)} %bitcast.75), channel_id=1, source_target_pairs={{0,4},{4,0},{1,5},{5,1},{2,6},{6,2},{3,7},{7,3},{8,12},{12,8},{9,1... | collective-permute-start | bytes 1572872 | tf_op jit(solution)/shard_map/ppermute | solution.py:33
  88.9 4.8 %collective-permute-start.1 = (bf16[256,896]{1,0:T(8,128)(2,1)}, bf16[256,896]{1,0:T(8,128)(2,1)S(1)}, u32[]{:S(2)}, u32[]{:S(2)}) collective-permute-start(bf16[256,896]{1,0:T(8,128)(2,1)} %get-tuple-element.19), channel_id=1, source_target_pairs={{0,4},{4,0},{1,5},{5,1},{2,6},{6,2},{3,7},{7,3},{8,12},{12,8},{9,1... | collective-permute-start | bytes 1376264 | tf_op jit(solution)/shard_map/ppermute | solution.py:33
  93.7 0.8 copy-start.5
  98.8 7.1 %collective-permute-start.3 = (bf16[352,128]{1,0:T(8,128)(2,1)}, bf16[352,128]{1,0:T(8,128)(2,1)S(1)}, u32[]{:S(2)}, u32[]{:S(2)}) collective-permute-start(bf16[352,128]{1,0:T(8,128)(2,1)} %get-tuple-element.21), channel_id=1, source_target_pairs={{0,0},{8,72},{16,144},{24,216},{32,288},{40,360},{48,432},{56,504}... | collective-permute-start | bytes 270344 | tf_op jit(solution)/shard_map/ppermute | solution.py:353
  106.9 29.3 %all-to-all-start.2 = ((bf16[8,352,128]{2,1,0:T(8,128)(2,1)}), bf16[8,352,128]{2,1,0:T(8,128)(2,1)S(1)}, u32[]{:S(2)}, u32[]{:S(2)}) async-start(bf16[8,352,128]{2,1,0:T(8,128)(2,1)} %broadcast_in_dim.116), calls=%async_computation.2 | async-start | bytes 1441792 | tf_op jit(solution)/shard_map/all_to_all | solution.py:29
  118.8 43.4 %all-gather.6.cloned.1.call-start = ((), (), s32[]{:S(2)}) async-start(), calls=%async_computation.6 | async-start | bytes 1179648 | tf_op jit(solution)/shard_map/all_gather | solution.py:352
  121.0 18.5 %slice-start = ((bf16[1024,1408]{1,0:T(8,128)(2,1)}), bf16[1024,9]{1,0:T(8,128)(2,1)S(1)}, s32[]{:S(2)}) async-start(bf16[1024,1408]{1,0:T(8,128)(2,1)} %all-gather.4.cloned.1.call-done.weights), calls=%async_computation.7 | async-start | bytes 524288 | tf_op jit(solution)/shard_map/slice | solution.py:356
  136.2 8.2 %copy-start.1 = (bf16[8,352,128]{2,1,0:T(8,128)(2,1)}, bf16[8,352,128]{2,1,0:T(8,128)(2,1)S(1)}, u32[]{:S(2)}) copy-start(bf16[8,352,128]{2,1,0:T(8,128)(2,1)S(1)} %all-to-all-done.2.held) | copy-start | bytes 2162692
  136.2 11.1 %collective-permute-start.4 = (bf16[8,352,128]{2,1,0:T(8,128)(2,1)S(1)}, bf16[8,352,128]{2,1,0:T(8,128)(2,1)S(1)}, u32[]{:S(2)}, u32[]{:S(2)}) collective-permute-start(bf16[8,352,128]{2,1,0:T(8,128)(2,1)S(1)} %all-to-all-done.2.held), channel_id=1, source_target_pairs={{0,4},{4,0},{1,5},{5,1},{2,6},{6,2},{3,7},{7,3},{8,12},{12,8},{9,1... | collective-permute-start | bytes 2162696 | tf_op jit(solution)/shard_map/ppermute | solution.py:33
  139.7 3.2 %collective-permute-start.2 = (f32[8,8,3]{1,0,2:T(8,128)S(1)}, f32[8,8,3]{1,0,2:T(8,128)S(1)}, u32[]{:S(2)}, u32[]{:S(2)}) collective-permute-start(f32[8,8,3]{1,0,2:T(8,128)S(1)} %convert_reduce_fusion), channel_id=1, source_target_pairs={{0,4},{4,0},{1,5},{5,1},{2,6},{6,2},{3,7},{7,3},{8,12},{12,8},{9,1... | collective-permute-start | bytes 2312 | tf_op jit(solution)/shard_map/ppermute | solution.py:33
  147.3 0.9 copy-start.3
  162.3 21.8 %copy-start = (bf16[1024,1408]{1,0:T(8,128)(2,1)S(1)}, bf16[1024,1408]{1,0:T(8,128)(2,1)}, u32[]{:S(2)}) copy-start(bf16[1024,1408]{1,0:T(8,128)(2,1)} %all-gather.4.cloned.1.call-done.weights) | copy-start | bytes 8650756
  179.8 28.9 %all-to-all-start.3 = ((bf16[8,256,256]{2,1,0:T(8,128)(2,1)}), bf16[8,256,256]{2,1,0:T(8,128)(2,1)}, u32[]{:S(2)}, u32[]{:S(2)}) async-start(bf16[8,256,256]{2,1,0:T(8,128)(2,1)} %attend.1), calls=%async_computation.3 | async-start | bytes 2097152 | tf_op jit(solution)/shard_map/all_to_all | solution.py:427
  184.1 6.7 %collective-permute-start.5 = (bf16[1024,384]{1,0:T(8,128)(2,1)S(1)}, bf16[1024,384]{1,0:T(8,128)(2,1)S(1)}, u32[]{:S(2)}, u32[]{:S(2)}) collective-permute-start(bf16[1024,384]{1,0:T(8,128)(2,1)S(1)} %slice.35), channel_id=1, source_target_pairs={{0,4},{4,0},{1,5},{5,1},{2,6},{6,2},{3,7},{7,3},{8,12},{12,8},{9,1... | collective-permute-start | bytes 2359304 | tf_op jit(solution)/shard_map/ppermute | solution.py:33
Sparse Core Ops, SparseCore 0:
  34.3 50.3 all-gather.3
  121.7 40.5 all-gather.5

commit v7 on v6

--- a/solution.py
+++ b/solution.py
@@ -41,22 +41,20 @@
     return [part.astype(BF16) for part in (high, middle, low)]
 
 
-def project_kernel(rows, weights, own_out, oth_out, product):
-    step = pl.program_id(0)
-    part = jnp.dot(rows[...], weights[...], preferred_element_type=F32)
-
-    @pl.when(step == 0)
-    def _():
-        product[...] = part
-
-    @pl.when(step > 0)
-    def _():
-        product[...] += part
-
-    @pl.when(step == pl.num_programs(0) - 1)
-    def _():
-        own_out[...] = product[:SPAN]
-        oth_out[...] = product[SPAN:].astype(BF16)
+def project_kernel(rows, weights, own_out, oth_out):
+    product = jnp.dot(rows[...], weights[...], preferred_element_type=F32)
+    own_out[...] = product[:SPAN]
+    oth_out[...] = product[SPAN:]
+
+
+def share_kernel(first_part, second_part, q_out, kv_out):
+    query = first_part[:, :192] + second_part[:, :192]
+    q_out[192:] = jnp.zeros((HEAD, SPAN), BF16)
+    q_out[:192] = jnp.transpose(query * (HEAD ** (-0.5) * LOG2E)).astype(BF16)
+    both = first_part[:, 192:320] + second_part[:, 192:320]
+    flipped = jnp.transpose(both)[HEAD:, :].astype(BF16)
+    kv_out[:128] = jnp.concatenate([both[:128, :HEAD], both[128:, :HEAD]], axis=1).astype(BF16)
+    kv_out[128:] = jnp.concatenate([flipped[:, :128], flipped[:, 128:]], axis=0)
 
 
 def turned(proj, at, cos, sin):
@@ -65,26 +63,18 @@
     return jnp.concatenate([first * cos - second * sin, first * sin + second * cos], axis=1)
 
 
-def front_kernel(first_part, second_part, cosine, sine, decay, q_out, kv_out, proj_out):
-    proj_out[...] = first_part[...] + second_part[...].astype(F32)
+def front_kernel(first_part, second_part, cosine, sine, decay, state_out, proj_out):
+    proj_out[...] = first_part[...] + second_part[...]
     cos = cosine[...]
     sin = sine[...]
     for h in range(3):
-        key = turned(proj_out, 192 + h * HEAD, cos, sin).astype(BF16)
-        value = proj_out[:, 384 + h * HEAD : 384 + (h + 1) * HEAD].astype(BF16)
+        key = turned(proj_out, 512 + h * HEAD, cos, sin).astype(BF16)
+        value = proj_out[:, 704 + h * HEAD : 704 + (h + 1) * HEAD].astype(BF16)
         column = decay[:, h : h + 1]
         last = decay[SPAN - 1 : SPAN, h : h + 1]
         faded = (key.astype(F32) * jnp.exp(last - column)).astype(BF16)
         update = lax.dot_general(faded, value, TN, preferred_element_type=F32).astype(BF16)
-        kv_out[SPAN + 32 * h : SPAN + 32 * (h + 1)] = jnp.concatenate(
-            [update[:32], update[32:]], axis=1
-        )
-    q_out[192:] = jnp.zeros((HEAD, SPAN), BF16)
-    q_out[:192] = jnp.transpose(proj_out[:, 576:768] * (HEAD ** (-0.5) * LOG2E)).astype(BF16)
-    both = proj_out[:, 768:896]
-    flipped = jnp.transpose(both)[HEAD:, :].astype(BF16)
-    kv_out[:128] = jnp.concatenate([both[:128, :HEAD], both[128:, :HEAD]], axis=1).astype(BF16)
-    kv_out[128:SPAN] = jnp.concatenate([flipped[:, :128], flipped[:, 128:]], axis=0)
+        state_out[32 * h : 32 * (h + 1)] = jnp.concatenate([update[:32], update[32:]], axis=1)
 
 
 def local_kernel(proj, cosine, sine, decay, decay_row, local_out, lifted_out):
@@ -94,9 +84,9 @@
     other = lax.broadcasted_iota(jnp.int32, (SPAN, SPAN), 1)
     causal = place >= other
     for h in range(3):
-        query = (turned(proj, h * HEAD, cos, sin) * HEAD ** (-0.5)).astype(BF16)
-        key = turned(proj, 192 + h * HEAD, cos, sin).astype(BF16)
-        value = proj[:, 384 + h * HEAD : 384 + (h + 1) * HEAD].astype(BF16)
+        query = (turned(proj, 320 + h * HEAD, cos, sin) * HEAD ** (-0.5)).astype(BF16)
+        key = turned(proj, 512 + h * HEAD, cos, sin).astype(BF16)
+        value = proj[:, 704 + h * HEAD : 704 + (h + 1) * HEAD].astype(BF16)
         column = decay[:, h : h + 1]
         scores = lax.dot_general(query, key, NT, preferred_element_type=F32)
         gap = jnp.where(causal, column - decay_row[h : h + 1, :], 0.0)
@@ -249,19 +239,21 @@
     ends = jnp.concatenate(three_parts(jnp.sum(retain_log, axis=0)))
     shard = jnp.concatenate(
         [
+            w_query_att,
+            w_key_att,
+            w_value_att,
             w_query_ret,
             w_key_ret,
             w_value_ret,
-            w_query_att,
-            w_key_att,
-            w_value_att,
             w_out_ret.T,
             w_out_att.T,
             jnp.pad(ends[None, :], ((0, 15), (0, 119))),
         ],
         axis=1,
     )
-    w_row = copies_from(shard, "y").reshape(128, 1408)
+    w_row = copies_from(shard, "y")
+    line_ends = jnp.sum(w_row[:, 0, 1280:1289].reshape(8, 3, 3).astype(F32), axis=1)
+    w_row = w_row[:, :, :1280].reshape(128, 1280)
     w_own = lax.all_gather(w_row, "z", axis=0, tiled=True)
 
     raw = tokens.astype(F32)
@@ -282,6 +274,14 @@
     cosine, sine = (jnp.cos(angles), jnp.sin(angles))
     decay = jnp.cumsum(retain_log, axis=0)
     decay_row = jnp.pad(decay.T, ((0, 5), (0, 0)))
+    ends_own = copies_from(line_ends, "z")
+    ends_oth = swapped_cores(ends_own)
+    ends = jnp.where(
+        c == 0,
+        jnp.stack([ends_own, ends_oth], axis=2),
+        jnp.stack([ends_oth, ends_own], axis=2),
+    ).reshape(128, 3)
+
     gate = (forget_total * LOG2E).reshape(3, 8, 8, 2, SPAN)
     spans = jnp.arange(8, dtype=jnp.int32)
     key_z = (z - spans) % 8
@@ -308,6 +308,14 @@
         ],
         axis=2,
     )
+    blocks = z * 16 + spans * 2
+    blocks = jnp.stack([blocks + c, blocks + 1 - c])
+    targets = spans * 16 + y * 2 + c
+    index = jnp.arange(128, dtype=jnp.int32)
+    between = (index > blocks[None, :, :, None]) & (index < targets[:, None, None, None])
+    fade = jnp.sum(jnp.where(between[..., None], ends, 0.0), axis=3)
+    earlier = blocks[None] < targets[:, None, None]
+    fade = jnp.where(earlier[..., None], jnp.exp(fade), 0.0).reshape(384)
     needed = (
         (key_z[None, :] < spans[:, None])
         | ((key_z[None, :] == spans[:, None]) & (spans[None, :] < y))
@@ -322,53 +330,40 @@
 
     own_part, oth_part = pl.pallas_call(
         project_kernel,
-        grid=(2,),
-        in_specs=[
-            pl.BlockSpec((2 * SPAN, 512), lambda i: (0, i)),
-            pl.BlockSpec((512, 896), lambda i: (i, 0)),
-        ],
-        out_specs=[pl.BlockSpec((SPAN, 896), lambda i: (0, 0))] * 2,
-        out_shape=[
-            jax.ShapeDtypeStruct((SPAN, 896), F32),
-            jax.ShapeDtypeStruct((SPAN, 896), BF16),
-        ],
-        scratch_shapes=[pltpu.VMEM((2 * SPAN, 896), F32)],
+        grid=(1,),
+        in_specs=[VMEM, pl.BlockSpec((1024, 896), lambda i: (0, 0))],
+        out_specs=[VMEM] * 2,
+        out_shape=[jax.ShapeDtypeStruct((SPAN, 896), F32)] * 2,
         compiler_params=PARAMS,
         name="project",
     )(rows, w_own)
-    q_send, kv_send, proj = pl.pallas_call(
+    came_part = swapped_cores(oth_part)
+    attention_part = pl.BlockSpec((SPAN, 384), lambda i: (0, 0))
+    q_send, kv_send = pl.pallas_call(
+        share_kernel,
+        grid=(1,),
+        in_specs=[attention_part] * 2,
+        out_specs=[VMEM] * 2,
+        out_shape=[
+            jax.ShapeDtypeStruct((SPAN, SPAN), BF16),
+            jax.ShapeDtypeStruct((SPAN, 128), BF16),
+        ],
+        compiler_params=PARAMS,
+        name="share",
+    )(own_part, came_part)
+    queries = lax.all_gather(q_send, "z", axis=0)
+    kv_send = lax.ppermute(kv_send, ("z", "y"), ROTATION)
+    state_send, proj = pl.pallas_call(
         front_kernel,
         in_specs=[VMEM] * 5,
-        out_specs=[VMEM] * 3,
-        out_shape=[
-            jax.ShapeDtypeStruct((SPAN, SPAN), BF16),
-            jax.ShapeDtypeStruct((SPAN + 96, 128), BF16),
-            jax.ShapeDtypeStruct((SPAN, 896), F32),
-        ],
+        out_specs=[VMEM] * 2,
+        out_shape=[jax.ShapeDtypeStruct((96, 128), BF16), jax.ShapeDtypeStruct((SPAN, 896), F32)],
         compiler_params=PARAMS,
         name="front",
-    )(own_part, swapped_cores(oth_part), cosine, sine, decay)
-
-    queries = lax.all_gather(q_send, "z", axis=0)
-    kv_send = lax.ppermute(kv_send, ("z", "y"), ROTATION)
+    )(own_part, came_part, cosine, sine, decay)
+    kv_send = jnp.concatenate([kv_send, state_send], axis=0)
     kv_own = copies_from(kv_send, "y")
     kv_oth = swapped_cores(kv_own)
-    ends_own = w_own[:, 1280:1289].reshape(8, 8, 16, 9)[:, :, 0].astype(F32)
-    ends_own = jnp.sum(ends_own.reshape(8, 8, 3, 3), axis=2)
-    ends_oth = swapped_cores(ends_own)
-    ends = jnp.where(
-        c == 0,
-        jnp.stack([ends_own, ends_oth], axis=2),
-        jnp.stack([ends_oth, ends_own], axis=2),
-    ).reshape(128, 3)
-    blocks = key_z * 16 + spans * 2
-    blocks = jnp.stack([blocks + c, blocks + 1 - c])
-    targets = spans * 16 + y * 2 + c
-    index = jnp.arange(128, dtype=jnp.int32)
-    between = (index > blocks[None, :, :, None]) & (index < targets[:, None, None, None])
-    fade = jnp.sum(jnp.where(between[..., None], ends, 0.0), axis=3)
-    earlier = blocks[None] < targets[:, None, None]
-    fade = jnp.where(earlier[..., None], jnp.exp(fade), 0.0).reshape(384)
     local, lifted = pl.pallas_call(
         local_kernel,
         in_specs=[VMEM] * 5,

time: 238 us -> 245 us (1.029)
  the two profiles are of different devices: /device:TPU:56 before, /device:TPU:1 now
where the time goes in v7:
time: 245 us; the launch traced here: 244 us
  waiting for transfers between devices  90.3 us (37%)
  starting transfers between devices  53.6 us (22%)
  Pallas kernels  39.7 us (16%)
  blocking collectives  18.1 us (7%)
  local copies, waits for them, and re-layouts  15.1 us (6%)
  between operations  14.4 us (6%)
  other arithmetic  13.1 us (5%)
    all_to_all x4, waiting for transfers between devices, copies_from(): return lax.all_to_all(copies, axis, split_axis=0, concat_axis=0, tiled=True)  43 us
    all_to_all x4, starting transfers between devices, copies_from(): return lax.all_to_all(copies, axis, split_axis=0, concat_axis=0, tiled=True)  30 us
    all_gather x1, waiting for transfers between devices, body(): w_own = lax.all_gather(w_row, 'z', axis=0, tiled=True)  25.6 us
    ppermute x5, starting transfers between devices, swapped_cores(): return lax.ppermute(value, 'c', [(0, 1), (1, 0)])  18.6 us
    all_to_all x1, waiting for transfers between devices, body(): parts = lax.all_to_all(partial, 'z', 0, 0, tiled=True)  18.4 us
    all_to_all x1, blocking collectives, body(): shares = lax.all_to_all(share.reshape(4, 64, 2048), 'tp', 0, 0, tiled=True)  18.1 us
    pallas_call x1, Pallas kernels, body(): pl.pallas_call(attend_kernel, in_specs=[SMEM] + [VMEM] * 8, out_specs=VME...  14.6 us
    pallas_call x2, Pallas kernels, prepared(): pl.pallas_call(functools.partial(prepare_kernel, side), in_specs=[SMEM] +...  5.93 us
  transfers between devices with their start and end apart: 13, of which 9 were waited for; matrix products, arithmetic and copies ran while one was open for 8% of the time, Pallas kernels for 6%

profile of v7, /device:TPU:1, one launch (start us, length us, event | category | flops | bytes accessed | tf_op | source)
XLA Modules:
  0.0 244.3 jit_solution(8993706906213861949)
XLA Ops:
  9.1 7.6 %all-to-all-start.1 = ((bf16[8,16,1408]{2,1,0:T(8,128)(2,1)}), bf16[8,16,1408]{2,1,0:T(8,128)(2,1)S(1)}, u32[]{:S(2)}, u32[]{:S(2)}) async-start(bf16[8,16,1408]{2,1,0:T(8,128)(2,1)} %broadcast_in_dim.111), calls=%async_computation.1 | async-start | bytes 720896 | tf_op jit(solution)/shard_map/all_to_all | solution.py:29
  18.9 8.5 %all-to-all-done.1 = bf16[8,16,1408]{2,1,0:T(8,128)(2,1)S(1)} async-done(((bf16[8,16,1408]{2,1,0:T(8,128)(2,1)}), bf16[8,16,1408]{2,1,0:T(8,128)(2,1)S(1)}, u32[]{:S(2)}, u32[]{:S(2)}) %all-to-all-start.1) | async-done | bytes 360480 | tf_op jit(solution)/shard_map/all_to_all | solution.py:29
  28.5 6.9 %all-to-all-start = ((bf16[4,2,64,1024]{3,2,1,0:T(8,128)(2,1)}), bf16[4,2,64,1024]{3,2,1,0:T(8,128)(2,1)S(1)}, u32[]{:S(2)}, u32[]{:S(2)}) async-start(bf16[4,2,64,1024]{3,2,1,0:T(8,128)(2,1)} %broadcast_in_dim.109), calls=%async_computation | async-start | bytes 2097152 | tf_op jit(solution)/shard_map/all_to_all | solution.py:29
  38.6 10.2 %all-to-all-done = bf16[4,2,64,1024]{3,2,1,0:T(8,128)(2,1)S(1)} async-done(((bf16[4,2,64,1024]{3,2,1,0:T(8,128)(2,1)}), bf16[4,2,64,1024]{3,2,1,0:T(8,128)(2,1)S(1)}, u32[]{:S(2)}, u32[]{:S(2)}) %all-to-all-start) | async-done | bytes 1048608 | tf_op jit(solution)/shard_map/all_to_all | solution.py:29
  48.9 4.6 %collective-permute-start = (bf16[256,1024]{1,0:T(8,128)(2,1)S(1)}, bf16[256,1024]{1,0:T(8,128)(2,1)S(1)}, u32[]{:S(2)}, u32[]{:S(2)}) collective-permute-start(bf16[256,1024]{1,0:T(8,128)(2,1)S(1)} %bitcast.73), channel_id=1, source_target_pairs={{0,4},{4,0},{1,5},{5,1},{2,6},{6,2},{3,7},{7,3},{8,12},{12,8},{9,1... | collective-permute-start | bytes 1572872 | tf_op jit(solution)/shard_map/ppermute | solution.py:33
  56.1 25.6 %all-gather.4.cloned.1.call-done.weights = bf16[1024,1280]{1,0:T(8,128)(2,1)} async-done(((bf16[128,1280]{1,0:T(8,128)(2,1)}), bf16[1024,1280]{1,0:T(8,128)(2,1)}) %all-gather.4.cloned.1.call-update) | async-done | bytes 2621456 | tf_op jit(solution)/shard_map/all_gather | solution.py:257
  81.7 4.3 %project.1 = (f32[256,896]{1,0:T(8,128)}, f32[256,896]{1,0:T(8,128)}) custom-call(bf16[512,1024]{1,0:T(8,128)(2,1)} %pad_maximum_fusion.rows, bf16[1024,1280]{1,0:T(8,128)(2,1)} %all-gather.4.cloned.1.call-done.weights), custom_call_target="tpu_custom_call" | custom-call | tf_op jit(solution)/shard_map/project/pallas_call | solution.py:331
  85.9 5.7 %collective-permute-start.1 = (f32[256,896]{1,0:T(8,128)}, f32[256,896]{1,0:T(8,128)S(1)}, u32[]{:S(2)}, u32[]{:S(2)}) collective-permute-start(f32[256,896]{1,0:T(8,128)} %get-tuple-element.20), channel_id=1, source_target_pairs={{0,4},{4,0},{1,5},{5,1},{2,6},{6,2},{3,7},{7,3},{8,12},{12,8},{9,1... | collective-permute-start | bytes 2752520 | tf_op jit(solution)/shard_map/ppermute | solution.py:33
  99.5 3.8 %front.1 = (bf16[96,128]{1,0:T(8,128)(2,1)}, f32[256,896]{1,0:T(8,128)}) custom-call(f32[256,896]{1,0:T(8,128)} %get-tuple-element.19.first_part, f32[256,896]{1,0:T(8,128)} %copy-done.1, f32[256,32]{1,0:T(8,128)} %get-tuple-element.45.cosine, f32[256,32]{1,0:T(8,128)} %get-tuple-element.44.sine, f32[256,3]{1,0:T(8,128)} %copy.151.decay), custom_call_target="tpu_custom_call" | custom-call | tf_op jit(solution)/shard_map/front/pallas_call | solution.py:356
  105.0 10.7 %all-to-all-start.3 = ((bf16[8,352,128]{2,1,0:T(8,128)(2,1)}), bf16[8,352,128]{2,1,0:T(8,128)(2,1)S(1)}, u32[]{:S(2)}, u32[]{:S(2)}) async-start(bf16[8,352,128]{2,1,0:T(8,128)(2,1)} %broadcast_in_dim.120), calls=%async_computation.3 | async-start | bytes 1441792 | tf_op jit(solution)/shard_map/all_to_all | solution.py:29
  119.1 18.9 %all-to-all-done.3.held = bf16[8,352,128]{2,1,0:T(8,128)(2,1)S(1)} async-done(((bf16[8,352,128]{2,1,0:T(8,128)(2,1)}), bf16[8,352,128]{2,1,0:T(8,128)(2,1)S(1)}, u32[]{:S(2)}, u32[]{:S(2)}) %all-to-all-start.3) | async-done | bytes 720928 | tf_op jit(solution)/shard_map/all_to_all | solution.py:29
  137.9 2.4 collective-permute-start.4
  141.1 4.7 %all-to-all-start.2 = ((f32[8,8,3]{1,2,0:T(4,128)}), f32[8,8,3]{1,2,0:T(4,128)S(1)}, u32[]{:S(2)}, u32[]{:S(2)}) async-start(f32[8,8,3]{1,2,0:T(4,128)} %broadcast_in_dim.116), calls=%async_computation.2 | async-start | bytes 32768 | tf_op jit(solution)/shard_map/all_to_all | solution.py:29
  147.0 5.4 %all-to-all-done.2 = f32[8,8,3]{1,2,0:T(4,128)S(1)} async-done(((f32[8,8,3]{1,2,0:T(4,128)}), f32[8,8,3]{1,2,0:T(4,128)S(1)}, u32[]{:S(2)}, u32[]{:S(2)}) %all-to-all-start.2) | async-done | bytes 800 | tf_op jit(solution)/shard_map/all_to_all | solution.py:29
  152.4 3.5 %collective-permute-start.2 = (f32[8,8,3]{1,2,0:T(4,128)S(1)}, f32[8,8,3]{1,2,0:T(4,128)S(1)}, u32[]{:S(2)}, u32[]{:S(2)}) collective-permute-start(f32[8,8,3]{1,2,0:T(4,128)S(1)} %all-to-all-done.2), channel_id=1, source_target_pairs={{0,4},{4,0},{1,5},{5,1},{2,6},{6,2},{3,7},{7,3},{8,12},{12,8},{9,1... | collective-permute-start | bytes 2312 | tf_op jit(solution)/shard_map/ppermute | solution.py:33
  158.2 3.0 %prepare.2 = (bf16[8,256,128]{2,1,0:T(8,128)(2,1)}, bf16[8,80,256]{2,1,0:T(8,128)(2,1)}, f32[8,96,128]{2,1,0:T(8,128)}) custom-call(f32[384]{0:T(512)} %select_n.129.fade, bf16[8,352,128]{2,1,0:T(8,128)(2,1)} %copy-done.2, bf16[2,8,256,64]{3,2,1,0:T(8,128)(2,1)} %maximum_bitcast_fusion.key_gate), custom_call_target="tpu_custom_call" | custom-call | tf_op jit(solution)/shard_map/prepare/pallas_call | solution.py:383
  162.1 3.0 %prepare.3 = (bf16[8,256,128]{2,1,0:T(8,128)(2,1)}, bf16[8,80,256]{2,1,0:T(8,128)(2,1)}, f32[8,96,128]{2,1,0:T(8,128)}) custom-call(f32[384]{0:T(512)} %select_n.129.fade, bf16[8,352,128]{2,1,0:T(8,128)(2,1)} %copy-done.3, bf16[2,8,256,64]{3,2,1,0:T(8,128)(2,1)} %maximum_bitcast_fusion.key_gate), custom_call_target="tpu_custom_call" | custom-call | tf_op jit(solution)/shard_map/prepare/pallas_call | solution.py:383
  165.1 14.6 %attend.1 = bf16[8,256,256]{2,1,0:T(8,128)(2,1)} custom-call(s32[67]{0:T(128)} %pad_add_fusion.1.plan, bf16[8,256,256]{2,1,0:T(8,128)(2,1)} %bitcast.71, bf16[8,3,64,256]{3,2,1,0:T(8,128)(2,1)} %maximum_maximum_fusion.query_gate, bf16[8,256,128]{2,1,0:T(8,128)(2,1)} %get-tuple-element.24.keys_own, bf16[8,256,128]{2,1,0:T(8,128)(2,1)} %get-tuple-element.25.keys_oth, ...), custom_call_target="tpu_custom_call" | custom-call | tf_op jit(solution)/shard_map/attend/pallas_call | solution.py:398
  179.7 3.6 %all-to-all-start.4 = ((bf16[8,256,256]{2,1,0:T(8,128)(2,1)}), bf16[8,256,256]{2,1,0:T(8,128)(2,1)S(1)}, u32[]{:S(2)}, u32[]{:S(2)}) async-start(bf16[8,256,256]{2,1,0:T(8,128)(2,1)} %attend.1), calls=%async_computation.4 | async-start | bytes 2097152 | tf_op jit(solution)/shard_map/all_to_all | solution.py:422
  184.5 2.4 collective-permute-start.5
  190.0 4.1 %local.1 = (f32[256,192]{1,0:T(8,128)}, bf16[256,192]{1,0:T(8,128)(2,1)}) custom-call(f32[256,896]{1,0:T(8,128)} %get-tuple-element.30.proj, f32[256,32]{1,0:T(8,128)} %get-tuple-element.45.cosine, f32[256,32]{1,0:T(8,128)} %get-tuple-element.44.sine, f32[256,3]{1,0:T(8,128)} %copy.151.decay, f32[8,256]{1,0:T(8,128)} %pad.9.decay_row), custom_call_target="tpu_custom_call" | custom-call | tf_op jit(solution)/shard_map/local/pallas_call | solution.py:367
  194.1 18.4 %all-to-all-done.4.parts = bf16[8,256,256]{2,1,0:T(8,128)(2,1)S(1)} async-done(((bf16[8,256,256]{2,1,0:T(8,128)(2,1)}), bf16[8,256,256]{2,1,0:T(8,128)(2,1)S(1)}, u32[]{:S(2)}, u32[]{:S(2)}) %all-to-all-start.4) | async-done | bytes 1048608 | tf_op jit(solution)/shard_map/all_to_all | solution.py:422
  213.5 5.0 %back.1 = bf16[256,2048]{1,0:T(8,128)(2,1)} custom-call(bf16[8,256,256]{2,1,0:T(8,128)(2,1)} %copy-done, f32[256,192]{1,0:T(8,128)} %get-tuple-element.31.local, bf16[256,192]{1,0:T(8,128)(2,1)} %get-tuple-element.32.lifted, bf16[2048,384]{1,0:T(8,128)(2,1)} %bitcast.64), custom_call_target="tpu_custom_call" | custom-call | tf_op jit(solution)/shard_map/back/pallas_call | solution.py:424
  218.5 18.1 %all_to_all.30 = bf16[4,64,2048]{2,1,0:T(8,128)(2,1)S(1)} all-to-all(bf16[4,64,2048]{2,1,0:T(8,128)(2,1)} %bitcast.65), channel_id=1, replica_groups=mesh['z'=8,'y'=8,'c'=2,'tp'=4] {'tp'}, dimensions={0} | all-to-all | bytes 2097152 | tf_op jit(solution)/shard_map/all_to_all | solution.py:433
  (118 shorter events, 35.0 us)
Async XLA Ops:
  6.5 11.7 %copy-start.6 = (f32[2048]{0:T(1024)S(1)}, f32[2048]{0:T(1024)}, u32[]{:S(2)}) copy-start(f32[2048]{0:T(1024)} %param.13) | copy-start | bytes 24580
  9.1 18.3 %all-to-all-start.1 = ((bf16[8,16,1408]{2,1,0:T(8,128)(2,1)}), bf16[8,16,1408]{2,1,0:T(8,128)(2,1)S(1)}, u32[]{:S(2)}, u32[]{:S(2)}) async-start(bf16[8,16,1408]{2,1,0:T(8,128)(2,1)} %broadcast_in_dim.111), calls=%async_computation.1 | async-start | bytes 720896 | tf_op jit(solution)/shard_map/all_to_all | solution.py:29
  28.5 7.7 %copy-start.4 = (f32[3,32768]{1,0:T(4,128)S(1)}, f32[3,32768]{1,0:T(4,128)}, u32[]{:S(2)}) copy-start(f32[3,32768]{1,0:T(4,128)} %param.23) | copy-start | bytes 1179652
  28.5 7.9 %copy-start.5 = (f32[256,3]{0,1:T(4,128)S(1)}, f32[256,3]{0,1:T(4,128)}, u32[]{:S(2)}) copy-start(f32[256,3]{0,1:T(4,128)} %param.22) | copy-start | bytes 9220
  28.5 20.3 %all-to-all-start = ((bf16[4,2,64,1024]{3,2,1,0:T(8,128)(2,1)}), bf16[4,2,64,1024]{3,2,1,0:T(8,128)(2,1)S(1)}, u32[]{:S(2)}, u32[]{:S(2)}) async-start(bf16[4,2,64,1024]{3,2,1,0:T(8,128)(2,1)} %broadcast_in_dim.109), calls=%async_computation | async-start | bytes 2097152 | tf_op jit(solution)/shard_map/all_to_all | solution.py:29
  35.5 46.2 %all-gather.4.cloned.1.call-start = ((), (), s32[]{:S(2)}) async-start(), calls=%async_computation.6 | async-start | bytes 2949120 | tf_op jit(solution)/shard_map/all_gather | solution.py:257
  48.9 6.1 %collective-permute-start = (bf16[256,1024]{1,0:T(8,128)(2,1)S(1)}, bf16[256,1024]{1,0:T(8,128)(2,1)S(1)}, u32[]{:S(2)}, u32[]{:S(2)}) collective-permute-start(bf16[256,1024]{1,0:T(8,128)(2,1)S(1)} %bitcast.73), channel_id=1, source_target_pairs={{0,4},{4,0},{1,5},{5,1},{2,6},{6,2},{3,7},{7,3},{8,12},{12,8},{9,1... | collective-permute-start | bytes 1572872 | tf_op jit(solution)/shard_map/ppermute | solution.py:33
  85.9 9.1 %collective-permute-start.1 = (f32[256,896]{1,0:T(8,128)}, f32[256,896]{1,0:T(8,128)S(1)}, u32[]{:S(2)}, u32[]{:S(2)}) collective-permute-start(f32[256,896]{1,0:T(8,128)} %get-tuple-element.20), channel_id=1, source_target_pairs={{0,4},{4,0},{1,5},{5,1},{2,6},{6,2},{3,7},{7,3},{8,12},{12,8},{9,1... | collective-permute-start | bytes 2752520 | tf_op jit(solution)/shard_map/ppermute | solution.py:33
  95.0 0.9 copy-start.1
  98.0 5.4 %collective-permute-start.3 = (bf16[256,128]{1,0:T(8,128)(2,1)}, bf16[256,128]{1,0:T(8,128)(2,1)S(1)}, u32[]{:S(2)}, u32[]{:S(2)}) collective-permute-start(bf16[256,128]{1,0:T(8,128)(2,1)} %get-tuple-element.22), channel_id=1, source_target_pairs={{0,0},{8,72},{16,144},{24,216},{32,288},{40,360},{48,432},{56,504}... | collective-permute-start | bytes 196616 | tf_op jit(solution)/shard_map/ppermute | solution.py:355
  105.0 32.9 %all-to-all-start.3 = ((bf16[8,352,128]{2,1,0:T(8,128)(2,1)}), bf16[8,352,128]{2,1,0:T(8,128)(2,1)S(1)}, u32[]{:S(2)}, u32[]{:S(2)}) async-start(bf16[8,352,128]{2,1,0:T(8,128)(2,1)} %broadcast_in_dim.120), calls=%async_computation.3 | async-start | bytes 1441792 | tf_op jit(solution)/shard_map/all_to_all | solution.py:29
  115.8 49.3 %all-gather.6.cloned.1.call-start = ((), (), s32[]{:S(2)}) async-start(), calls=%async_computation.7 | async-start | bytes 1179648 | tf_op jit(solution)/shard_map/all_gather | solution.py:354
  137.9 20.3 %copy-start.2 = (bf16[8,352,128]{2,1,0:T(8,128)(2,1)}, bf16[8,352,128]{2,1,0:T(8,128)(2,1)S(1)}, u32[]{:S(2)}) copy-start(bf16[8,352,128]{2,1,0:T(8,128)(2,1)S(1)} %all-to-all-done.3.held) | copy-start | bytes 2162692
  137.9 23.3 %collective-permute-start.4 = (bf16[8,352,128]{2,1,0:T(8,128)(2,1)S(1)}, bf16[8,352,128]{2,1,0:T(8,128)(2,1)S(1)}, u32[]{:S(2)}, u32[]{:S(2)}) collective-permute-start(bf16[8,352,128]{2,1,0:T(8,128)(2,1)S(1)} %all-to-all-done.3.held), channel_id=1, source_target_pairs={{0,4},{4,0},{1,5},{5,1},{2,6},{6,2},{3,7},{7,3},{8,12},{12,8},{9,1... | collective-permute-start | bytes 2162696 | tf_op jit(solution)/shard_map/ppermute | solution.py:33
  141.1 11.3 %all-to-all-start.2 = ((f32[8,8,3]{1,2,0:T(4,128)}), f32[8,8,3]{1,2,0:T(4,128)S(1)}, u32[]{:S(2)}, u32[]{:S(2)}) async-start(f32[8,8,3]{1,2,0:T(4,128)} %broadcast_in_dim.116), calls=%async_computation.2 | async-start | bytes 32768 | tf_op jit(solution)/shard_map/all_to_all | solution.py:29
  152.4 4.3 %collective-permute-start.2 = (f32[8,8,3]{1,2,0:T(4,128)S(1)}, f32[8,8,3]{1,2,0:T(4,128)S(1)}, u32[]{:S(2)}, u32[]{:S(2)}) collective-permute-start(f32[8,8,3]{1,2,0:T(4,128)S(1)} %all-to-all-done.2), channel_id=1, source_target_pairs={{0,4},{4,0},{1,5},{5,1},{2,6},{6,2},{3,7},{7,3},{8,12},{12,8},{9,1... | collective-permute-start | bytes 2312 | tf_op jit(solution)/shard_map/ppermute | solution.py:33
  161.2 0.9 copy-start.3
  179.7 32.8 %all-to-all-start.4 = ((bf16[8,256,256]{2,1,0:T(8,128)(2,1)}), bf16[8,256,256]{2,1,0:T(8,128)(2,1)S(1)}, u32[]{:S(2)}, u32[]{:S(2)}) async-start(bf16[8,256,256]{2,1,0:T(8,128)(2,1)} %attend.1), calls=%async_computation.4 | async-start | bytes 2097152 | tf_op jit(solution)/shard_map/all_to_all | solution.py:422
  184.5 4.2 %collective-permute-start.5 = (bf16[1024,384]{1,0:T(8,128)(2,1)S(1)}, bf16[1024,384]{1,0:T(8,128)(2,1)S(1)}, u32[]{:S(2)}, u32[]{:S(2)}) collective-permute-start(bf16[1024,384]{1,0:T(8,128)(2,1)S(1)} %slice.35), channel_id=1, source_target_pairs={{0,4},{4,0},{1,5},{5,1},{2,6},{6,2},{3,7},{7,3},{8,12},{12,8},{9,1... | collective-permute-start | bytes 2359304 | tf_op jit(solution)/shard_map/ppermute | solution.py:33
  212.5 1.0 copy-start
Sparse Core Ops, SparseCore 0:
  38.3 43.3 all-gather.3
  118.7 37.4 all-gather.5

commit v8 on v4

--- a/solution.py
+++ b/solution.py
@@ -45,32 +45,34 @@
     oth_out[...] = product[SPAN:]
 
 
+def share_kernel(first_part, second_part, q_out, kv_out):
+    query = first_part[:, :192] + second_part[:, :192]
+    q_out[192:] = jnp.zeros((HEAD, SPAN), BF16)
+    q_out[:192] = jnp.transpose(query * (HEAD ** (-0.5) * LOG2E)).astype(BF16)
+    both = first_part[:, 192:320] + second_part[:, 192:320]
+    flipped = jnp.transpose(both)[HEAD:, :].astype(BF16)
+    kv_out[:128] = jnp.concatenate([both[:128, :HEAD], both[128:, :HEAD]], axis=1).astype(BF16)
+    kv_out[128:] = jnp.concatenate([flipped[:, :128], flipped[:, 128:]], axis=0)
+
+
 def turned(proj, at, cos, sin):
     first = proj[:, at : at + 32]
     second = proj[:, at + 32 : at + 64]
     return jnp.concatenate([first * cos - second * sin, first * sin + second * cos], axis=1)
 
 
-def front_kernel(first_part, second_part, cosine, sine, decay, q_out, kv_out, proj_out):
+def front_kernel(first_part, second_part, cosine, sine, decay, state_out, proj_out):
     proj_out[...] = first_part[...] + second_part[...]
     cos = cosine[...]
     sin = sine[...]
     for h in range(3):
-        key = turned(proj_out, 192 + h * HEAD, cos, sin).astype(BF16)
-        value = proj_out[:, 384 + h * HEAD : 384 + (h + 1) * HEAD].astype(BF16)
+        key = turned(proj_out, 512 + h * HEAD, cos, sin).astype(BF16)
+        value = proj_out[:, 704 + h * HEAD : 704 + (h + 1) * HEAD].astype(BF16)
         column = decay[:, h : h + 1]
         last = decay[SPAN - 1 : SPAN, h : h + 1]
         faded = (key.astype(F32) * jnp.exp(last - column)).astype(BF16)
         update = lax.dot_general(faded, value, TN, preferred_element_type=F32).astype(BF16)
-        kv_out[SPAN + 32 * h : SPAN + 32 * (h + 1)] = jnp.concatenate(
-            [update[:32], update[32:]], axis=1
-        )
-    q_out[192:] = jnp.zeros((HEAD, SPAN), BF16)
-    q_out[:192] = jnp.transpose(proj_out[:, 576:768] * (HEAD ** (-0.5) * LOG2E)).astype(BF16)
-    both = proj_out[:, 768:896]
-    flipped = jnp.transpose(both)[HEAD:, :].astype(BF16)
-    kv_out[:128] = jnp.concatenate([both[:128, :HEAD], both[128:, :HEAD]], axis=1).astype(BF16)
-    kv_out[128:SPAN] = jnp.concatenate([flipped[:, :128], flipped[:, 128:]], axis=0)
+        state_out[32 * h : 32 * (h + 1)] = jnp.concatenate([update[:32], update[32:]], axis=1)
 
 
 def local_kernel(proj, cosine, sine, decay, decay_row, local_out, lifted_out):
@@ -80,9 +82,9 @@
     other = lax.broadcasted_iota(jnp.int32, (SPAN, SPAN), 1)
     causal = place >= other
     for h in range(3):
-        query = (turned(proj, h * HEAD, cos, sin) * HEAD ** (-0.5)).astype(BF16)
-        key = turned(proj, 192 + h * HEAD, cos, sin).astype(BF16)
-        value = proj[:, 384 + h * HEAD : 384 + (h + 1) * HEAD].astype(BF16)
+        query = (turned(proj, 320 + h * HEAD, cos, sin) * HEAD ** (-0.5)).astype(BF16)
+        key = turned(proj, 512 + h * HEAD, cos, sin).astype(BF16)
+        value = proj[:, 704 + h * HEAD : 704 + (h + 1) * HEAD].astype(BF16)
         column = decay[:, h : h + 1]
         scores = lax.dot_general(query, key, NT, preferred_element_type=F32)
         gap = jnp.where(causal, column - decay_row[h : h + 1, :], 0.0)
@@ -182,20 +184,36 @@
         out[z, 192:208] = jnp.concatenate(
             high + low + [jnp.zeros((10, SPAN), F32)], axis=0
         ).astype(BF16)
+
+    leaving = []
+    here = []
+    for h in range(3):
+        at = SPAN + 32 * h
+        left = jnp.zeros((32, 128), F32)
+        kept = jnp.zeros((32, 128), F32)
+        for side, held in enumerate((kv_own, kv_oth)):
+            for y in range(8):
+                state = held[y, at : at + 32].astype(F32)
+                place = (side * 8 + y) * 3 + h
+                left = left + state * fade[place]
+                kept = kept + state * fade[48 + place]
+        leaving.append(left)
+        here.append(kept)
+
+    def put(z, states):
+        states = jnp.concatenate(states, axis=0).astype(BF16)
+        out[z, 208:, :128] = states[:48]
+        out[z, 208:, 128:] = states[48:]
+
     for z in range(8):
-        sums = []
-        for h in range(3):
-            at = SPAN + 32 * h
-            state = jnp.zeros((32, 128), F32)
-            for side, held in enumerate((kv_own, kv_oth)):
-                for y in range(8):
-                    state = state + held[y, at : at + 32].astype(F32) * fade[
-                        ((z * 2 + side) * 8 + y) * 3 + h
-                    ]
-            sums.append(state)
-        sums = jnp.concatenate(sums, axis=0).astype(BF16)
-        out[z, 208:, :128] = sums[:48]
-        out[z, 208:, 128:] = sums[48:]
+        put(
+            z,
+            [
+                jnp.where(z > plan[67], leaving[h] * fade[96 + z * 3 + h], 0.0)
+                for h in range(3)
+            ],
+        )
+    put(plan[67], here)
 
 
 def back_kernel(parts, local, lifted, w_out, out, mixed):
@@ -235,16 +253,15 @@
     forget_total,
 ):
     z, y, c = (lax.axis_index("z"), lax.axis_index("y"), lax.axis_index("c"))
-    decay = jnp.cumsum(retain_log, axis=0)
-    ends = jnp.concatenate(three_parts(decay[-1]))
+    ends = jnp.concatenate(three_parts(jnp.sum(retain_log, axis=0)))
     shard = jnp.concatenate(
         [
+            w_query_att,
+            w_key_att,
+            w_value_att,
             w_query_ret,
             w_key_ret,
             w_value_ret,
-            w_query_att,
-            w_key_att,
-            w_value_att,
             w_out_ret.T,
             w_out_att.T,
             jnp.pad(ends[None, :], ((0, 15), (0, 119))),
@@ -272,6 +289,7 @@
     inverse = THETA ** (-jnp.arange(32, dtype=F32) / 32)
     angles = positions[:, None] * inverse[None, :]
     cosine, sine = (jnp.cos(angles), jnp.sin(angles))
+    decay = jnp.cumsum(retain_log, axis=0)
     decay_row = jnp.pad(decay.T, ((0, 5), (0, 0)))
     ends_own = copies_from(line_ends, "z")
     ends_oth = swapped_cores(ends_own)
@@ -307,14 +325,24 @@
         ],
         axis=2,
     )
-    blocks = key_z * 16 + spans * 2
-    blocks = jnp.stack([blocks + c, blocks + 1 - c])
+    first = z * 16 + spans * 2
+    blocks = jnp.stack([first + c, first + 1 - c])
     targets = spans * 16 + y * 2 + c
     index = jnp.arange(128, dtype=jnp.int32)
-    between = (index > blocks[None, :, :, None]) & (index < targets[:, None, None, None])
-    fade = jnp.sum(jnp.where(between[..., None], ends, 0.0), axis=3)
-    earlier = blocks[None] < targets[:, None, None]
-    fade = jnp.where(earlier[..., None], jnp.exp(fade), 0.0).reshape(384)
+    plane_end = z * 16 + 15
+
+    def faded(chosen, valid):
+        total = jnp.sum(jnp.where(chosen[..., None], ends, 0.0), axis=-2)
+        return jnp.where(valid[..., None], jnp.exp(total), 0.0).reshape(-1)
+
+    after = index > blocks[..., None]
+    fade = jnp.concatenate(
+        [
+            faded(after & (index <= plane_end), blocks >= 0),
+            faded(after & (index < here), blocks < here),
+            faded((index > plane_end) & (index < targets[:, None]), spans > z),
+        ]
+    )
     needed = (
         (key_z[None, :] < spans[:, None])
         | ((key_z[None, :] == spans[:, None]) & (spans[None, :] < y))
@@ -325,7 +353,7 @@
         jnp.where(needed[None, :] & (slot[None, :] == order[:, None]), order[None, :], 0), axis=1
     )
     own = jnp.stack([(z - y) % 8 * 8 + y])
-    plan = jnp.concatenate([own, units, jnp.stack([jnp.sum(needed.astype(jnp.int32)) + 1, c])])
+    plan = jnp.concatenate([own, units, jnp.stack([jnp.sum(needed.astype(jnp.int32)) + 1, c, z])])
 
     own_part, oth_part = pl.pallas_call(
         project_kernel,
@@ -336,21 +364,32 @@
         compiler_params=PARAMS,
         name="project",
     )(rows, w_own)
-    q_send, kv_send, proj = pl.pallas_call(
+    came_part = swapped_cores(oth_part)
+    attention_part = pl.BlockSpec((SPAN, 384), lambda i: (0, 0))
+    q_send, kv_send = pl.pallas_call(
+        share_kernel,
+        grid=(1,),
+        in_specs=[attention_part] * 2,
+        out_specs=[VMEM] * 2,
+        out_shape=[
+            jax.ShapeDtypeStruct((SPAN, SPAN), BF16),
+            jax.ShapeDtypeStruct((SPAN, 128), BF16),
+        ],
+        compiler_params=PARAMS,
+        name="share",
+    )(own_part, came_part)
+    queries = lax.all_gather(q_send, "z", axis=0)
+    kv_send = lax.ppermute(kv_send, ("z", "y"), ROTATION)
+    state_send, proj = pl.pallas_call(
         front_kernel,
         in_specs=[VMEM] * 5,
-        out_specs=[VMEM] * 3,
-        out_shape=[
-            jax.ShapeDtypeStruct((SPAN, SPAN), BF16),
-            jax.ShapeDtypeStruct((SPAN + 96, 128), BF16),
-            jax.ShapeDtypeStruct((SPAN, 896), F32),
-        ],
+        out_specs=[VMEM] * 2,
+        out_shape=[jax.ShapeDtypeStruct((96, 128), BF16), jax.ShapeDtypeStruct((SPAN, 896), F32)],
         compiler_params=PARAMS,
         name="front",
-    )(own_part, swapped_cores(oth_part), cosine, sine, decay)
-
-    queries = lax.all_gather(q_send, "z", axis=0)
-    kv_own = copies_from(lax.ppermute(kv_send, ("z", "y"), ROTATION), "y")
+    )(own_part, came_part, cosine, sine, decay)
+    kv_send = jnp.concatenate([kv_send, state_send], axis=0)
+    kv_own = copies_from(kv_send, "y")
     kv_oth = swapped_cores(kv_own)
     local, lifted = pl.pallas_call(
         local_kernel,
@@ -360,7 +399,7 @@
         compiler_params=PARAMS,
         name="local",
     )(proj, cosine, sine, decay, decay_row)
-    out_own = w_own[:, 896:]
+    out_own = w_own[:, 896:1280]
     out_oth = swapped_cores(out_own).reshape(64, 16, 384)
     out_own = out_own.reshape(64, 16, 384)
     w_out = jnp.where(

time: 242 us -> 242 us (level)
  the two profiles are of different devices: /device:TPU:2 before, /device:TPU:56 now
where the time goes in v8:
time: 242 us; the launch traced here: 241 us
  waiting for transfers between devices  103 us (43%)
  starting transfers between devices  42.3 us (17%)
  Pallas kernels  37.3 us (15%)
  blocking collectives  15.4 us (6%)
  local copies, waits for them, and re-layouts  15.3 us (6%)
  between operations  14.5 us (6%)
  other arithmetic  13.3 us (5%)
    all_gather x1, waiting for transfers between devices, body(): w_own = lax.all_gather(w_row, 'z', axis=0, tiled=True)  35.3 us
    all_to_all x4, waiting for transfers between devices, copies_from(): return lax.all_to_all(copies, axis, split_axis=0, concat_axis=0, tiled=True)  27.3 us
    all_to_all x4, starting transfers between devices, copies_from(): return lax.all_to_all(copies, axis, split_axis=0, concat_axis=0, tiled=True)  24.5 us
    all_gather x1, waiting for transfers between devices, body(): queries = lax.all_gather(q_send, 'z', axis=0)  22.8 us
    pallas_call x1, Pallas kernels, body(): pl.pallas_call(attend_kernel, in_specs=[SMEM] * 2 + [VMEM] * 5, out_specs...  18.3 us
    all_to_all x1, blocking collectives, body(): shares = lax.all_to_all(share.reshape(4, 64, 2048), 'tp', 0, 0, tiled=True)  15.4 us
    all_to_all x1, waiting for transfers between devices, body(): parts = lax.all_to_all(partial, 'z', 0, 0, tiled=True)  13.8 us
    ppermute x5, starting transfers between devices, swapped_cores(): return lax.ppermute(value, 'c', [(0, 1), (1, 0)])  9.75 us
  transfers between devices with their start and end apart: 13, of which 9 were waited for; matrix products, arithmetic and copies ran while one was open for 8% of the time, Pallas kernels for 3%

profile of v8, /device:TPU:56, one launch (start us, length us, event | category | flops | bytes accessed | tf_op | source)
XLA Modules:
  0.0 241.3 jit_solution(17613014554603177341)
XLA Ops:
  9.1 8.5 %all-to-all-start = ((bf16[8,16,1408]{2,1,0:T(8,128)(2,1)}), bf16[8,16,1408]{2,1,0:T(8,128)(2,1)S(1)}, u32[]{:S(2)}, u32[]{:S(2)}) async-start(bf16[8,16,1408]{2,1,0:T(8,128)(2,1)} %broadcast_in_dim.158), calls=%async_computation | async-start | bytes 720896 | tf_op jit(solution)/shard_map/all_to_all | solution.py:27
  19.7 6.9 %all-to-all-done = bf16[8,16,1408]{2,1,0:T(8,128)(2,1)S(1)} async-done(((bf16[8,16,1408]{2,1,0:T(8,128)(2,1)}), bf16[8,16,1408]{2,1,0:T(8,128)(2,1)S(1)}, u32[]{:S(2)}, u32[]{:S(2)}) %all-to-all-start) | async-done | bytes 360480 | tf_op jit(solution)/shard_map/all_to_all | solution.py:27
  27.7 3.6 %all-to-all-start.2 = ((bf16[4,2,64,1024]{3,2,1,0:T(8,128)(2,1)}), bf16[4,2,64,1024]{3,2,1,0:T(8,128)(2,1)S(1)}, u32[]{:S(2)}, u32[]{:S(2)}) async-start(bf16[4,2,64,1024]{3,2,1,0:T(8,128)(2,1)} %broadcast_in_dim.170), calls=%async_computation.2 | async-start | bytes 2097152 | tf_op jit(solution)/shard_map/all_to_all | solution.py:27
  35.7 7.5 %all-to-all-done.2 = bf16[4,2,64,1024]{3,2,1,0:T(8,128)(2,1)S(1)} async-done(((bf16[4,2,64,1024]{3,2,1,0:T(8,128)(2,1)}), bf16[4,2,64,1024]{3,2,1,0:T(8,128)(2,1)S(1)}, u32[]{:S(2)}, u32[]{:S(2)}) %all-to-all-start.2) | async-done | bytes 1048608 | tf_op jit(solution)/shard_map/all_to_all | solution.py:27
  43.2 1.9 collective-permute-start.1
  48.1 35.3 %all-gather.4.cloned.1.call-done.weights = bf16[1024,1280]{1,0:T(8,128)(2,1)} async-done(((bf16[128,1280]{1,0:T(8,128)(2,1)}), bf16[1024,1280]{1,0:T(8,128)(2,1)}) %all-gather.4.cloned.1.call-update) | async-done | bytes 2621456 | tf_op jit(solution)/shard_map/all_gather | solution.py:274
  83.4 4.2 %project.1 = (f32[256,896]{1,0:T(8,128)}, f32[256,896]{1,0:T(8,128)}) custom-call(bf16[512,1024]{1,0:T(8,128)(2,1)} %pad_maximum_fusion.rows, bf16[1024,1280]{1,0:T(8,128)(2,1)} %all-gather.4.cloned.1.call-done.weights), custom_call_target="tpu_custom_call" | custom-call | tf_op jit(solution)/shard_map/project/pallas_call | solution.py:358
  93.7 2.0 share.1
  95.7 3.9 %collective-permute-start.3 = (bf16[256,128]{1,0:T(8,128)(2,1)}, bf16[256,128]{1,0:T(8,128)(2,1)S(1)}, u32[]{:S(2)}, u32[]{:S(2)}) collective-permute-start(bf16[256,128]{1,0:T(8,128)(2,1)} %get-tuple-element.16), channel_id=1, source_target_pairs={{0,0},{8,72},{16,144},{24,216},{32,288},{40,360},{48,432},{56,504}... | collective-permute-start | bytes 196616 | tf_op jit(solution)/shard_map/ppermute | solution.py:382
  100.3 4.5 %all-to-all-start.1 = ((f32[8,8,3]{1,2,0:T(4,128)}), f32[8,8,3]{1,2,0:T(4,128)S(1)}, u32[]{:S(2)}, u32[]{:S(2)}) async-start(f32[8,8,3]{1,2,0:T(4,128)} %broadcast_in_dim.159), calls=%async_computation.1 | async-start | bytes 32768 | tf_op jit(solution)/shard_map/all_to_all | solution.py:27
  104.8 3.7 %front.1 = (bf16[96,128]{1,0:T(8,128)(2,1)}, f32[256,896]{1,0:T(8,128)}) custom-call(f32[256,896]{1,0:T(8,128)} %get-tuple-element.13.first_part, f32[256,896]{1,0:T(8,128)} %copy-done.1, f32[256,32]{1,0:T(8,128)} %get-tuple-element.35.cosine, f32[256,32]{1,0:T(8,128)} %get-tuple-element.34.sine, f32[256,3]{1,0:T(8,128)} %copy.156.decay), custom_call_target="tpu_custom_call" | custom-call | tf_op jit(solution)/shard_map/front/pallas_call | solution.py:383
  109.3 3.3 %all-to-all-done.1 = f32[8,8,3]{1,2,0:T(4,128)S(1)} async-done(((f32[8,8,3]{1,2,0:T(4,128)}), f32[8,8,3]{1,2,0:T(4,128)S(1)}, u32[]{:S(2)}, u32[]{:S(2)}) %all-to-all-start.1) | async-done | bytes 800 | tf_op jit(solution)/shard_map/all_to_all | solution.py:27
  113.5 7.9 %all-to-all-start.3 = ((bf16[8,352,128]{2,1,0:T(8,128)(2,1)}), bf16[8,352,128]{2,1,0:T(8,128)(2,1)S(1)}, u32[]{:S(2)}, u32[]{:S(2)}) async-start(bf16[8,352,128]{2,1,0:T(8,128)(2,1)} %broadcast_in_dim.173), calls=%async_computation.3 | async-start | bytes 1441792 | tf_op jit(solution)/shard_map/all_to_all | solution.py:27
  124.7 1.9 collective-permute-start
  128.5 9.6 %all-to-all-done.3.kv_own = bf16[8,352,128]{2,1,0:T(8,128)(2,1)S(1)} async-done(((bf16[8,352,128]{2,1,0:T(8,128)(2,1)}), bf16[8,352,128]{2,1,0:T(8,128)(2,1)S(1)}, u32[]{:S(2)}, u32[]{:S(2)}) %all-to-all-start.3) | async-done | bytes 720928 | tf_op jit(solution)/shard_map/all_to_all | solution.py:27
  138.1 1.9 collective-permute-start.4
  141.3 22.8 %all-gather.6.cloned.1.call-done = bf16[2048,256]{1,0:T(8,128)(2,1)} async-done(((bf16[256,256]{1,0:T(8,128)(2,1)}), bf16[2048,256]{1,0:T(8,128)(2,1)}) %all-gather.6.cloned.1.call-update) | async-done | bytes 1048592 | tf_op jit(solution)/shard_map/all_gather | solution.py:381
  165.0 18.3 %attend.1 = bf16[8,256,256]{2,1,0:T(8,128)(2,1)} custom-call(s32[68]{0:T(128)} %concatenate.32.plan, f32[120]{0:T(128)} %pad_maximum_fusion.3.fade, bf16[8,256,256]{2,1,0:T(8,128)(2,1)} %bitcast.70, bf16[8,3,64,256]{3,2,1,0:T(8,128)(2,1)} %maximum_maximum_fusion.query_gate, bf16[8,352,128]{2,1,0:T(8,128)(2,1)} %copy-done.2, bf16[8,352,128]{2,1,0:T(8,128)(2,1)} %copy-done.3, ...), custom_call_target="tpu_custom_call" | custom-call | tf_op jit(solution)/shard_map/attend/pallas_call | solution.py:409
  183.3 4.1 %all-to-all-start.4 = ((bf16[8,256,256]{2,1,0:T(8,128)(2,1)}), bf16[8,256,256]{2,1,0:T(8,128)(2,1)S(1)}, u32[]{:S(2)}, u32[]{:S(2)}) async-start(bf16[8,256,256]{2,1,0:T(8,128)(2,1)} %attend.1), calls=%async_computation.4 | async-start | bytes 2097152 | tf_op jit(solution)/shard_map/all_to_all | solution.py:425
  188.7 2.1 collective-permute-start.5
  194.2 4.1 %local.1 = (f32[256,192]{1,0:T(8,128)}, bf16[256,192]{1,0:T(8,128)(2,1)}) custom-call(f32[256,896]{1,0:T(8,128)} %get-tuple-element.18.proj, f32[256,32]{1,0:T(8,128)} %get-tuple-element.35.cosine, f32[256,32]{1,0:T(8,128)} %get-tuple-element.34.sine, f32[256,3]{1,0:T(8,128)} %copy.156.decay, f32[8,256]{1,0:T(8,128)} %pad.9.decay_row), custom_call_target="tpu_custom_call" | custom-call | tf_op jit(solution)/shard_map/local/pallas_call | solution.py:394
  198.3 13.8 %all-to-all-done.4.parts = bf16[8,256,256]{2,1,0:T(8,128)(2,1)S(1)} async-done(((bf16[8,256,256]{2,1,0:T(8,128)(2,1)}), bf16[8,256,256]{2,1,0:T(8,128)(2,1)S(1)}, u32[]{:S(2)}, u32[]{:S(2)}) %all-to-all-start.4) | async-done | bytes 1048608 | tf_op jit(solution)/shard_map/all_to_all | solution.py:425
  213.1 5.0 %back.1 = bf16[256,2048]{1,0:T(8,128)(2,1)} custom-call(bf16[8,256,256]{2,1,0:T(8,128)(2,1)} %copy-done, f32[256,192]{1,0:T(8,128)} %get-tuple-element.19.local, bf16[256,192]{1,0:T(8,128)(2,1)} %get-tuple-element.20.lifted, bf16[2048,384]{1,0:T(8,128)(2,1)} %bitcast.63), custom_call_target="tpu_custom_call" | custom-call | tf_op jit(solution)/shard_map/back/pallas_call | solution.py:427
  218.1 15.4 %all_to_all.30 = bf16[4,64,2048]{2,1,0:T(8,128)(2,1)S(1)} all-to-all(bf16[4,64,2048]{2,1,0:T(8,128)(2,1)} %bitcast.64), channel_id=1, replica_groups=mesh['z'=8,'y'=8,'c'=2,'tp'=4] {'tp'}, dimensions={0} | all-to-all | bytes 2097152 | tf_op jit(solution)/shard_map/all_to_all | solution.py:436
  (126 shorter events, 34.5 us)
Async XLA Ops:
  6.5 12.6 %copy-start.6 = (f32[2048]{0:T(1024)S(1)}, f32[2048]{0:T(1024)}, u32[]{:S(2)}) copy-start(f32[2048]{0:T(1024)} %param.13) | copy-start | bytes 24580
  9.1 17.5 %all-to-all-start = ((bf16[8,16,1408]{2,1,0:T(8,128)(2,1)}), bf16[8,16,1408]{2,1,0:T(8,128)(2,1)S(1)}, u32[]{:S(2)}, u32[]{:S(2)}) async-start(bf16[8,16,1408]{2,1,0:T(8,128)(2,1)} %broadcast_in_dim.158), calls=%async_computation | async-start | bytes 720896 | tf_op jit(solution)/shard_map/all_to_all | solution.py:27
  27.7 4.5 %copy-start.4 = (f32[3,32768]{1,0:T(4,128)S(1)}, f32[3,32768]{1,0:T(4,128)}, u32[]{:S(2)}) copy-start(f32[3,32768]{1,0:T(4,128)} %param.23) | copy-start | bytes 1179652
  27.7 4.6 %copy-start.5 = (f32[256,3]{0,1:T(4,128)S(1)}, f32[256,3]{0,1:T(4,128)}, u32[]{:S(2)}) copy-start(f32[256,3]{0,1:T(4,128)} %param.22) | copy-start | bytes 9220
  27.7 15.4 %all-to-all-start.2 = ((bf16[4,2,64,1024]{3,2,1,0:T(8,128)(2,1)}), bf16[4,2,64,1024]{3,2,1,0:T(8,128)(2,1)S(1)}, u32[]{:S(2)}, u32[]{:S(2)}) async-start(bf16[4,2,64,1024]{3,2,1,0:T(8,128)(2,1)} %broadcast_in_dim.170), calls=%async_computation.2 | async-start | bytes 2097152 | tf_op jit(solution)/shard_map/all_to_all | solution.py:27
  31.4 52.0 %all-gather.4.cloned.1.call-start = ((), (), s32[]{:S(2)}) async-start(), calls=%async_computation.6 | async-start | bytes 2949120 | tf_op jit(solution)/shard_map/all_gather | solution.py:274
  43.2 3.8 %collective-permute-start.1 = (bf16[256,1024]{1,0:T(8,128)(2,1)S(1)}, bf16[256,1024]{1,0:T(8,128)(2,1)S(1)}, u32[]{:S(2)}, u32[]{:S(2)}) collective-permute-start(bf16[256,1024]{1,0:T(8,128)(2,1)S(1)} %bitcast.72), channel_id=1, source_target_pairs={{0,4},{4,0},{1,5},{5,1},{2,6},{6,2},{3,7},{7,3},{8,12},{12,8},{9,1... | collective-permute-start | bytes 1572872 | tf_op jit(solution)/shard_map/ppermute | solution.py:31
  87.6 5.1 %collective-permute-start.2 = (f32[256,896]{1,0:T(8,128)}, f32[256,896]{1,0:T(8,128)S(1)}, u32[]{:S(2)}, u32[]{:S(2)}) collective-permute-start(f32[256,896]{1,0:T(8,128)} %get-tuple-element.14), channel_id=1, source_target_pairs={{0,4},{4,0},{1,5},{5,1},{2,6},{6,2},{3,7},{7,3},{8,12},{12,8},{9,1... | collective-permute-start | bytes 2752520 | tf_op jit(solution)/shard_map/ppermute | solution.py:31
  92.8 1.0 copy-start.1
  95.7 12.8 %collective-permute-start.3 = (bf16[256,128]{1,0:T(8,128)(2,1)}, bf16[256,128]{1,0:T(8,128)(2,1)S(1)}, u32[]{:S(2)}, u32[]{:S(2)}) collective-permute-start(bf16[256,128]{1,0:T(8,128)(2,1)} %get-tuple-element.16), channel_id=1, source_target_pairs={{0,0},{8,72},{16,144},{24,216},{32,288},{40,360},{48,432},{56,504}... | collective-permute-start | bytes 196616 | tf_op jit(solution)/shard_map/ppermute | solution.py:382
  100.3 12.2 %all-to-all-start.1 = ((f32[8,8,3]{1,2,0:T(4,128)}), f32[8,8,3]{1,2,0:T(4,128)S(1)}, u32[]{:S(2)}, u32[]{:S(2)}) async-start(f32[8,8,3]{1,2,0:T(4,128)} %broadcast_in_dim.159), calls=%async_computation.1 | async-start | bytes 32768 | tf_op jit(solution)/shard_map/all_to_all | solution.py:27
  113.5 24.5 %all-to-all-start.3 = ((bf16[8,352,128]{2,1,0:T(8,128)(2,1)}), bf16[8,352,128]{2,1,0:T(8,128)(2,1)S(1)}, u32[]{:S(2)}, u32[]{:S(2)}) async-start(bf16[8,352,128]{2,1,0:T(8,128)(2,1)} %broadcast_in_dim.173), calls=%async_computation.3 | async-start | bytes 1441792 | tf_op jit(solution)/shard_map/all_to_all | solution.py:27
  121.4 42.7 %all-gather.6.cloned.1.call-start = ((), (), s32[]{:S(2)}) async-start(), calls=%async_computation.7 | async-start | bytes 1179648 | tf_op jit(solution)/shard_map/all_gather | solution.py:381
  124.7 3.3 %collective-permute-start = (f32[8,8,3]{1,2,0:T(4,128)S(1)}, f32[8,8,3]{1,2,0:T(4,128)S(1)}, u32[]{:S(2)}, u32[]{:S(2)}) collective-permute-start(f32[8,8,3]{1,2,0:T(4,128)S(1)} %all-to-all-done.1), channel_id=1, source_target_pairs={{0,4},{4,0},{1,5},{5,1},{2,6},{6,2},{3,7},{7,3},{8,12},{12,8},{9,1... | collective-permute-start | bytes 2312 | tf_op jit(solution)/shard_map/ppermute | solution.py:31
  138.1 26.1 %copy-start.2 = (bf16[8,352,128]{2,1,0:T(8,128)(2,1)}, bf16[8,352,128]{2,1,0:T(8,128)(2,1)S(1)}, u32[]{:S(2)}) copy-start(bf16[8,352,128]{2,1,0:T(8,128)(2,1)S(1)} %all-to-all-done.3.kv_own) | copy-start | bytes 2162692
  138.1 26.0 %collective-permute-start.4 = (bf16[8,352,128]{2,1,0:T(8,128)(2,1)S(1)}, bf16[8,352,128]{2,1,0:T(8,128)(2,1)S(1)}, u32[]{:S(2)}, u32[]{:S(2)}) collective-permute-start(bf16[8,352,128]{2,1,0:T(8,128)(2,1)S(1)} %all-to-all-done.3.kv_own), channel_id=1, source_target_pairs={{0,4},{4,0},{1,5},{5,1},{2,6},{6,2},{3,7},{7,3},{8,12},{12,8},{9,1... | collective-permute-start | bytes 2162696 | tf_op jit(solution)/shard_map/ppermute | solution.py:31
  164.1 0.9 copy-start.3
  183.3 28.8 %all-to-all-start.4 = ((bf16[8,256,256]{2,1,0:T(8,128)(2,1)}), bf16[8,256,256]{2,1,0:T(8,128)(2,1)S(1)}, u32[]{:S(2)}, u32[]{:S(2)}) async-start(bf16[8,256,256]{2,1,0:T(8,128)(2,1)} %attend.1), calls=%async_computation.4 | async-start | bytes 2097152 | tf_op jit(solution)/shard_map/all_to_all | solution.py:425
  188.7 4.2 %collective-permute-start.5 = (bf16[1024,384]{1,0:T(8,128)(2,1)S(1)}, bf16[1024,384]{1,0:T(8,128)(2,1)S(1)}, u32[]{:S(2)}, u32[]{:S(2)}) collective-permute-start(bf16[1024,384]{1,0:T(8,128)(2,1)S(1)} %slice.35), channel_id=1, source_target_pairs={{0,4},{4,0},{1,5},{5,1},{2,6},{6,2},{3,7},{7,3},{8,12},{12,8},{9,1... | collective-permute-start | bytes 2359304 | tf_op jit(solution)/shard_map/ppermute | solution.py:31
  212.1 1.0 copy-start
Sparse Core Ops, SparseCore 0:
  34.3 49.0 all-gather.3
  124.3 39.7 all-gather.5

commit v9 on v8

--- a/solution.py
+++ b/solution.py
@@ -14,7 +14,7 @@
 LOG2E = 1.4426950408889634
 F32 = jnp.float32
 BF16 = jnp.bfloat16
-ROTATION = [(z * 8 + y, ((z + y) % 8) * 8 + y) for z in range(8) for y in range(8)]
+MIRROR = [(z * 8 + y, (7 - z if y % 2 else z) * 8 + y) for z in range(8) for y in range(8)]
 NT = (((1,), (1,)), ((), ()))
 TN = (((0,), (0,)), ((), ()))
 VMEM = pl.BlockSpec(memory_space=pltpu.VMEM)
@@ -73,6 +73,12 @@
         faded = (key.astype(F32) * jnp.exp(last - column)).astype(BF16)
         update = lax.dot_general(faded, value, TN, preferred_element_type=F32).astype(BF16)
         state_out[32 * h : 32 * (h + 1)] = jnp.concatenate([update[:32], update[32:]], axis=1)
+
+
+def spread_kernel(pairs, states, out):
+    for y in range(8):
+        out[y, :SPAN] = pairs[...]
+        out[y, SPAN:] = states[...]
 
 
 def local_kernel(proj, cosine, sine, decay, decay_row, local_out, lifted_out):
@@ -217,22 +223,25 @@
 
 
 def back_kernel(parts, local, lifted, w_out, out, mixed):
-    total = parts[0].astype(F32)
-    for z in range(1, 8):
-        total = total + parts[z].astype(F32)
-    states = jnp.concatenate([total[208:, :128], total[208:, 128:]], axis=0)
-    for h in range(3):
-        held = states[32 * h : 32 * (h + 1)]
-        held = jnp.concatenate([held[:, :HEAD], held[:, HEAD:]], axis=0).astype(BF16)
-        raw = local[:, h * HEAD : (h + 1) * HEAD] + jnp.dot(
-            lifted[:, h * HEAD : (h + 1) * HEAD], held, preferred_element_type=F32
-        )
-        centred = raw - jnp.mean(raw, axis=-1, keepdims=True)
-        spread = jnp.mean(centred * centred, axis=-1, keepdims=True)
-        mixed[:, h * HEAD : (h + 1) * HEAD] = (centred * lax.rsqrt(spread + EPS)).astype(BF16)
-        weight = total[192 + h : 193 + h] + total[195 + h : 196 + h]
-        attended = total[h * HEAD : (h + 1) * HEAD] / weight
-        mixed[:, 192 + h * HEAD : 192 + (h + 1) * HEAD] = jnp.transpose(attended).astype(BF16)
+    @pl.when(pl.program_id(0) == 0)
+    def _():
+        total = parts[0].astype(F32)
+        for z in range(1, 8):
+            total = total + parts[z].astype(F32)
+        states = jnp.concatenate([total[208:, :128], total[208:, 128:]], axis=0)
+        for h in range(3):
+            held = states[32 * h : 32 * (h + 1)]
+            held = jnp.concatenate([held[:, :HEAD], held[:, HEAD:]], axis=0).astype(BF16)
+            raw = local[:, h * HEAD : (h + 1) * HEAD] + jnp.dot(
+                lifted[:, h * HEAD : (h + 1) * HEAD], held, preferred_element_type=F32
+            )
+            centred = raw - jnp.mean(raw, axis=-1, keepdims=True)
+            spread = jnp.mean(centred * centred, axis=-1, keepdims=True)
+            mixed[:, h * HEAD : (h + 1) * HEAD] = (centred * lax.rsqrt(spread + EPS)).astype(BF16)
+            weight = total[192 + h : 193 + h] + total[195 + h : 196 + h]
+            attended = total[h * HEAD : (h + 1) * HEAD] / weight
+            mixed[:, 192 + h * HEAD : 192 + (h + 1) * HEAD] = jnp.transpose(attended).astype(BF16)
+
     out[...] = lax.dot_general(
         mixed[...], w_out[...], NT, preferred_element_type=F32
     ).astype(BF16)
@@ -301,7 +310,7 @@
 
     gate = (forget_total * LOG2E).reshape(3, 8, 8, 2, SPAN)
     spans = jnp.arange(8, dtype=jnp.int32)
-    key_z = (z - spans) % 8
+    key_z = jnp.where(spans % 2 == 0, z, 7 - z)
     chosen = (spans[:, None] == key_z[None, :])[None, :, :, None, None]
     key_side = jnp.sum(jnp.where(chosen, gate, 0.0), axis=1)
     key_side = jnp.where(c == 0, key_side, key_side[:, :, ::-1])
@@ -352,7 +361,7 @@
     units = jnp.sum(
         jnp.where(needed[None, :] & (slot[None, :] == order[:, None]), order[None, :], 0), axis=1
     )
-    own = jnp.stack([(z - y) % 8 * 8 + y])
+    own = jnp.stack([jnp.where(y % 2 == 0, z, 7 - z) * 8 + y])
     plan = jnp.concatenate([own, units, jnp.stack([jnp.sum(needed.astype(jnp.int32)) + 1, c, z])])
 
     own_part, oth_part = pl.pallas_call(
@@ -379,7 +388,7 @@
         name="share",
     )(own_part, came_part)
     queries = lax.all_gather(q_send, "z", axis=0)
-    kv_send = lax.ppermute(kv_send, ("z", "y"), ROTATION)
+    kv_send = lax.ppermute(kv_send, ("z", "y"), MIRROR)
     state_send, proj = pl.pallas_call(
         front_kernel,
         in_specs=[VMEM] * 5,
@@ -388,8 +397,15 @@
         compiler_params=PARAMS,
         name="front",
     )(own_part, came_part, cosine, sine, decay)
-    kv_send = jnp.concatenate([kv_send, state_send], axis=0)
-    kv_own = copies_from(kv_send, "y")
+    kv_send = pl.pallas_call(
+        spread_kernel,
+        in_specs=[VMEM] * 2,
+        out_specs=VMEM,
+        out_shape=jax.ShapeDtypeStruct((8, SPAN + 96, 128), BF16),
+        compiler_params=PARAMS,
+        name="spread",
+    )(kv_send, state_send)
+    kv_own = lax.all_to_all(kv_send, "y", 0, 0, tiled=True)
     kv_oth = swapped_cores(kv_own)
     local, lifted = pl.pallas_call(
         local_kernel,
@@ -426,8 +442,9 @@
 
     share = pl.pallas_call(
         back_kernel,
-        in_specs=[VMEM] * 4,
-        out_specs=VMEM,
+        grid=(2,),
+        in_specs=[VMEM] * 3 + [pl.BlockSpec((1024, 384), lambda i: (i, 0))],
+        out_specs=pl.BlockSpec((SPAN, 1024), lambda i: (0, i)),
         out_shape=jax.ShapeDtypeStruct((SPAN, 2048), BF16),
         scratch_shapes=[pltpu.VMEM((SPAN, 384), BF16)],
         compiler_params=PARAMS,

time: 242 us -> 241 us (level)
    all_to_all x4 -> x3, waiting for transfers between devices: 27.3 us -> 15.5 us  [copies_from(): return lax.all_to_all(copies, axis, split_axis=0, concat_axis=0, tiled=True)]
    all_to_all x0 -> x1, waiting for transfers between devices: none -> 10.4 us  [body(): kv_own = lax.all_to_all(kv_send, 'y', 0, 0, tiled=True)]
    all_to_all x4 -> x3, starting transfers between devices: 24.5 us -> 16.4 us  [copies_from(): return lax.all_to_all(copies, axis, split_axis=0, concat_axis=0, tiled=True)]
    all_to_all x0 -> x1, starting transfers between devices: none -> 6.26 us  [body(): kv_own = lax.all_to_all(kv_send, 'y', 0, 0, tiled=True)]
    pallas_call x1 -> x2, Pallas kernels: 5.02 us -> 6.28 us  [the longest x1 4.48 us: body(): pl.pallas_call(back_kernel, grid=(2,), in_specs=[VMEM] * 3 + [pl.BlockSpe...]
  transfers between devices with their start and end apart: 13 -> 13, of which waited for: 9 -> 8; matrix products, arithmetic and copies ran while one was open for 8% -> 8% of each run, Pallas kernels for 3% -> 5%
where the time goes in v9:
time: 241 us; the launch traced here: 240 us
  waiting for transfers between devices  103 us (43%)
  starting transfers between devices  41.7 us (17%)
  Pallas kernels  38.6 us (16%)
  blocking collectives  15.4 us (6%)
  local copies, waits for them, and re-layouts  15 us (6%)
  between operations  14.4 us (6%)
  other arithmetic  12.4 us (5%)
    all_gather x1, waiting for transfers between devices, body(): w_own = lax.all_gather(w_row, 'z', axis=0, tiled=True)  35.3 us
    all_gather x1, waiting for transfers between devices, body(): queries = lax.all_gather(q_send, 'z', axis=0)  23.8 us
    pallas_call x1, Pallas kernels, body(): pl.pallas_call(attend_kernel, in_specs=[SMEM] * 2 + [VMEM] * 5, out_specs...  18.3 us
    all_to_all x3, starting transfers between devices, copies_from(): return lax.all_to_all(copies, axis, split_axis=0, concat_axis=0, tiled=True)  16.4 us
    all_to_all x3, waiting for transfers between devices, copies_from(): return lax.all_to_all(copies, axis, split_axis=0, concat_axis=0, tiled=True)  15.5 us
    all_to_all x1, blocking collectives, body(): shares = lax.all_to_all(share.reshape(4, 64, 2048), 'tp', 0, 0, tiled=True)  15.4 us
    all_to_all x1, waiting for transfers between devices, body(): parts = lax.all_to_all(partial, 'z', 0, 0, tiled=True)  13.8 us
    all_to_all x1, waiting for transfers between devices, body(): kv_own = lax.all_to_all(kv_send, 'y', 0, 0, tiled=True)  10.4 us
  transfers between devices with their start and end apart: 13, of which 8 were waited for; matrix products, arithmetic and copies ran while one was open for 8% of the time, Pallas kernels for 5%

profile of v9, /device:TPU:56, one launch (start us, length us, event | category | flops | bytes accessed | tf_op | source)
XLA Modules:
  0.0 240.3 jit_solution(1760206465341829376)
XLA Ops:
  9.1 8.5 %all-to-all-start = ((bf16[8,16,1408]{2,1,0:T(8,128)(2,1)}), bf16[8,16,1408]{2,1,0:T(8,128)(2,1)S(1)}, u32[]{:S(2)}, u32[]{:S(2)}) async-start(bf16[8,16,1408]{2,1,0:T(8,128)(2,1)} %broadcast_in_dim.165), calls=%async_computation | async-start | bytes 720896 | tf_op jit(solution)/shard_map/all_to_all | solution.py:27
  19.8 6.9 %all-to-all-done = bf16[8,16,1408]{2,1,0:T(8,128)(2,1)S(1)} async-done(((bf16[8,16,1408]{2,1,0:T(8,128)(2,1)}), bf16[8,16,1408]{2,1,0:T(8,128)(2,1)S(1)}, u32[]{:S(2)}, u32[]{:S(2)}) %all-to-all-start) | async-done | bytes 360480 | tf_op jit(solution)/shard_map/all_to_all | solution.py:27
  27.8 3.6 %all-to-all-start.2 = ((bf16[4,2,64,1024]{3,2,1,0:T(8,128)(2,1)}), bf16[4,2,64,1024]{3,2,1,0:T(8,128)(2,1)S(1)}, u32[]{:S(2)}, u32[]{:S(2)}) async-start(bf16[4,2,64,1024]{3,2,1,0:T(8,128)(2,1)} %broadcast_in_dim.177), calls=%async_computation.2 | async-start | bytes 2097152 | tf_op jit(solution)/shard_map/all_to_all | solution.py:27
  34.5 8.7 %all-to-all-done.2 = bf16[4,2,64,1024]{3,2,1,0:T(8,128)(2,1)S(1)} async-done(((bf16[4,2,64,1024]{3,2,1,0:T(8,128)(2,1)}), bf16[4,2,64,1024]{3,2,1,0:T(8,128)(2,1)S(1)}, u32[]{:S(2)}, u32[]{:S(2)}) %all-to-all-start.2) | async-done | bytes 1048608 | tf_op jit(solution)/shard_map/all_to_all | solution.py:27
  43.3 1.9 collective-permute-start.1
  48.1 35.3 %all-gather.4.cloned.1.call-done.weights = bf16[1024,1280]{1,0:T(8,128)(2,1)} async-done(((bf16[128,1280]{1,0:T(8,128)(2,1)}), bf16[1024,1280]{1,0:T(8,128)(2,1)}) %all-gather.4.cloned.1.call-update) | async-done | bytes 2621456 | tf_op jit(solution)/shard_map/all_gather | solution.py:283
  83.4 4.2 %project.1 = (f32[256,896]{1,0:T(8,128)}, f32[256,896]{1,0:T(8,128)}) custom-call(bf16[512,1024]{1,0:T(8,128)(2,1)} %pad_maximum_fusion.rows, bf16[1024,1280]{1,0:T(8,128)(2,1)} %all-gather.4.cloned.1.call-done.weights), custom_call_target="tpu_custom_call" | custom-call | tf_op jit(solution)/shard_map/project/pallas_call | solution.py:367
  87.6 1.9 collective-permute-start.2
  93.0 4.3 %all-to-all-start.1 = ((f32[8,8,3]{1,2,0:T(4,128)}), f32[8,8,3]{1,2,0:T(4,128)S(1)}, u32[]{:S(2)}, u32[]{:S(2)}) async-start(f32[8,8,3]{1,2,0:T(4,128)} %broadcast_in_dim.166), calls=%async_computation.1 | async-start | bytes 32768 | tf_op jit(solution)/shard_map/all_to_all | solution.py:27
  98.2 2.0 share.1
  100.2 5.1 %collective-permute-start.3 = (bf16[256,128]{1,0:T(8,128)(2,1)}, bf16[256,128]{1,0:T(8,128)(2,1)S(1)}, u32[]{:S(2)}, u32[]{:S(2)}) collective-permute-start(bf16[256,128]{1,0:T(8,128)(2,1)} %get-tuple-element.16), channel_id=1, source_target_pairs={{0,0},{8,456},{16,16},{24,472},{32,32},{40,488},{48,48},{56,504},{... | collective-permute-start | bytes 196616 | tf_op jit(solution)/shard_map/ppermute | solution.py:391
  106.8 3.7 %front.1 = (bf16[96,128]{1,0:T(8,128)(2,1)}, f32[256,896]{1,0:T(8,128)}) custom-call(f32[256,896]{1,0:T(8,128)} %get-tuple-element.13.first_part, f32[256,896]{1,0:T(8,128)} %copy-done.1, f32[256,32]{1,0:T(8,128)} %get-tuple-element.35.cosine, f32[256,32]{1,0:T(8,128)} %get-tuple-element.34.sine, f32[256,3]{1,0:T(8,128)} %copy.156.decay), custom_call_target="tpu_custom_call" | custom-call | tf_op jit(solution)/shard_map/front/pallas_call | solution.py:392
  113.0 6.3 %all-to-all-start.3 = ((bf16[8,352,128]{2,1,0:T(8,128)(2,1)}), bf16[8,352,128]{2,1,0:T(8,128)(2,1)S(1)}, u32[]{:S(2)}, u32[]{:S(2)}) async-start(bf16[8,352,128]{2,1,0:T(8,128)(2,1)} %spread.1), calls=%async_computation.3 | async-start | bytes 1441792 | tf_op jit(solution)/shard_map/all_to_all | solution.py:408
  122.6 1.9 collective-permute-start
  126.2 10.4 %all-to-all-done.3.kv_own = bf16[8,352,128]{2,1,0:T(8,128)(2,1)S(1)} async-done(((bf16[8,352,128]{2,1,0:T(8,128)(2,1)}), bf16[8,352,128]{2,1,0:T(8,128)(2,1)S(1)}, u32[]{:S(2)}, u32[]{:S(2)}) %all-to-all-start.3) | async-done | bytes 720928 | tf_op jit(solution)/shard_map/all_to_all | solution.py:408
  136.6 1.9 collective-permute-start.4
  139.9 23.8 %all-gather.6.cloned.1.call-done = bf16[2048,256]{1,0:T(8,128)(2,1)} async-done(((bf16[256,256]{1,0:T(8,128)(2,1)}), bf16[2048,256]{1,0:T(8,128)(2,1)}) %all-gather.6.cloned.1.call-update) | async-done | bytes 1048592 | tf_op jit(solution)/shard_map/all_gather | solution.py:390
  164.7 18.3 %attend.1 = bf16[8,256,256]{2,1,0:T(8,128)(2,1)} custom-call(s32[68]{0:T(128)} %concatenate.29.plan, f32[120]{0:T(128)} %pad_maximum_fusion.2.fade, bf16[8,256,256]{2,1,0:T(8,128)(2,1)} %bitcast.70, bf16[8,3,64,256]{3,2,1,0:T(8,128)(2,1)} %maximum_maximum_fusion.query_gate, bf16[8,352,128]{2,1,0:T(8,128)(2,1)} %copy-done.2, bf16[8,352,128]{2,1,0:T(8,128)(2,1)} %copy-done.3, ...), custom_call_target="tpu_custom_call" | custom-call | tf_op jit(solution)/shard_map/attend/pallas_call | solution.py:425
  182.9 4.1 %all-to-all-start.4 = ((bf16[8,256,256]{2,1,0:T(8,128)(2,1)}), bf16[8,256,256]{2,1,0:T(8,128)(2,1)S(1)}, u32[]{:S(2)}, u32[]{:S(2)}) async-start(bf16[8,256,256]{2,1,0:T(8,128)(2,1)} %attend.1), calls=%async_computation.4 | async-start | bytes 2097152 | tf_op jit(solution)/shard_map/all_to_all | solution.py:441
  188.3 2.1 collective-permute-start.5
  193.8 4.1 %local.1 = (f32[256,192]{1,0:T(8,128)}, bf16[256,192]{1,0:T(8,128)(2,1)}) custom-call(f32[256,896]{1,0:T(8,128)} %get-tuple-element.18.proj, f32[256,32]{1,0:T(8,128)} %get-tuple-element.35.cosine, f32[256,32]{1,0:T(8,128)} %get-tuple-element.34.sine, f32[256,3]{1,0:T(8,128)} %copy.156.decay, f32[8,256]{1,0:T(8,128)} %pad.9.decay_row), custom_call_target="tpu_custom_call" | custom-call | tf_op jit(solution)/shard_map/local/pallas_call | solution.py:410
  197.9 13.8 %all-to-all-done.4.parts = bf16[8,256,256]{2,1,0:T(8,128)(2,1)S(1)} async-done(((bf16[8,256,256]{2,1,0:T(8,128)(2,1)}), bf16[8,256,256]{2,1,0:T(8,128)(2,1)S(1)}, u32[]{:S(2)}, u32[]{:S(2)}) %all-to-all-start.4) | async-done | bytes 1048608 | tf_op jit(solution)/shard_map/all_to_all | solution.py:441
  212.7 4.5 %back.1 = bf16[256,2048]{1,0:T(8,128)(2,1)} custom-call(bf16[8,256,256]{2,1,0:T(8,128)(2,1)} %copy-done, f32[256,192]{1,0:T(8,128)} %get-tuple-element.19.local, bf16[256,192]{1,0:T(8,128)(2,1)} %get-tuple-element.20.lifted, bf16[2048,384]{1,0:T(8,128)(2,1)} %bitcast.63), custom_call_target="tpu_custom_call" | custom-call | tf_op jit(solution)/shard_map/back/pallas_call | solution.py:443
  217.1 15.4 %all_to_all.30 = bf16[4,64,2048]{2,1,0:T(8,128)(2,1)S(1)} all-to-all(bf16[4,64,2048]{2,1,0:T(8,128)(2,1)} %bitcast.64), channel_id=1, replica_groups=mesh['z'=8,'y'=8,'c'=2,'tp'=4] {'tp'}, dimensions={0} | all-to-all | bytes 2097152 | tf_op jit(solution)/shard_map/all_to_all | solution.py:453
  (127 shorter events, 33.1 us)
Async XLA Ops:
  6.5 12.6 %copy-start.7 = (f32[2048]{0:T(1024)S(1)}, f32[2048]{0:T(1024)}, u32[]{:S(2)}) copy-start(f32[2048]{0:T(1024)} %param.13) | copy-start | bytes 24580
  9.1 17.5 %all-to-all-start = ((bf16[8,16,1408]{2,1,0:T(8,128)(2,1)}), bf16[8,16,1408]{2,1,0:T(8,128)(2,1)S(1)}, u32[]{:S(2)}, u32[]{:S(2)}) async-start(bf16[8,16,1408]{2,1,0:T(8,128)(2,1)} %broadcast_in_dim.165), calls=%async_computation | async-start | bytes 720896 | tf_op jit(solution)/shard_map/all_to_all | solution.py:27
  27.8 4.5 %copy-start.4 = (f32[3,32768]{1,0:T(4,128)S(1)}, f32[3,32768]{1,0:T(4,128)}, u32[]{:S(2)}) copy-start(f32[3,32768]{1,0:T(4,128)} %param.23) | copy-start | bytes 1179652
  27.8 15.4 %all-to-all-start.2 = ((bf16[4,2,64,1024]{3,2,1,0:T(8,128)(2,1)}), bf16[4,2,64,1024]{3,2,1,0:T(8,128)(2,1)S(1)}, u32[]{:S(2)}, u32[]{:S(2)}) async-start(bf16[4,2,64,1024]{3,2,1,0:T(8,128)(2,1)} %broadcast_in_dim.177), calls=%async_computation.2 | async-start | bytes 2097152 | tf_op jit(solution)/shard_map/all_to_all | solution.py:27
  31.4 52.0 %all-gather.4.cloned.1.call-start = ((), (), s32[]{:S(2)}) async-start(), calls=%async_computation.6 | async-start | bytes 2949120 | tf_op jit(solution)/shard_map/all_gather | solution.py:283
  43.3 3.8 %collective-permute-start.1 = (bf16[256,1024]{1,0:T(8,128)(2,1)S(1)}, bf16[256,1024]{1,0:T(8,128)(2,1)S(1)}, u32[]{:S(2)}, u32[]{:S(2)}) collective-permute-start(bf16[256,1024]{1,0:T(8,128)(2,1)S(1)} %bitcast.72), channel_id=1, source_target_pairs={{0,4},{4,0},{1,5},{5,1},{2,6},{6,2},{3,7},{7,3},{8,12},{12,8},{9,1... | collective-permute-start | bytes 1572872 | tf_op jit(solution)/shard_map/ppermute | solution.py:31
  48.1 41.4 %copy-start.6 = (f32[256,3]{0,1:T(4,128)S(1)}, f32[256,3]{0,1:T(4,128)}, u32[]{:S(2)}) copy-start(f32[256,3]{0,1:T(4,128)} %param.22) | copy-start | bytes 9220
  87.6 9.6 %collective-permute-start.2 = (f32[256,896]{1,0:T(8,128)}, f32[256,896]{1,0:T(8,128)S(1)}, u32[]{:S(2)}, u32[]{:S(2)}) collective-permute-start(f32[256,896]{1,0:T(8,128)} %get-tuple-element.14), channel_id=1, source_target_pairs={{0,4},{4,0},{1,5},{5,1},{2,6},{6,2},{3,7},{7,3},{8,12},{12,8},{9,1... | collective-permute-start | bytes 2752520 | tf_op jit(solution)/shard_map/ppermute | solution.py:31
  93.0 20.0 %all-to-all-start.1 = ((f32[8,8,3]{1,2,0:T(4,128)}), f32[8,8,3]{1,2,0:T(4,128)S(1)}, u32[]{:S(2)}, u32[]{:S(2)}) async-start(f32[8,8,3]{1,2,0:T(4,128)} %broadcast_in_dim.166), calls=%async_computation.1 | async-start | bytes 32768 | tf_op jit(solution)/shard_map/all_to_all | solution.py:27
  97.2 1.0 copy-start.1
  100.2 10.4 %collective-permute-start.3 = (bf16[256,128]{1,0:T(8,128)(2,1)}, bf16[256,128]{1,0:T(8,128)(2,1)S(1)}, u32[]{:S(2)}, u32[]{:S(2)}) collective-permute-start(bf16[256,128]{1,0:T(8,128)(2,1)} %get-tuple-element.16), channel_id=1, source_target_pairs={{0,0},{8,456},{16,16},{24,472},{32,32},{40,488},{48,48},{56,504},{... | collective-permute-start | bytes 196616 | tf_op jit(solution)/shard_map/ppermute | solution.py:391
  110.5 0.6 copy-start.5
  113.0 23.6 %all-to-all-start.3 = ((bf16[8,352,128]{2,1,0:T(8,128)(2,1)}), bf16[8,352,128]{2,1,0:T(8,128)(2,1)S(1)}, u32[]{:S(2)}, u32[]{:S(2)}) async-start(bf16[8,352,128]{2,1,0:T(8,128)(2,1)} %spread.1), calls=%async_computation.3 | async-start | bytes 1441792 | tf_op jit(solution)/shard_map/all_to_all | solution.py:408
  119.3 44.5 %all-gather.6.cloned.1.call-start = ((), (), s32[]{:S(2)}) async-start(), calls=%async_computation.7 | async-start | bytes 1179648 | tf_op jit(solution)/shard_map/all_gather | solution.py:390
  122.6 3.2 %collective-permute-start = (f32[8,8,3]{1,2,0:T(4,128)S(1)}, f32[8,8,3]{1,2,0:T(4,128)S(1)}, u32[]{:S(2)}, u32[]{:S(2)}) collective-permute-start(f32[8,8,3]{1,2,0:T(4,128)S(1)} %all-to-all-done.1), channel_id=1, source_target_pairs={{0,4},{4,0},{1,5},{5,1},{2,6},{6,2},{3,7},{7,3},{8,12},{12,8},{9,1... | collective-permute-start | bytes 2312 | tf_op jit(solution)/shard_map/ppermute | solution.py:31
  136.6 27.1 %copy-start.2 = (bf16[8,352,128]{2,1,0:T(8,128)(2,1)}, bf16[8,352,128]{2,1,0:T(8,128)(2,1)S(1)}, u32[]{:S(2)}) copy-start(bf16[8,352,128]{2,1,0:T(8,128)(2,1)S(1)} %all-to-all-done.3.kv_own) | copy-start | bytes 2162692
  136.6 27.1 %collective-permute-start.4 = (bf16[8,352,128]{2,1,0:T(8,128)(2,1)S(1)}, bf16[8,352,128]{2,1,0:T(8,128)(2,1)S(1)}, u32[]{:S(2)}, u32[]{:S(2)}) collective-permute-start(bf16[8,352,128]{2,1,0:T(8,128)(2,1)S(1)} %all-to-all-done.3.kv_own), channel_id=1, source_target_pairs={{0,4},{4,0},{1,5},{5,1},{2,6},{6,2},{3,7},{7,3},{8,12},{12,8},{9,1... | collective-permute-start | bytes 2162696 | tf_op jit(solution)/shard_map/ppermute | solution.py:31
  163.7 0.9 copy-start.3
  182.9 28.8 %all-to-all-start.4 = ((bf16[8,256,256]{2,1,0:T(8,128)(2,1)}), bf16[8,256,256]{2,1,0:T(8,128)(2,1)S(1)}, u32[]{:S(2)}, u32[]{:S(2)}) async-start(bf16[8,256,256]{2,1,0:T(8,128)(2,1)} %attend.1), calls=%async_computation.4 | async-start | bytes 2097152 | tf_op jit(solution)/shard_map/all_to_all | solution.py:441
  188.3 4.2 %collective-permute-start.5 = (bf16[1024,384]{1,0:T(8,128)(2,1)S(1)}, bf16[1024,384]{1,0:T(8,128)(2,1)S(1)}, u32[]{:S(2)}, u32[]{:S(2)}) collective-permute-start(bf16[1024,384]{1,0:T(8,128)(2,1)S(1)} %slice.35), channel_id=1, source_target_pairs={{0,4},{4,0},{1,5},{5,1},{2,6},{6,2},{3,7},{7,3},{8,12},{12,8},{9,1... | collective-permute-start | bytes 2359304 | tf_op jit(solution)/shard_map/ppermute | solution.py:31
  211.7 1.0 copy-start
Sparse Core Ops, SparseCore 0:
  34.3 49.0 all-gather.3
  122.1 41.5 all-gather.5

commit v10 on v8

--- a/solution.py
+++ b/solution.py
@@ -14,7 +14,7 @@
 LOG2E = 1.4426950408889634
 F32 = jnp.float32
 BF16 = jnp.bfloat16
-ROTATION = [(z * 8 + y, ((z + y) % 8) * 8 + y) for z in range(8) for y in range(8)]
+MIRROR = [(z * 8 + y, (7 - z if y % 2 else z) * 8 + y) for z in range(8) for y in range(8)]
 NT = (((1,), (1,)), ((), ()))
 TN = (((0,), (0,)), ((), ()))
 VMEM = pl.BlockSpec(memory_space=pltpu.VMEM)
@@ -73,6 +73,12 @@
         faded = (key.astype(F32) * jnp.exp(last - column)).astype(BF16)
         update = lax.dot_general(faded, value, TN, preferred_element_type=F32).astype(BF16)
         state_out[32 * h : 32 * (h + 1)] = jnp.concatenate([update[:32], update[32:]], axis=1)
+
+
+def spread_kernel(pairs, states, out):
+    for y in range(8):
+        out[y, :SPAN] = pairs[...]
+        out[y, SPAN:] = states[...]
 
 
 def local_kernel(proj, cosine, sine, decay, decay_row, local_out, lifted_out):
@@ -216,7 +222,7 @@
     put(plan[67], here)
 
 
-def back_kernel(parts, local, lifted, w_out, out, mixed):
+def back_kernel(turn, parts, local, lifted, w_out, far, mixed):
     total = parts[0].astype(F32)
     for z in range(1, 8):
         total = total + parts[z].astype(F32)
@@ -233,9 +239,20 @@
         weight = total[192 + h : 193 + h] + total[195 + h : 196 + h]
         attended = total[h * HEAD : (h + 1) * HEAD] / weight
         mixed[:, 192 + h * HEAD : 192 + (h + 1) * HEAD] = jnp.transpose(attended).astype(BF16)
-    out[...] = lax.dot_general(
-        mixed[...], w_out[...], NT, preferred_element_type=F32
+
+    far[...] = lax.dot_general(
+        mixed[pl.ds((turn[0] + 2) % 4 * 64, 64)], w_out[...], NT, preferred_element_type=F32
     ).astype(BF16)
+
+
+def rest_kernel(turn, mixed, w_out, ahead, behind, own):
+    rows = [mixed[pl.ds((turn[0] + k) % 4 * 64, 64)] for k in (1, 3, 0)]
+    product = lax.dot_general(
+        jnp.concatenate(rows, axis=0), w_out[...], NT, preferred_element_type=F32
+    ).astype(BF16)
+    ahead[...] = product[:64]
+    behind[...] = product[64:128]
+    own[...] = product[128:]
 
 
 def body(
@@ -301,7 +318,7 @@
 
     gate = (forget_total * LOG2E).reshape(3, 8, 8, 2, SPAN)
     spans = jnp.arange(8, dtype=jnp.int32)
-    key_z = (z - spans) % 8
+    key_z = jnp.where(spans % 2 == 0, z, 7 - z)
     chosen = (spans[:, None] == key_z[None, :])[None, :, :, None, None]
     key_side = jnp.sum(jnp.where(chosen, gate, 0.0), axis=1)
     key_side = jnp.where(c == 0, key_side, key_side[:, :, ::-1])
@@ -352,7 +369,7 @@
     units = jnp.sum(
         jnp.where(needed[None, :] & (slot[None, :] == order[:, None]), order[None, :], 0), axis=1
     )
-    own = jnp.stack([(z - y) % 8 * 8 + y])
+    own = jnp.stack([jnp.where(y % 2 == 0, z, 7 - z) * 8 + y])
     plan = jnp.concatenate([own, units, jnp.stack([jnp.sum(needed.astype(jnp.int32)) + 1, c, z])])
 
     own_part, oth_part = pl.pallas_call(
@@ -379,7 +396,7 @@
         name="share",
     )(own_part, came_part)
     queries = lax.all_gather(q_send, "z", axis=0)
-    kv_send = lax.ppermute(kv_send, ("z", "y"), ROTATION)
+    kv_send = lax.ppermute(kv_send, ("z", "y"), MIRROR)
     state_send, proj = pl.pallas_call(
         front_kernel,
         in_specs=[VMEM] * 5,
@@ -388,8 +405,15 @@
         compiler_params=PARAMS,
         name="front",
     )(own_part, came_part, cosine, sine, decay)
-    kv_send = jnp.concatenate([kv_send, state_send], axis=0)
-    kv_own = copies_from(kv_send, "y")
+    kv_send = pl.pallas_call(
+        spread_kernel,
+        in_specs=[VMEM] * 2,
+        out_specs=VMEM,
+        out_shape=jax.ShapeDtypeStruct((8, SPAN + 96, 128), BF16),
+        compiler_params=PARAMS,
+        name="spread",
+    )(kv_send, state_send)
+    kv_own = lax.all_to_all(kv_send, "y", 0, 0, tiled=True)
     kv_oth = swapped_cores(kv_own)
     local, lifted = pl.pallas_call(
         local_kernel,
@@ -424,17 +448,29 @@
     )(plan, fade, queries, query_gate, kv_own, kv_oth, key_gate)
     parts = lax.all_to_all(partial, "z", 0, 0, tiled=True)
 
-    share = pl.pallas_call(
+    turn = lax.axis_index("tp").reshape(1)
+    chunk = jax.ShapeDtypeStruct((64, 2048), BF16)
+    far, mixed = pl.pallas_call(
         back_kernel,
-        in_specs=[VMEM] * 4,
-        out_specs=VMEM,
-        out_shape=jax.ShapeDtypeStruct((SPAN, 2048), BF16),
-        scratch_shapes=[pltpu.VMEM((SPAN, 384), BF16)],
+        in_specs=[SMEM] + [VMEM] * 4,
+        out_specs=[VMEM] * 2,
+        out_shape=[chunk, jax.ShapeDtypeStruct((SPAN, 384), BF16)],
         compiler_params=PARAMS,
         name="back",
-    )(parts, local, lifted, w_out)
-    shares = lax.all_to_all(share.reshape(4, 64, 2048), "tp", 0, 0, tiled=True)
-    return jnp.sum(shares.astype(F32), axis=0).astype(BF16)
+    )(turn, parts, local, lifted, w_out)
+    far = lax.ppermute(far, "tp", [(i, (i + 2) % 4) for i in range(4)])
+    ahead, behind, own = pl.pallas_call(
+        rest_kernel,
+        in_specs=[SMEM] + [VMEM] * 2,
+        out_specs=[VMEM] * 3,
+        out_shape=[chunk] * 3,
+        compiler_params=PARAMS,
+        name="rest",
+    )(turn, mixed, w_out)
+    ahead = lax.ppermute(ahead, "tp", [(i, (i + 1) % 4) for i in range(4)])
+    behind = lax.ppermute(behind, "tp", [(i, (i + 3) % 4) for i in range(4)])
+    total = own.astype(F32) + far.astype(F32) + ahead.astype(F32) + behind.astype(F32)
+    return total.astype(BF16)
 
 
 def solution(mesh):

time: 242 us -> 247 us (1.021)
  blocking collectives: 15.4 us -> 0 us
  starting transfers between devices: 42.3 us -> 52.4 us
  waiting for transfers between devices: 103 us -> 109 us
  Pallas kernels: 37.3 us -> 41.8 us
    all_to_all x1 -> x0, blocking collectives: 15.4 us -> none  [body(): shares = lax.all_to_all(share.reshape(4, 64, 2048), 'tp', 0, 0, tiled=True)]
    ppermute x1 -> x4, starting transfers between devices: 3.91 us -> 15.8 us  [the longest x1 5.13 us: body(): kv_send = lax.ppermute(kv_send, ('z', 'y'), MIRROR)]
    all_to_all x4 -> x3, waiting for transfers between devices: 27.3 us -> 15.4 us  [copies_from(): return lax.all_to_all(copies, axis, split_axis=0, concat_axis=0, tiled=True)]
    all_to_all x0 -> x1, waiting for transfers between devices: none -> 10.4 us  [body(): kv_own = lax.all_to_all(kv_send, 'y', 0, 0, tiled=True)]
    all_to_all x4 -> x3, starting transfers between devices: 24.5 us -> 16.4 us  [copies_from(): return lax.all_to_all(copies, axis, split_axis=0, concat_axis=0, tiled=True)]
    all_to_all x0 -> x1, starting transfers between devices: none -> 6.26 us  [body(): kv_own = lax.all_to_all(kv_send, 'y', 0, 0, tiled=True)]
    ppermute x1 -> x4, waiting for transfers between devices: 0.01 us -> 6.09 us  [the longest x1 4 us: body(): far = lax.ppermute(far, 'tp', [(i, (i + 2) % 4) for i in range(4)])]
    pallas_call x1 -> x3, Pallas kernels: 5.02 us -> 9.47 us  [the longest x1 4.53 us: body(): pl.pallas_call(back_kernel, in_specs=[SMEM] + [VMEM] * 4, out_specs=[VMEM...]
  transfers between devices with their start and end apart: 13 -> 16, of which waited for: 9 -> 11; matrix products, arithmetic and copies ran while one was open for 8% -> 8% of each run, Pallas kernels for 3% -> 5%
where the time goes in v10:
time: 247 us; the launch traced here: 246 us
  waiting for transfers between devices  109 us (44%)
  starting transfers between devices  52.4 us (21%)
  Pallas kernels  41.8 us (17%)
  local copies, waits for them, and re-layouts  14.9 us (6%)
  between operations  14.6 us (6%)
  other arithmetic  13.4 us (5%)
    all_gather x1, waiting for transfers between devices, body(): w_own = lax.all_gather(w_row, 'z', axis=0, tiled=True)  35.3 us
    all_gather x1, waiting for transfers between devices, body(): queries = lax.all_gather(q_send, 'z', axis=0)  23.8 us
    pallas_call x1, Pallas kernels, body(): pl.pallas_call(attend_kernel, in_specs=[SMEM] * 2 + [VMEM] * 5, out_specs...  18.3 us
    all_to_all x3, starting transfers between devices, copies_from(): return lax.all_to_all(copies, axis, split_axis=0, concat_axis=0, tiled=True)  16.4 us
    all_to_all x3, waiting for transfers between devices, copies_from(): return lax.all_to_all(copies, axis, split_axis=0, concat_axis=0, tiled=True)  15.4 us
    all_to_all x1, waiting for transfers between devices, body(): parts = lax.all_to_all(partial, 'z', 0, 0, tiled=True)  13.8 us
    all_to_all x1, waiting for transfers between devices, body(): kv_own = lax.all_to_all(kv_send, 'y', 0, 0, tiled=True)  10.4 us
    ppermute x5, starting transfers between devices, swapped_cores(): return lax.ppermute(value, 'c', [(0, 1), (1, 0)])  9.75 us
  transfers between devices with their start and end apart: 16, of which 11 were waited for; matrix products, arithmetic and copies ran while one was open for 8% of the time, Pallas kernels for 5%

profile of v10, /device:TPU:56, one launch (start us, length us, event | category | flops | bytes accessed | tf_op | source)
XLA Modules:
  0.0 245.8 jit_solution(2622513456684717818)
XLA Ops:
  9.1 8.5 %all-to-all-start = ((bf16[8,16,1408]{2,1,0:T(8,128)(2,1)}), bf16[8,16,1408]{2,1,0:T(8,128)(2,1)S(1)}, u32[]{:S(2)}, u32[]{:S(2)}) async-start(bf16[8,16,1408]{2,1,0:T(8,128)(2,1)} %broadcast_in_dim.165), calls=%async_computation | async-start | bytes 720896 | tf_op jit(solution)/shard_map/all_to_all | solution.py:27
  19.7 6.9 %all-to-all-done = bf16[8,16,1408]{2,1,0:T(8,128)(2,1)S(1)} async-done(((bf16[8,16,1408]{2,1,0:T(8,128)(2,1)}), bf16[8,16,1408]{2,1,0:T(8,128)(2,1)S(1)}, u32[]{:S(2)}, u32[]{:S(2)}) %all-to-all-start) | async-done | bytes 360480 | tf_op jit(solution)/shard_map/all_to_all | solution.py:27
  27.7 3.6 %all-to-all-start.2 = ((bf16[4,2,64,1024]{3,2,1,0:T(8,128)(2,1)}), bf16[4,2,64,1024]{3,2,1,0:T(8,128)(2,1)S(1)}, u32[]{:S(2)}, u32[]{:S(2)}) async-start(bf16[4,2,64,1024]{3,2,1,0:T(8,128)(2,1)} %broadcast_in_dim.177), calls=%async_computation.2 | async-start | bytes 2097152 | tf_op jit(solution)/shard_map/all_to_all | solution.py:27
  34.6 8.5 %all-to-all-done.2 = bf16[4,2,64,1024]{3,2,1,0:T(8,128)(2,1)S(1)} async-done(((bf16[4,2,64,1024]{3,2,1,0:T(8,128)(2,1)}), bf16[4,2,64,1024]{3,2,1,0:T(8,128)(2,1)S(1)}, u32[]{:S(2)}, u32[]{:S(2)}) %all-to-all-start.2) | async-done | bytes 1048608 | tf_op jit(solution)/shard_map/all_to_all | solution.py:27
  48.1 35.3 %all-gather.4.cloned.1.call-done.weights = bf16[1024,1280]{1,0:T(8,128)(2,1)} async-done(((bf16[128,1280]{1,0:T(8,128)(2,1)}), bf16[1024,1280]{1,0:T(8,128)(2,1)}) %all-gather.4.cloned.1.call-update) | async-done | bytes 2621456 | tf_op jit(solution)/shard_map/all_gather | solution.py:291
  83.4 4.3 %project.1 = (f32[256,896]{1,0:T(8,128)}, f32[256,896]{1,0:T(8,128)}) custom-call(bf16[512,1024]{1,0:T(8,128)(2,1)} %pad_maximum_fusion.rows, bf16[1024,1280]{1,0:T(8,128)(2,1)} %all-gather.4.cloned.1.call-done.weights), custom_call_target="tpu_custom_call" | custom-call | tf_op jit(solution)/shard_map/project/pallas_call | solution.py:375
  93.0 4.3 %all-to-all-start.1 = ((f32[8,8,3]{1,2,0:T(4,128)}), f32[8,8,3]{1,2,0:T(4,128)S(1)}, u32[]{:S(2)}, u32[]{:S(2)}) async-start(f32[8,8,3]{1,2,0:T(4,128)} %broadcast_in_dim.166), calls=%async_computation.1 | async-start | bytes 32768 | tf_op jit(solution)/shard_map/all_to_all | solution.py:27
  98.2 2.0 share.1
  100.1 5.1 %collective-permute-start.3 = (bf16[256,128]{1,0:T(8,128)(2,1)}, bf16[256,128]{1,0:T(8,128)(2,1)S(1)}, u32[]{:S(2)}, u32[]{:S(2)}) collective-permute-start(bf16[256,128]{1,0:T(8,128)(2,1)} %get-tuple-element.21), channel_id=1, source_target_pairs={{0,0},{8,456},{16,16},{24,472},{32,32},{40,488},{48,48},{56,504},{... | collective-permute-start | bytes 196616 | tf_op jit(solution)/shard_map/ppermute | solution.py:399
  106.8 3.7 %front.1 = (bf16[96,128]{1,0:T(8,128)(2,1)}, f32[256,896]{1,0:T(8,128)}) custom-call(f32[256,896]{1,0:T(8,128)} %get-tuple-element.18.first_part, f32[256,896]{1,0:T(8,128)} %copy-done.1, f32[256,32]{1,0:T(8,128)} %get-tuple-element.45.cosine, f32[256,32]{1,0:T(8,128)} %get-tuple-element.44.sine, f32[256,3]{1,0:T(8,128)} %copy.156.decay), custom_call_target="tpu_custom_call" | custom-call | tf_op jit(solution)/shard_map/front/pallas_call | solution.py:400
  113.0 6.3 %all-to-all-start.3 = ((bf16[8,352,128]{2,1,0:T(8,128)(2,1)}), bf16[8,352,128]{2,1,0:T(8,128)(2,1)S(1)}, u32[]{:S(2)}, u32[]{:S(2)}) async-start(bf16[8,352,128]{2,1,0:T(8,128)(2,1)} %spread.1), calls=%async_computation.3 | async-start | bytes 1441792 | tf_op jit(solution)/shard_map/all_to_all | solution.py:416
  126.2 10.4 %all-to-all-done.3.kv_own = bf16[8,352,128]{2,1,0:T(8,128)(2,1)S(1)} async-done(((bf16[8,352,128]{2,1,0:T(8,128)(2,1)}), bf16[8,352,128]{2,1,0:T(8,128)(2,1)S(1)}, u32[]{:S(2)}, u32[]{:S(2)}) %all-to-all-start.3) | async-done | bytes 720928 | tf_op jit(solution)/shard_map/all_to_all | solution.py:416
  139.9 23.8 %all-gather.6.cloned.1.call-done = bf16[2048,256]{1,0:T(8,128)(2,1)} async-done(((bf16[256,256]{1,0:T(8,128)(2,1)}), bf16[2048,256]{1,0:T(8,128)(2,1)}) %all-gather.6.cloned.1.call-update) | async-done | bytes 1048592 | tf_op jit(solution)/shard_map/all_gather | solution.py:398
  164.6 18.3 %attend.1 = bf16[8,256,256]{2,1,0:T(8,128)(2,1)} custom-call(s32[68]{0:T(128)} %concatenate.29.plan, f32[120]{0:T(128)} %pad_maximum_fusion.2.fade, bf16[8,256,256]{2,1,0:T(8,128)(2,1)} %bitcast.70, bf16[8,3,64,256]{3,2,1,0:T(8,128)(2,1)} %maximum_maximum_fusion.query_gate, bf16[8,352,128]{2,1,0:T(8,128)(2,1)} %copy-done.2, bf16[8,352,128]{2,1,0:T(8,128)(2,1)} %copy-done.3, ...), custom_call_target="tpu_custom_call" | custom-call | tf_op jit(solution)/shard_map/attend/pallas_call | solution.py:433
  182.9 4.1 %all-to-all-start.4 = ((bf16[8,256,256]{2,1,0:T(8,128)(2,1)}), bf16[8,256,256]{2,1,0:T(8,128)(2,1)S(1)}, u32[]{:S(2)}, u32[]{:S(2)}) async-start(bf16[8,256,256]{2,1,0:T(8,128)(2,1)} %attend.1), calls=%async_computation.4 | async-start | bytes 2097152 | tf_op jit(solution)/shard_map/all_to_all | solution.py:449
  188.2 2.1 collective-permute-start.5
  193.8 4.1 %local.1 = (f32[256,192]{1,0:T(8,128)}, bf16[256,192]{1,0:T(8,128)(2,1)}) custom-call(f32[256,896]{1,0:T(8,128)} %get-tuple-element.23.proj, f32[256,32]{1,0:T(8,128)} %get-tuple-element.45.cosine, f32[256,32]{1,0:T(8,128)} %get-tuple-element.44.sine, f32[256,3]{1,0:T(8,128)} %copy.156.decay, f32[8,256]{1,0:T(8,128)} %pad.9.decay_row), custom_call_target="tpu_custom_call" | custom-call | tf_op jit(solution)/shard_map/local/pallas_call | solution.py:418
  197.9 13.8 %all-to-all-done.4.parts = bf16[8,256,256]{2,1,0:T(8,128)(2,1)S(1)} async-done(((bf16[8,256,256]{2,1,0:T(8,128)(2,1)}), bf16[8,256,256]{2,1,0:T(8,128)(2,1)S(1)}, u32[]{:S(2)}, u32[]{:S(2)}) %all-to-all-start.4) | async-done | bytes 1048608 | tf_op jit(solution)/shard_map/all_to_all | solution.py:449
  212.6 4.5 %back.1 = (bf16[64,2048]{1,0:T(8,128)(2,1)}, bf16[256,384]{1,0:T(8,128)(2,1)}) custom-call(s32[1]{0:T(128)} %bitcast.turn, bf16[8,256,256]{2,1,0:T(8,128)(2,1)} %copy-done, f32[256,192]{1,0:T(8,128)} %get-tuple-element.24.local, bf16[256,192]{1,0:T(8,128)(2,1)} %get-tuple-element.25.lifted, bf16[2048,384]{1,0:T(8,128)(2,1)} %bitcast.63), custom_call_target="tpu_custom_call" | custom-call | tf_op jit(solution)/shard_map/back/pallas_call | solution.py:453
  217.2 3.1 %rest.1 = (bf16[64,2048]{1,0:T(8,128)(2,1)}, bf16[64,2048]{1,0:T(8,128)(2,1)}, bf16[64,2048]{1,0:T(8,128)(2,1)}) custom-call(s32[1]{0:T(128)} %bitcast.turn, bf16[256,384]{1,0:T(8,128)(2,1)} %get-tuple-element.26.mixed, bf16[2048,384]{1,0:T(8,128)(2,1)} %bitcast.64), custom_call_target="tpu_custom_call" | custom-call | tf_op jit(solution)/shard_map/rest/pallas_call | solution.py:462
  220.3 3.4 %collective-permute-start.7 = (bf16[64,2048]{1,0:T(8,128)(2,1)}, bf16[64,2048]{1,0:T(8,128)(2,1)S(1)}, u32[]{:S(2)}, u32[]{:S(2)}) collective-permute-start(bf16[64,2048]{1,0:T(8,128)(2,1)} %get-tuple-element.29), channel_id=1, source_target_pairs={{0,1},{1,2},{2,3},{3,0},{4,5},{5,6},{6,7},{7,4},{8,9},{9,10},{10,1... | collective-permute-start | bytes 786440 | tf_op jit(solution)/shard_map/ppermute | solution.py:470
  223.7 3.7 %collective-permute-start.8 = (bf16[64,2048]{1,0:T(8,128)(2,1)}, bf16[64,2048]{1,0:T(8,128)(2,1)S(1)}, u32[]{:S(2)}, u32[]{:S(2)}) collective-permute-start(bf16[64,2048]{1,0:T(8,128)(2,1)} %get-tuple-element.30), channel_id=1, source_target_pairs={{0,3},{1,0},{2,1},{3,2},{4,7},{5,4},{6,5},{7,6},{8,11},{9,8},{10,9... | collective-permute-start | bytes 786440 | tf_op jit(solution)/shard_map/ppermute | solution.py:471
  227.4 3.7 %collective-permute-start.6 = (bf16[64,2048]{1,0:T(8,128)(2,1)S(1)}, bf16[64,2048]{1,0:T(8,128)(2,1)S(1)}, u32[]{:S(2)}, u32[]{:S(2)}) collective-permute-start(bf16[64,2048]{1,0:T(8,128)(2,1)S(1)} %copy-done.8), channel_id=1, source_target_pairs={{0,2},{1,3},{2,0},{3,1},{4,6},{5,7},{6,4},{7,5},{8,10},{9,11},{10,... | collective-permute-start | bytes 786440 | tf_op jit(solution)/shard_map/ppermute | solution.py:461
  233.1 4.0 %collective-permute-done.6 = bf16[64,2048]{1,0:T(8,128)(2,1)S(1)} collective-permute-done((bf16[64,2048]{1,0:T(8,128)(2,1)S(1)}, bf16[64,2048]{1,0:T(8,128)(2,1)S(1)}, u32[]{:S(2)}, u32[]{:S(2)}) %collective-permute-start.6) | collective-permute-done | bytes 262176 | tf_op jit(solution)/shard_map/ppermute | solution.py:461
  (135 shorter events, 43.7 us)
Async XLA Ops:
  6.5 12.6 %copy-start.7 = (f32[2048]{0:T(1024)S(1)}, f32[2048]{0:T(1024)}, u32[]{:S(2)}) copy-start(f32[2048]{0:T(1024)} %param.13) | copy-start | bytes 24580
  9.1 17.5 %all-to-all-start = ((bf16[8,16,1408]{2,1,0:T(8,128)(2,1)}), bf16[8,16,1408]{2,1,0:T(8,128)(2,1)S(1)}, u32[]{:S(2)}, u32[]{:S(2)}) async-start(bf16[8,16,1408]{2,1,0:T(8,128)(2,1)} %broadcast_in_dim.165), calls=%async_computation | async-start | bytes 720896 | tf_op jit(solution)/shard_map/all_to_all | solution.py:27
  27.7 4.5 %copy-start.4 = (f32[3,32768]{1,0:T(4,128)S(1)}, f32[3,32768]{1,0:T(4,128)}, u32[]{:S(2)}) copy-start(f32[3,32768]{1,0:T(4,128)} %param.23) | copy-start | bytes 1179652
  27.7 15.4 %all-to-all-start.2 = ((bf16[4,2,64,1024]{3,2,1,0:T(8,128)(2,1)}), bf16[4,2,64,1024]{3,2,1,0:T(8,128)(2,1)S(1)}, u32[]{:S(2)}, u32[]{:S(2)}) async-start(bf16[4,2,64,1024]{3,2,1,0:T(8,128)(2,1)} %broadcast_in_dim.177), calls=%async_computation.2 | async-start | bytes 2097152 | tf_op jit(solution)/shard_map/all_to_all | solution.py:27
  31.4 52.0 %all-gather.4.cloned.1.call-start = ((), (), s32[]{:S(2)}) async-start(), calls=%async_computation.5 | async-start | bytes 2949120 | tf_op jit(solution)/shard_map/all_gather | solution.py:291
  43.2 3.8 %collective-permute-start.1 = (bf16[256,1024]{1,0:T(8,128)(2,1)S(1)}, bf16[256,1024]{1,0:T(8,128)(2,1)S(1)}, u32[]{:S(2)}, u32[]{:S(2)}) collective-permute-start(bf16[256,1024]{1,0:T(8,128)(2,1)S(1)} %bitcast.72), channel_id=1, source_target_pairs={{0,4},{4,0},{1,5},{5,1},{2,6},{6,2},{3,7},{7,3},{8,12},{12,8},{9,1... | collective-permute-start | bytes 1572872 | tf_op jit(solution)/shard_map/ppermute | solution.py:31
  48.1 41.5 %copy-start.6 = (f32[256,3]{0,1:T(4,128)S(1)}, f32[256,3]{0,1:T(4,128)}, u32[]{:S(2)}) copy-start(f32[256,3]{0,1:T(4,128)} %param.22) | copy-start | bytes 9220
  87.6 9.6 %collective-permute-start.2 = (f32[256,896]{1,0:T(8,128)}, f32[256,896]{1,0:T(8,128)S(1)}, u32[]{:S(2)}, u32[]{:S(2)}) collective-permute-start(f32[256,896]{1,0:T(8,128)} %get-tuple-element.19), channel_id=1, source_target_pairs={{0,4},{4,0},{1,5},{5,1},{2,6},{6,2},{3,7},{7,3},{8,12},{12,8},{9,1... | collective-permute-start | bytes 2752520 | tf_op jit(solution)/shard_map/ppermute | solution.py:31
  93.0 20.0 %all-to-all-start.1 = ((f32[8,8,3]{1,2,0:T(4,128)}), f32[8,8,3]{1,2,0:T(4,128)S(1)}, u32[]{:S(2)}, u32[]{:S(2)}) async-start(f32[8,8,3]{1,2,0:T(4,128)} %broadcast_in_dim.166), calls=%async_computation.1 | async-start | bytes 32768 | tf_op jit(solution)/shard_map/all_to_all | solution.py:27
  97.2 0.9 copy-start.1
  100.1 10.4 %collective-permute-start.3 = (bf16[256,128]{1,0:T(8,128)(2,1)}, bf16[256,128]{1,0:T(8,128)(2,1)S(1)}, u32[]{:S(2)}, u32[]{:S(2)}) collective-permute-start(bf16[256,128]{1,0:T(8,128)(2,1)} %get-tuple-element.21), channel_id=1, source_target_pairs={{0,0},{8,456},{16,16},{24,472},{32,32},{40,488},{48,48},{56,504},{... | collective-permute-start | bytes 196616 | tf_op jit(solution)/shard_map/ppermute | solution.py:399
  113.0 23.6 %all-to-all-start.3 = ((bf16[8,352,128]{2,1,0:T(8,128)(2,1)}), bf16[8,352,128]{2,1,0:T(8,128)(2,1)S(1)}, u32[]{:S(2)}, u32[]{:S(2)}) async-start(bf16[8,352,128]{2,1,0:T(8,128)(2,1)} %spread.1), calls=%async_computation.3 | async-start | bytes 1441792 | tf_op jit(solution)/shard_map/all_to_all | solution.py:416
  119.2 44.5 %all-gather.6.cloned.1.call-start = ((), (), s32[]{:S(2)}) async-start(), calls=%async_computation.6 | async-start | bytes 1179648 | tf_op jit(solution)/shard_map/all_gather | solution.py:398
  122.5 3.2 %collective-permute-start = (f32[8,8,3]{1,2,0:T(4,128)S(1)}, f32[8,8,3]{1,2,0:T(4,128)S(1)}, u32[]{:S(2)}, u32[]{:S(2)}) collective-permute-start(f32[8,8,3]{1,2,0:T(4,128)S(1)} %all-to-all-done.1), channel_id=1, source_target_pairs={{0,4},{4,0},{1,5},{5,1},{2,6},{6,2},{3,7},{7,3},{8,12},{12,8},{9,1... | collective-permute-start | bytes 2312 | tf_op jit(solution)/shard_map/ppermute | solution.py:31
  136.6 27.1 %copy-start.2 = (bf16[8,352,128]{2,1,0:T(8,128)(2,1)}, bf16[8,352,128]{2,1,0:T(8,128)(2,1)S(1)}, u32[]{:S(2)}) copy-start(bf16[8,352,128]{2,1,0:T(8,128)(2,1)S(1)} %all-to-all-done.3.kv_own) | copy-start | bytes 2162692
  136.6 27.1 %collective-permute-start.4 = (bf16[8,352,128]{2,1,0:T(8,128)(2,1)S(1)}, bf16[8,352,128]{2,1,0:T(8,128)(2,1)S(1)}, u32[]{:S(2)}, u32[]{:S(2)}) collective-permute-start(bf16[8,352,128]{2,1,0:T(8,128)(2,1)S(1)} %all-to-all-done.3.kv_own), channel_id=1, source_target_pairs={{0,4},{4,0},{1,5},{5,1},{2,6},{6,2},{3,7},{7,3},{8,12},{12,8},{9,1... | collective-permute-start | bytes 2162696 | tf_op jit(solution)/shard_map/ppermute | solution.py:31
  163.7 0.9 copy-start.3
  182.9 28.8 %all-to-all-start.4 = ((bf16[8,256,256]{2,1,0:T(8,128)(2,1)}), bf16[8,256,256]{2,1,0:T(8,128)(2,1)S(1)}, u32[]{:S(2)}, u32[]{:S(2)}) async-start(bf16[8,256,256]{2,1,0:T(8,128)(2,1)} %attend.1), calls=%async_computation.4 | async-start | bytes 2097152 | tf_op jit(solution)/shard_map/all_to_all | solution.py:449
  188.2 4.2 %collective-permute-start.5 = (bf16[1024,384]{1,0:T(8,128)(2,1)S(1)}, bf16[1024,384]{1,0:T(8,128)(2,1)S(1)}, u32[]{:S(2)}, u32[]{:S(2)}) collective-permute-start(bf16[1024,384]{1,0:T(8,128)(2,1)S(1)} %slice.35), channel_id=1, source_target_pairs={{0,4},{4,0},{1,5},{5,1},{2,6},{6,2},{3,7},{7,3},{8,12},{12,8},{9,1... | collective-permute-start | bytes 2359304 | tf_op jit(solution)/shard_map/ppermute | solution.py:31
  211.7 1.0 copy-start
  217.2 10.2 %copy-start.8 = (bf16[64,2048]{1,0:T(8,128)(2,1)S(1)}, bf16[64,2048]{1,0:T(8,128)(2,1)}, u32[]{:S(2)}) copy-start(bf16[64,2048]{1,0:T(8,128)(2,1)} %get-tuple-element.28) | copy-start | bytes 786436
  220.3 10.9 %collective-permute-start.7 = (bf16[64,2048]{1,0:T(8,128)(2,1)}, bf16[64,2048]{1,0:T(8,128)(2,1)S(1)}, u32[]{:S(2)}, u32[]{:S(2)}) collective-permute-start(bf16[64,2048]{1,0:T(8,128)(2,1)} %get-tuple-element.29), channel_id=1, source_target_pairs={{0,1},{1,2},{2,3},{3,0},{4,5},{5,6},{6,7},{7,4},{8,9},{9,10},{10,1... | collective-permute-start | bytes 786440 | tf_op jit(solution)/shard_map/ppermute | solution.py:470
  223.7 9.5 %collective-permute-start.8 = (bf16[64,2048]{1,0:T(8,128)(2,1)}, bf16[64,2048]{1,0:T(8,128)(2,1)S(1)}, u32[]{:S(2)}, u32[]{:S(2)}) collective-permute-start(bf16[64,2048]{1,0:T(8,128)(2,1)} %get-tuple-element.30), channel_id=1, source_target_pairs={{0,3},{1,0},{2,1},{3,2},{4,7},{5,4},{6,5},{7,6},{8,11},{9,8},{10,9... | collective-permute-start | bytes 786440 | tf_op jit(solution)/shard_map/ppermute | solution.py:471
  227.4 9.8 %collective-permute-start.6 = (bf16[64,2048]{1,0:T(8,128)(2,1)S(1)}, bf16[64,2048]{1,0:T(8,128)(2,1)S(1)}, u32[]{:S(2)}, u32[]{:S(2)}) collective-permute-start(bf16[64,2048]{1,0:T(8,128)(2,1)S(1)} %copy-done.8), channel_id=1, source_target_pairs={{0,2},{1,3},{2,0},{3,1},{4,6},{5,7},{6,4},{7,5},{8,10},{9,11},{10,... | collective-permute-start | bytes 786440 | tf_op jit(solution)/shard_map/ppermute | solution.py:461
  (1 other events, 0.6 us)
Sparse Core Ops, SparseCore 0:
  34.3 49.0 all-gather.3
  122.1 41.5 all-gather.5

commit v11 on v9

--- a/solution.py
+++ b/solution.py
@@ -61,13 +61,13 @@
     return jnp.concatenate([first * cos - second * sin, first * sin + second * cos], axis=1)
 
 
-def front_kernel(first_part, second_part, cosine, sine, decay, state_out, proj_out):
-    proj_out[...] = first_part[...] + second_part[...]
+def front_kernel(first_part, second_part, cosine, sine, decay, state_out, proj):
+    proj[...] = first_part[:, 512:] + second_part[:, 512:]
     cos = cosine[...]
     sin = sine[...]
     for h in range(3):
-        key = turned(proj_out, 512 + h * HEAD, cos, sin).astype(BF16)
-        value = proj_out[:, 704 + h * HEAD : 704 + (h + 1) * HEAD].astype(BF16)
+        key = turned(proj, h * HEAD, cos, sin).astype(BF16)
+        value = proj[:, 192 + h * HEAD : 192 + (h + 1) * HEAD].astype(BF16)
         column = decay[:, h : h + 1]
         last = decay[SPAN - 1 : SPAN, h : h + 1]
         faded = (key.astype(F32) * jnp.exp(last - column)).astype(BF16)
@@ -81,7 +81,10 @@
         out[y, SPAN:] = states[...]
 
 
-def local_kernel(proj, cosine, sine, decay, decay_row, local_out, lifted_out):
+def local_kernel(
+    first_part, second_part, cosine, sine, decay, decay_row, local_out, lifted_out, proj
+):
+    proj[...] = first_part[...] + second_part[...]
     cos = cosine[...]
     sin = sine[...]
     place = lax.broadcasted_iota(jnp.int32, (SPAN, SPAN), 0)
@@ -161,17 +164,25 @@
     for h in range(3):
         score(0, even, h, allowed)
 
-    def pair(i, carry):
-        for h in range(3):
-            score(2 * i + 1, odd, h)
-            weigh(2 * i, even, h)
-        for h in range(3):
-            score(2 * i + 2, even, h)
-            weigh(2 * i + 1, odd, h)
+    def advance(first):
+        for h in range(3):
+            score(first + 1, odd, h)
+            weigh(first, even, h)
+        for h in range(3):
+            score(first + 2, even, h)
+            weigh(first + 1, odd, h)
+
+    def four(i, carry):
+        advance(4 * i)
+        advance(4 * i + 2)
         return carry
 
     count = plan[65]
-    lax.fori_loop(0, count // 2, pair, 0)
+    lax.fori_loop(0, count // 4, four, 0)
+
+    @pl.when(count % 4 >= 2)
+    def _():
+        advance(count // 4 * 4)
 
     @pl.when(count % 2 == 1)
     def _():
@@ -389,11 +400,12 @@
     )(own_part, came_part)
     queries = lax.all_gather(q_send, "z", axis=0)
     kv_send = lax.ppermute(kv_send, ("z", "y"), MIRROR)
-    state_send, proj = pl.pallas_call(
+    state_send = pl.pallas_call(
         front_kernel,
         in_specs=[VMEM] * 5,
-        out_specs=[VMEM] * 2,
-        out_shape=[jax.ShapeDtypeStruct((96, 128), BF16), jax.ShapeDtypeStruct((SPAN, 896), F32)],
+        out_specs=VMEM,
+        out_shape=jax.ShapeDtypeStruct((96, 128), BF16),
+        scratch_shapes=[pltpu.VMEM((SPAN, 384), F32)],
         compiler_params=PARAMS,
         name="front",
     )(own_part, came_part, cosine, sine, decay)
@@ -409,12 +421,13 @@
     kv_oth = swapped_cores(kv_own)
     local, lifted = pl.pallas_call(
         local_kernel,
-        in_specs=[VMEM] * 5,
+        in_specs=[VMEM] * 6,
         out_specs=[VMEM] * 2,
         out_shape=[jax.ShapeDtypeStruct((SPAN, 192), F32), jax.ShapeDtypeStruct((SPAN, 192), BF16)],
+        scratch_shapes=[pltpu.VMEM((SPAN, 896), F32)],
         compiler_params=PARAMS,
         name="local",
-    )(proj, cosine, sine, decay, decay_row)
+    )(own_part, came_part, cosine, sine, decay, decay_row)
     out_own = w_own[:, 896:1280]
     out_oth = swapped_cores(out_own).reshape(64, 16, 384)
     out_own = out_own.reshape(64, 16, 384)

time: 241 us -> 240 us (level)
  no operation moved by 1% of the time
where the time goes in v11:
time: 240 us; the launch traced here: 239 us
  waiting for transfers between devices  103 us (43%)
  starting transfers between devices  41.5 us (17%)
  Pallas kernels  37.2 us (16%)
  blocking collectives  15.4 us (6%)
  local copies, waits for them, and re-layouts  14.9 us (6%)
  between operations  14.5 us (6%)
  other arithmetic  12.5 us (5%)
    all_gather x1, waiting for transfers between devices, body(): w_own = lax.all_gather(w_row, 'z', axis=0, tiled=True)  35.3 us
    all_gather x1, waiting for transfers between devices, body(): queries = lax.all_gather(q_send, 'z', axis=0)  24.2 us
    pallas_call x1, Pallas kernels, body(): pl.pallas_call(attend_kernel, in_specs=[SMEM] * 2 + [VMEM] * 5, out_specs...  17 us
    all_to_all x3, starting transfers between devices, copies_from(): return lax.all_to_all(copies, axis, split_axis=0, concat_axis=0, tiled=True)  16.4 us
    all_to_all x3, waiting for transfers between devices, copies_from(): return lax.all_to_all(copies, axis, split_axis=0, concat_axis=0, tiled=True)  15.5 us
    all_to_all x1, blocking collectives, body(): shares = lax.all_to_all(share.reshape(4, 64, 2048), 'tp', 0, 0, tiled=True)  15.4 us
    all_to_all x1, waiting for transfers between devices, body(): parts = lax.all_to_all(partial, 'z', 0, 0, tiled=True)  13.6 us
    all_to_all x1, waiting for transfers between devices, body(): kv_own = lax.all_to_all(kv_send, 'y', 0, 0, tiled=True)  10.4 us
  transfers between devices with their start and end apart: 13, of which 8 were waited for; matrix products, arithmetic and copies ran while one was open for 8% of the time, Pallas kernels for 5%

profile of v11, /device:TPU:56, one launch (start us, length us, event | category | flops | bytes accessed | tf_op | source)
XLA Modules:
  0.0 238.9 jit_solution(18039556390861717357)
XLA Ops:
  9.1 8.5 %all-to-all-start = ((bf16[8,16,1408]{2,1,0:T(8,128)(2,1)}), bf16[8,16,1408]{2,1,0:T(8,128)(2,1)S(1)}, u32[]{:S(2)}, u32[]{:S(2)}) async-start(bf16[8,16,1408]{2,1,0:T(8,128)(2,1)} %broadcast_in_dim.165), calls=%async_computation | async-start | bytes 720896 | tf_op jit(solution)/shard_map/all_to_all | solution.py:27
  19.7 6.9 %all-to-all-done = bf16[8,16,1408]{2,1,0:T(8,128)(2,1)S(1)} async-done(((bf16[8,16,1408]{2,1,0:T(8,128)(2,1)}), bf16[8,16,1408]{2,1,0:T(8,128)(2,1)S(1)}, u32[]{:S(2)}, u32[]{:S(2)}) %all-to-all-start) | async-done | bytes 360480 | tf_op jit(solution)/shard_map/all_to_all | solution.py:27
  27.7 3.6 %all-to-all-start.2 = ((bf16[4,2,64,1024]{3,2,1,0:T(8,128)(2,1)}), bf16[4,2,64,1024]{3,2,1,0:T(8,128)(2,1)S(1)}, u32[]{:S(2)}, u32[]{:S(2)}) async-start(bf16[4,2,64,1024]{3,2,1,0:T(8,128)(2,1)} %broadcast_in_dim.177), calls=%async_computation.2 | async-start | bytes 2097152 | tf_op jit(solution)/shard_map/all_to_all | solution.py:27
  34.6 8.6 %all-to-all-done.2 = bf16[4,2,64,1024]{3,2,1,0:T(8,128)(2,1)S(1)} async-done(((bf16[4,2,64,1024]{3,2,1,0:T(8,128)(2,1)}), bf16[4,2,64,1024]{3,2,1,0:T(8,128)(2,1)S(1)}, u32[]{:S(2)}, u32[]{:S(2)}) %all-to-all-start.2) | async-done | bytes 1048608 | tf_op jit(solution)/shard_map/all_to_all | solution.py:27
  43.2 1.9 collective-permute-start.1
  48.1 35.3 %all-gather.4.cloned.1.call-done.weights = bf16[1024,1280]{1,0:T(8,128)(2,1)} async-done(((bf16[128,1280]{1,0:T(8,128)(2,1)}), bf16[1024,1280]{1,0:T(8,128)(2,1)}) %all-gather.4.cloned.1.call-update) | async-done | bytes 2621456 | tf_op jit(solution)/shard_map/all_gather | solution.py:294
  83.4 4.2 %project.1 = (f32[256,896]{1,0:T(8,128)}, f32[256,896]{1,0:T(8,128)}) custom-call(bf16[512,1024]{1,0:T(8,128)(2,1)} %pad_maximum_fusion.rows, bf16[1024,1280]{1,0:T(8,128)(2,1)} %all-gather.4.cloned.1.call-done.weights), custom_call_target="tpu_custom_call" | custom-call | tf_op jit(solution)/shard_map/project/pallas_call | solution.py:378
  87.6 1.9 collective-permute-start.2
  92.9 4.3 %all-to-all-start.1 = ((f32[8,8,3]{1,2,0:T(4,128)}), f32[8,8,3]{1,2,0:T(4,128)S(1)}, u32[]{:S(2)}, u32[]{:S(2)}) async-start(f32[8,8,3]{1,2,0:T(4,128)} %broadcast_in_dim.166), calls=%async_computation.1 | async-start | bytes 32768 | tf_op jit(solution)/shard_map/all_to_all | solution.py:27
  98.1 2.0 share.1
  100.1 5.1 %collective-permute-start.3 = (bf16[256,128]{1,0:T(8,128)(2,1)}, bf16[256,128]{1,0:T(8,128)(2,1)S(1)}, u32[]{:S(2)}, u32[]{:S(2)}) collective-permute-start(bf16[256,128]{1,0:T(8,128)(2,1)} %get-tuple-element.14), channel_id=1, source_target_pairs={{0,0},{8,456},{16,16},{24,472},{32,32},{40,488},{48,48},{56,504},{... | collective-permute-start | bytes 196616 | tf_op jit(solution)/shard_map/ppermute | solution.py:402
  106.7 3.4 %front.1.states = bf16[96,128]{1,0:T(8,128)(2,1)} custom-call(f32[256,896]{1,0:T(8,128)} %get-tuple-element.11.first_part, f32[256,896]{1,0:T(8,128)} %copy-done, f32[256,32]{1,0:T(8,128)} %get-tuple-element.31.cosine, f32[256,32]{1,0:T(8,128)} %get-tuple-element.30.sine, f32[256,3]{1,0:T(8,128)} %copy.156.decay), custom_call_target="tpu_custom_call" | custom-call | tf_op jit(solution)/shard_map/front/pallas_call | solution.py:403
  112.5 6.3 %all-to-all-start.3 = ((bf16[8,352,128]{2,1,0:T(8,128)(2,1)}), bf16[8,352,128]{2,1,0:T(8,128)(2,1)S(1)}, u32[]{:S(2)}, u32[]{:S(2)}) async-start(bf16[8,352,128]{2,1,0:T(8,128)(2,1)} %spread.1), calls=%async_computation.3 | async-start | bytes 1441792 | tf_op jit(solution)/shard_map/all_to_all | solution.py:420
  122.2 1.9 collective-permute-start
  125.8 10.4 %all-to-all-done.3.kv_own = bf16[8,352,128]{2,1,0:T(8,128)(2,1)S(1)} async-done(((bf16[8,352,128]{2,1,0:T(8,128)(2,1)}), bf16[8,352,128]{2,1,0:T(8,128)(2,1)S(1)}, u32[]{:S(2)}, u32[]{:S(2)}) %all-to-all-start.3) | async-done | bytes 720928 | tf_op jit(solution)/shard_map/all_to_all | solution.py:420
  136.2 1.9 collective-permute-start.4
  139.4 24.2 %all-gather.6.cloned.1.call-done = bf16[2048,256]{1,0:T(8,128)(2,1)} async-done(((bf16[256,256]{1,0:T(8,128)(2,1)}), bf16[2048,256]{1,0:T(8,128)(2,1)}) %all-gather.6.cloned.1.call-update) | async-done | bytes 1048592 | tf_op jit(solution)/shard_map/all_gather | solution.py:401
  164.5 17.0 %attend.1 = bf16[8,256,256]{2,1,0:T(8,128)(2,1)} custom-call(s32[68]{0:T(128)} %concatenate.29.plan, f32[120]{0:T(128)} %pad_maximum_fusion.2.fade, bf16[8,256,256]{2,1,0:T(8,128)(2,1)} %bitcast.70, bf16[8,3,64,256]{3,2,1,0:T(8,128)(2,1)} %maximum_maximum_fusion.query_gate, bf16[8,352,128]{2,1,0:T(8,128)(2,1)} %copy-done.2, bf16[8,352,128]{2,1,0:T(8,128)(2,1)} %copy-done.3, ...), custom_call_target="tpu_custom_call" | custom-call | tf_op jit(solution)/shard_map/attend/pallas_call | solution.py:438
  181.5 4.1 %all-to-all-start.4 = ((bf16[8,256,256]{2,1,0:T(8,128)(2,1)}), bf16[8,256,256]{2,1,0:T(8,128)(2,1)S(1)}, u32[]{:S(2)}, u32[]{:S(2)}) async-start(bf16[8,256,256]{2,1,0:T(8,128)(2,1)} %attend.1), calls=%async_computation.4 | async-start | bytes 2097152 | tf_op jit(solution)/shard_map/all_to_all | solution.py:454
  186.8 1.9 collective-permute-start.5
  192.4 4.3 %local.1 = (f32[256,192]{1,0:T(8,128)}, bf16[256,192]{1,0:T(8,128)(2,1)}) custom-call(f32[256,896]{1,0:T(8,128)} %get-tuple-element.11.first_part, f32[256,896]{1,0:T(8,128)} %copy-done, f32[256,32]{1,0:T(8,128)} %get-tuple-element.31.cosine, f32[256,32]{1,0:T(8,128)} %get-tuple-element.30.sine, f32[256,3]{1,0:T(8,128)} %copy.156.decay, f32[8,256]{1,0:T(8,128)} %pad.9.decay_row), custom_call_target="tpu_custom_call" | custom-call | tf_op jit(solution)/shard_map/local/pallas_call | solution.py:422
  196.7 13.6 %all-to-all-done.4.parts = bf16[8,256,256]{2,1,0:T(8,128)(2,1)S(1)} async-done(((bf16[8,256,256]{2,1,0:T(8,128)(2,1)}), bf16[8,256,256]{2,1,0:T(8,128)(2,1)S(1)}, u32[]{:S(2)}, u32[]{:S(2)}) %all-to-all-start.4) | async-done | bytes 1048608 | tf_op jit(solution)/shard_map/all_to_all | solution.py:454
  211.2 4.5 %back.1 = bf16[256,2048]{1,0:T(8,128)(2,1)} custom-call(bf16[8,256,256]{2,1,0:T(8,128)(2,1)} %copy-done.1, f32[256,192]{1,0:T(8,128)} %get-tuple-element.15.local, bf16[256,192]{1,0:T(8,128)(2,1)} %get-tuple-element.16.lifted, bf16[2048,384]{1,0:T(8,128)(2,1)} %bitcast.63), custom_call_target="tpu_custom_call" | custom-call | tf_op jit(solution)/shard_map/back/pallas_call | solution.py:456
  215.8 15.4 %all_to_all.30 = bf16[4,64,2048]{2,1,0:T(8,128)(2,1)S(1)} all-to-all(bf16[4,64,2048]{2,1,0:T(8,128)(2,1)} %bitcast.64), channel_id=1, replica_groups=mesh['z'=8,'y'=8,'c'=2,'tp'=4] {'tp'}, dimensions={0} | all-to-all | bytes 2097152 | tf_op jit(solution)/shard_map/all_to_all | solution.py:466
  (127 shorter events, 33.2 us)
Async XLA Ops:
  6.5 12.6 %copy-start.7 = (f32[2048]{0:T(1024)S(1)}, f32[2048]{0:T(1024)}, u32[]{:S(2)}) copy-start(f32[2048]{0:T(1024)} %param.13) | copy-start | bytes 24580
  9.1 17.5 %all-to-all-start = ((bf16[8,16,1408]{2,1,0:T(8,128)(2,1)}), bf16[8,16,1408]{2,1,0:T(8,128)(2,1)S(1)}, u32[]{:S(2)}, u32[]{:S(2)}) async-start(bf16[8,16,1408]{2,1,0:T(8,128)(2,1)} %broadcast_in_dim.165), calls=%async_computation | async-start | bytes 720896 | tf_op jit(solution)/shard_map/all_to_all | solution.py:27
  27.7 4.5 %copy-start.4 = (f32[3,32768]{1,0:T(4,128)S(1)}, f32[3,32768]{1,0:T(4,128)}, u32[]{:S(2)}) copy-start(f32[3,32768]{1,0:T(4,128)} %param.23) | copy-start | bytes 1179652
  27.7 15.4 %all-to-all-start.2 = ((bf16[4,2,64,1024]{3,2,1,0:T(8,128)(2,1)}), bf16[4,2,64,1024]{3,2,1,0:T(8,128)(2,1)S(1)}, u32[]{:S(2)}, u32[]{:S(2)}) async-start(bf16[4,2,64,1024]{3,2,1,0:T(8,128)(2,1)} %broadcast_in_dim.177), calls=%async_computation.2 | async-start | bytes 2097152 | tf_op jit(solution)/shard_map/all_to_all | solution.py:27
  31.4 52.0 %all-gather.4.cloned.1.call-start = ((), (), s32[]{:S(2)}) async-start(), calls=%async_computation.6 | async-start | bytes 2949120 | tf_op jit(solution)/shard_map/all_gather | solution.py:294
  43.2 3.8 %collective-permute-start.1 = (bf16[256,1024]{1,0:T(8,128)(2,1)S(1)}, bf16[256,1024]{1,0:T(8,128)(2,1)S(1)}, u32[]{:S(2)}, u32[]{:S(2)}) collective-permute-start(bf16[256,1024]{1,0:T(8,128)(2,1)S(1)} %bitcast.72), channel_id=1, source_target_pairs={{0,4},{4,0},{1,5},{5,1},{2,6},{6,2},{3,7},{7,3},{8,12},{12,8},{9,1... | collective-permute-start | bytes 1572872 | tf_op jit(solution)/shard_map/ppermute | solution.py:31
  48.1 41.4 %copy-start.6 = (f32[256,3]{0,1:T(4,128)S(1)}, f32[256,3]{0,1:T(4,128)}, u32[]{:S(2)}) copy-start(f32[256,3]{0,1:T(4,128)} %param.22) | copy-start | bytes 9220
  87.6 9.6 %collective-permute-start.2 = (f32[256,896]{1,0:T(8,128)}, f32[256,896]{1,0:T(8,128)S(1)}, u32[]{:S(2)}, u32[]{:S(2)}) collective-permute-start(f32[256,896]{1,0:T(8,128)} %get-tuple-element.12), channel_id=1, source_target_pairs={{0,4},{4,0},{1,5},{5,1},{2,6},{6,2},{3,7},{7,3},{8,12},{12,8},{9,1... | collective-permute-start | bytes 2752520 | tf_op jit(solution)/shard_map/ppermute | solution.py:31
  92.9 19.7 %all-to-all-start.1 = ((f32[8,8,3]{1,2,0:T(4,128)}), f32[8,8,3]{1,2,0:T(4,128)S(1)}, u32[]{:S(2)}, u32[]{:S(2)}) async-start(f32[8,8,3]{1,2,0:T(4,128)} %broadcast_in_dim.166), calls=%async_computation.1 | async-start | bytes 32768 | tf_op jit(solution)/shard_map/all_to_all | solution.py:27
  97.2 0.9 copy-start
  100.1 10.0 %collective-permute-start.3 = (bf16[256,128]{1,0:T(8,128)(2,1)}, bf16[256,128]{1,0:T(8,128)(2,1)S(1)}, u32[]{:S(2)}, u32[]{:S(2)}) collective-permute-start(bf16[256,128]{1,0:T(8,128)(2,1)} %get-tuple-element.14), channel_id=1, source_target_pairs={{0,0},{8,456},{16,16},{24,472},{32,32},{40,488},{48,48},{56,504},{... | collective-permute-start | bytes 196616 | tf_op jit(solution)/shard_map/ppermute | solution.py:402
  110.1 0.6 copy-start.5
  112.5 23.6 %all-to-all-start.3 = ((bf16[8,352,128]{2,1,0:T(8,128)(2,1)}), bf16[8,352,128]{2,1,0:T(8,128)(2,1)S(1)}, u32[]{:S(2)}, u32[]{:S(2)}) async-start(bf16[8,352,128]{2,1,0:T(8,128)(2,1)} %spread.1), calls=%async_computation.3 | async-start | bytes 1441792 | tf_op jit(solution)/shard_map/all_to_all | solution.py:420
  118.8 44.8 %all-gather.6.cloned.1.call-start = ((), (), s32[]{:S(2)}) async-start(), calls=%async_computation.7 | async-start | bytes 1179648 | tf_op jit(solution)/shard_map/all_gather | solution.py:401
  122.2 3.2 %collective-permute-start = (f32[8,8,3]{1,2,0:T(4,128)S(1)}, f32[8,8,3]{1,2,0:T(4,128)S(1)}, u32[]{:S(2)}, u32[]{:S(2)}) collective-permute-start(f32[8,8,3]{1,2,0:T(4,128)S(1)} %all-to-all-done.1), channel_id=1, source_target_pairs={{0,4},{4,0},{1,5},{5,1},{2,6},{6,2},{3,7},{7,3},{8,12},{12,8},{9,1... | collective-permute-start | bytes 2312 | tf_op jit(solution)/shard_map/ppermute | solution.py:31
  136.2 27.4 %copy-start.2 = (bf16[8,352,128]{2,1,0:T(8,128)(2,1)}, bf16[8,352,128]{2,1,0:T(8,128)(2,1)S(1)}, u32[]{:S(2)}) copy-start(bf16[8,352,128]{2,1,0:T(8,128)(2,1)S(1)} %all-to-all-done.3.kv_own) | copy-start | bytes 2162692
  136.2 27.4 %collective-permute-start.4 = (bf16[8,352,128]{2,1,0:T(8,128)(2,1)S(1)}, bf16[8,352,128]{2,1,0:T(8,128)(2,1)S(1)}, u32[]{:S(2)}, u32[]{:S(2)}) collective-permute-start(bf16[8,352,128]{2,1,0:T(8,128)(2,1)S(1)} %all-to-all-done.3.kv_own), channel_id=1, source_target_pairs={{0,4},{4,0},{1,5},{5,1},{2,6},{6,2},{3,7},{7,3},{8,12},{12,8},{9,1... | collective-permute-start | bytes 2162696 | tf_op jit(solution)/shard_map/ppermute | solution.py:31
  163.6 0.9 copy-start.3
  181.5 28.8 %all-to-all-start.4 = ((bf16[8,256,256]{2,1,0:T(8,128)(2,1)}), bf16[8,256,256]{2,1,0:T(8,128)(2,1)S(1)}, u32[]{:S(2)}, u32[]{:S(2)}) async-start(bf16[8,256,256]{2,1,0:T(8,128)(2,1)} %attend.1), calls=%async_computation.4 | async-start | bytes 2097152 | tf_op jit(solution)/shard_map/all_to_all | solution.py:454
  186.8 4.2 %collective-permute-start.5 = (bf16[1024,384]{1,0:T(8,128)(2,1)S(1)}, bf16[1024,384]{1,0:T(8,128)(2,1)S(1)}, u32[]{:S(2)}, u32[]{:S(2)}) collective-permute-start(bf16[1024,384]{1,0:T(8,128)(2,1)S(1)} %slice.35), channel_id=1, source_target_pairs={{0,4},{4,0},{1,5},{5,1},{2,6},{6,2},{3,7},{7,3},{8,12},{12,8},{9,1... | collective-permute-start | bytes 2359304 | tf_op jit(solution)/shard_map/ppermute | solution.py:31
  210.3 1.0 copy-start.1
Sparse Core Ops, SparseCore 0:
  34.3 49.0 all-gather.3
  121.7 41.8 all-gather.5

commit v12 on v11

--- a/solution.py
+++ b/solution.py
@@ -172,13 +172,18 @@
             score(first + 2, even, h)
             weigh(first + 1, odd, h)
 
-    def four(i, carry):
-        advance(4 * i)
-        advance(4 * i + 2)
+    def eight(i, carry):
+        for k in range(0, 8, 2):
+            advance(8 * i + k)
         return carry
 
     count = plan[65]
-    lax.fori_loop(0, count // 4, four, 0)
+    lax.fori_loop(0, count // 8, eight, 0)
+
+    @pl.when(count % 8 >= 4)
+    def _():
+        advance(count // 8 * 8)
+        advance(count // 8 * 8 + 2)
 
     @pl.when(count % 4 >= 2)
     def _():

time: 240 us -> 239 us (level)
  no operation moved by 1% of the time
where the time goes in v12:
time: 239 us; the launch traced here: 238 us
  waiting for transfers between devices  103 us (43%)
  starting transfers between devices  41.5 us (17%)
  Pallas kernels  36.5 us (15%)
  blocking collectives  15.4 us (6%)
  local copies, waits for them, and re-layouts  14.9 us (6%)
  between operations  14.5 us (6%)
  other arithmetic  12.5 us (5%)
    all_gather x1, waiting for transfers between devices, body(): w_own = lax.all_gather(w_row, 'z', axis=0, tiled=True)  35.3 us
    all_gather x1, waiting for transfers between devices, body(): queries = lax.all_gather(q_send, 'z', axis=0)  24.2 us
    all_to_all x3, starting transfers between devices, copies_from(): return lax.all_to_all(copies, axis, split_axis=0, concat_axis=0, tiled=True)  16.4 us
    pallas_call x1, Pallas kernels, body(): pl.pallas_call(attend_kernel, in_specs=[SMEM] * 2 + [VMEM] * 5, out_specs...  16.4 us
    all_to_all x3, waiting for transfers between devices, copies_from(): return lax.all_to_all(copies, axis, split_axis=0, concat_axis=0, tiled=True)  15.5 us
    all_to_all x1, blocking collectives, body(): shares = lax.all_to_all(share.reshape(4, 64, 2048), 'tp', 0, 0, tiled=True)  15.4 us
    all_to_all x1, waiting for transfers between devices, body(): parts = lax.all_to_all(partial, 'z', 0, 0, tiled=True)  13.6 us
    all_to_all x1, waiting for transfers between devices, body(): kv_own = lax.all_to_all(kv_send, 'y', 0, 0, tiled=True)  10.4 us
  transfers between devices with their start and end apart: 13, of which 8 were waited for; matrix products, arithmetic and copies ran while one was open for 8% of the time, Pallas kernels for 5%

profile of v12, /device:TPU:56, one launch (start us, length us, event | category | flops | bytes accessed | tf_op | source)
XLA Modules:
  0.0 238.3 jit_solution(5874298837191021862)
XLA Ops:
  9.1 8.5 %all-to-all-start = ((bf16[8,16,1408]{2,1,0:T(8,128)(2,1)}), bf16[8,16,1408]{2,1,0:T(8,128)(2,1)S(1)}, u32[]{:S(2)}, u32[]{:S(2)}) async-start(bf16[8,16,1408]{2,1,0:T(8,128)(2,1)} %broadcast_in_dim.165), calls=%async_computation | async-start | bytes 720896 | tf_op jit(solution)/shard_map/all_to_all | solution.py:27
  19.7 6.9 %all-to-all-done = bf16[8,16,1408]{2,1,0:T(8,128)(2,1)S(1)} async-done(((bf16[8,16,1408]{2,1,0:T(8,128)(2,1)}), bf16[8,16,1408]{2,1,0:T(8,128)(2,1)S(1)}, u32[]{:S(2)}, u32[]{:S(2)}) %all-to-all-start) | async-done | bytes 360480 | tf_op jit(solution)/shard_map/all_to_all | solution.py:27
  27.7 3.6 %all-to-all-start.2 = ((bf16[4,2,64,1024]{3,2,1,0:T(8,128)(2,1)}), bf16[4,2,64,1024]{3,2,1,0:T(8,128)(2,1)S(1)}, u32[]{:S(2)}, u32[]{:S(2)}) async-start(bf16[4,2,64,1024]{3,2,1,0:T(8,128)(2,1)} %broadcast_in_dim.177), calls=%async_computation.2 | async-start | bytes 2097152 | tf_op jit(solution)/shard_map/all_to_all | solution.py:27
  34.6 8.6 %all-to-all-done.2 = bf16[4,2,64,1024]{3,2,1,0:T(8,128)(2,1)S(1)} async-done(((bf16[4,2,64,1024]{3,2,1,0:T(8,128)(2,1)}), bf16[4,2,64,1024]{3,2,1,0:T(8,128)(2,1)S(1)}, u32[]{:S(2)}, u32[]{:S(2)}) %all-to-all-start.2) | async-done | bytes 1048608 | tf_op jit(solution)/shard_map/all_to_all | solution.py:27
  43.2 1.9 collective-permute-start.1
  48.1 35.3 %all-gather.4.cloned.1.call-done.weights = bf16[1024,1280]{1,0:T(8,128)(2,1)} async-done(((bf16[128,1280]{1,0:T(8,128)(2,1)}), bf16[1024,1280]{1,0:T(8,128)(2,1)}) %all-gather.4.cloned.1.call-update) | async-done | bytes 2621456 | tf_op jit(solution)/shard_map/all_gather | solution.py:299
  83.4 4.2 %project.1 = (f32[256,896]{1,0:T(8,128)}, f32[256,896]{1,0:T(8,128)}) custom-call(bf16[512,1024]{1,0:T(8,128)(2,1)} %pad_maximum_fusion.rows, bf16[1024,1280]{1,0:T(8,128)(2,1)} %all-gather.4.cloned.1.call-done.weights), custom_call_target="tpu_custom_call" | custom-call | tf_op jit(solution)/shard_map/project/pallas_call | solution.py:383
  87.6 1.9 collective-permute-start.2
  92.9 4.3 %all-to-all-start.1 = ((f32[8,8,3]{1,2,0:T(4,128)}), f32[8,8,3]{1,2,0:T(4,128)S(1)}, u32[]{:S(2)}, u32[]{:S(2)}) async-start(f32[8,8,3]{1,2,0:T(4,128)} %broadcast_in_dim.166), calls=%async_computation.1 | async-start | bytes 32768 | tf_op jit(solution)/shard_map/all_to_all | solution.py:27
  98.1 2.0 share.1
  100.1 5.1 %collective-permute-start.3 = (bf16[256,128]{1,0:T(8,128)(2,1)}, bf16[256,128]{1,0:T(8,128)(2,1)S(1)}, u32[]{:S(2)}, u32[]{:S(2)}) collective-permute-start(bf16[256,128]{1,0:T(8,128)(2,1)} %get-tuple-element.14), channel_id=1, source_target_pairs={{0,0},{8,456},{16,16},{24,472},{32,32},{40,488},{48,48},{56,504},{... | collective-permute-start | bytes 196616 | tf_op jit(solution)/shard_map/ppermute | solution.py:407
  106.7 3.4 %front.1.states = bf16[96,128]{1,0:T(8,128)(2,1)} custom-call(f32[256,896]{1,0:T(8,128)} %get-tuple-element.11.first_part, f32[256,896]{1,0:T(8,128)} %copy-done, f32[256,32]{1,0:T(8,128)} %get-tuple-element.31.cosine, f32[256,32]{1,0:T(8,128)} %get-tuple-element.30.sine, f32[256,3]{1,0:T(8,128)} %copy.156.decay), custom_call_target="tpu_custom_call" | custom-call | tf_op jit(solution)/shard_map/front/pallas_call | solution.py:408
  112.5 6.3 %all-to-all-start.3 = ((bf16[8,352,128]{2,1,0:T(8,128)(2,1)}), bf16[8,352,128]{2,1,0:T(8,128)(2,1)S(1)}, u32[]{:S(2)}, u32[]{:S(2)}) async-start(bf16[8,352,128]{2,1,0:T(8,128)(2,1)} %spread.1), calls=%async_computation.3 | async-start | bytes 1441792 | tf_op jit(solution)/shard_map/all_to_all | solution.py:425
  122.2 1.9 collective-permute-start
  125.8 10.4 %all-to-all-done.3.kv_own = bf16[8,352,128]{2,1,0:T(8,128)(2,1)S(1)} async-done(((bf16[8,352,128]{2,1,0:T(8,128)(2,1)}), bf16[8,352,128]{2,1,0:T(8,128)(2,1)S(1)}, u32[]{:S(2)}, u32[]{:S(2)}) %all-to-all-start.3) | async-done | bytes 720928 | tf_op jit(solution)/shard_map/all_to_all | solution.py:425
  136.2 1.9 collective-permute-start.4
  139.4 24.2 %all-gather.6.cloned.1.call-done = bf16[2048,256]{1,0:T(8,128)(2,1)} async-done(((bf16[256,256]{1,0:T(8,128)(2,1)}), bf16[2048,256]{1,0:T(8,128)(2,1)}) %all-gather.6.cloned.1.call-update) | async-done | bytes 1048592 | tf_op jit(solution)/shard_map/all_gather | solution.py:406
  164.5 16.4 %attend.1 = bf16[8,256,256]{2,1,0:T(8,128)(2,1)} custom-call(s32[68]{0:T(128)} %concatenate.29.plan, f32[120]{0:T(128)} %pad_maximum_fusion.2.fade, bf16[8,256,256]{2,1,0:T(8,128)(2,1)} %bitcast.70, bf16[8,3,64,256]{3,2,1,0:T(8,128)(2,1)} %maximum_maximum_fusion.query_gate, bf16[8,352,128]{2,1,0:T(8,128)(2,1)} %copy-done.2, bf16[8,352,128]{2,1,0:T(8,128)(2,1)} %copy-done.3, ...), custom_call_target="tpu_custom_call" | custom-call | tf_op jit(solution)/shard_map/attend/pallas_call | solution.py:443
  180.9 4.1 %all-to-all-start.4 = ((bf16[8,256,256]{2,1,0:T(8,128)(2,1)}), bf16[8,256,256]{2,1,0:T(8,128)(2,1)S(1)}, u32[]{:S(2)}, u32[]{:S(2)}) async-start(bf16[8,256,256]{2,1,0:T(8,128)(2,1)} %attend.1), calls=%async_computation.4 | async-start | bytes 2097152 | tf_op jit(solution)/shard_map/all_to_all | solution.py:459
  186.2 1.9 collective-permute-start.5
  191.8 4.3 %local.1 = (f32[256,192]{1,0:T(8,128)}, bf16[256,192]{1,0:T(8,128)(2,1)}) custom-call(f32[256,896]{1,0:T(8,128)} %get-tuple-element.11.first_part, f32[256,896]{1,0:T(8,128)} %copy-done, f32[256,32]{1,0:T(8,128)} %get-tuple-element.31.cosine, f32[256,32]{1,0:T(8,128)} %get-tuple-element.30.sine, f32[256,3]{1,0:T(8,128)} %copy.156.decay, f32[8,256]{1,0:T(8,128)} %pad.9.decay_row), custom_call_target="tpu_custom_call" | custom-call | tf_op jit(solution)/shard_map/local/pallas_call | solution.py:427
  196.0 13.6 %all-to-all-done.4.parts = bf16[8,256,256]{2,1,0:T(8,128)(2,1)S(1)} async-done(((bf16[8,256,256]{2,1,0:T(8,128)(2,1)}), bf16[8,256,256]{2,1,0:T(8,128)(2,1)S(1)}, u32[]{:S(2)}, u32[]{:S(2)}) %all-to-all-start.4) | async-done | bytes 1048608 | tf_op jit(solution)/shard_map/all_to_all | solution.py:459
  210.6 4.5 %back.1 = bf16[256,2048]{1,0:T(8,128)(2,1)} custom-call(bf16[8,256,256]{2,1,0:T(8,128)(2,1)} %copy-done.1, f32[256,192]{1,0:T(8,128)} %get-tuple-element.15.local, bf16[256,192]{1,0:T(8,128)(2,1)} %get-tuple-element.16.lifted, bf16[2048,384]{1,0:T(8,128)(2,1)} %bitcast.63), custom_call_target="tpu_custom_call" | custom-call | tf_op jit(solution)/shard_map/back/pallas_call | solution.py:461
  215.1 15.4 %all_to_all.30 = bf16[4,64,2048]{2,1,0:T(8,128)(2,1)S(1)} all-to-all(bf16[4,64,2048]{2,1,0:T(8,128)(2,1)} %bitcast.64), channel_id=1, replica_groups=mesh['z'=8,'y'=8,'c'=2,'tp'=4] {'tp'}, dimensions={0} | all-to-all | bytes 2097152 | tf_op jit(solution)/shard_map/all_to_all | solution.py:471
  (127 shorter events, 33.2 us)
Async XLA Ops:
  6.5 12.6 %copy-start.7 = (f32[2048]{0:T(1024)S(1)}, f32[2048]{0:T(1024)}, u32[]{:S(2)}) copy-start(f32[2048]{0:T(1024)} %param.13) | copy-start | bytes 24580
  9.1 17.5 %all-to-all-start = ((bf16[8,16,1408]{2,1,0:T(8,128)(2,1)}), bf16[8,16,1408]{2,1,0:T(8,128)(2,1)S(1)}, u32[]{:S(2)}, u32[]{:S(2)}) async-start(bf16[8,16,1408]{2,1,0:T(8,128)(2,1)} %broadcast_in_dim.165), calls=%async_computation | async-start | bytes 720896 | tf_op jit(solution)/shard_map/all_to_all | solution.py:27
  27.7 4.5 %copy-start.4 = (f32[3,32768]{1,0:T(4,128)S(1)}, f32[3,32768]{1,0:T(4,128)}, u32[]{:S(2)}) copy-start(f32[3,32768]{1,0:T(4,128)} %param.23) | copy-start | bytes 1179652
  27.7 15.4 %all-to-all-start.2 = ((bf16[4,2,64,1024]{3,2,1,0:T(8,128)(2,1)}), bf16[4,2,64,1024]{3,2,1,0:T(8,128)(2,1)S(1)}, u32[]{:S(2)}, u32[]{:S(2)}) async-start(bf16[4,2,64,1024]{3,2,1,0:T(8,128)(2,1)} %broadcast_in_dim.177), calls=%async_computation.2 | async-start | bytes 2097152 | tf_op jit(solution)/shard_map/all_to_all | solution.py:27
  31.4 52.0 %all-gather.4.cloned.1.call-start = ((), (), s32[]{:S(2)}) async-start(), calls=%async_computation.6 | async-start | bytes 2949120 | tf_op jit(solution)/shard_map/all_gather | solution.py:299
  43.2 3.8 %collective-permute-start.1 = (bf16[256,1024]{1,0:T(8,128)(2,1)S(1)}, bf16[256,1024]{1,0:T(8,128)(2,1)S(1)}, u32[]{:S(2)}, u32[]{:S(2)}) collective-permute-start(bf16[256,1024]{1,0:T(8,128)(2,1)S(1)} %bitcast.72), channel_id=1, source_target_pairs={{0,4},{4,0},{1,5},{5,1},{2,6},{6,2},{3,7},{7,3},{8,12},{12,8},{9,1... | collective-permute-start | bytes 1572872 | tf_op jit(solution)/shard_map/ppermute | solution.py:31
  48.1 41.4 %copy-start.6 = (f32[256,3]{0,1:T(4,128)S(1)}, f32[256,3]{0,1:T(4,128)}, u32[]{:S(2)}) copy-start(f32[256,3]{0,1:T(4,128)} %param.22) | copy-start | bytes 9220
  87.6 9.6 %collective-permute-start.2 = (f32[256,896]{1,0:T(8,128)}, f32[256,896]{1,0:T(8,128)S(1)}, u32[]{:S(2)}, u32[]{:S(2)}) collective-permute-start(f32[256,896]{1,0:T(8,128)} %get-tuple-element.12), channel_id=1, source_target_pairs={{0,4},{4,0},{1,5},{5,1},{2,6},{6,2},{3,7},{7,3},{8,12},{12,8},{9,1... | collective-permute-start | bytes 2752520 | tf_op jit(solution)/shard_map/ppermute | solution.py:31
  92.9 19.7 %all-to-all-start.1 = ((f32[8,8,3]{1,2,0:T(4,128)}), f32[8,8,3]{1,2,0:T(4,128)S(1)}, u32[]{:S(2)}, u32[]{:S(2)}) async-start(f32[8,8,3]{1,2,0:T(4,128)} %broadcast_in_dim.166), calls=%async_computation.1 | async-start | bytes 32768 | tf_op jit(solution)/shard_map/all_to_all | solution.py:27
  97.2 0.9 copy-start
  100.1 10.0 %collective-permute-start.3 = (bf16[256,128]{1,0:T(8,128)(2,1)}, bf16[256,128]{1,0:T(8,128)(2,1)S(1)}, u32[]{:S(2)}, u32[]{:S(2)}) collective-permute-start(bf16[256,128]{1,0:T(8,128)(2,1)} %get-tuple-element.14), channel_id=1, source_target_pairs={{0,0},{8,456},{16,16},{24,472},{32,32},{40,488},{48,48},{56,504},{... | collective-permute-start | bytes 196616 | tf_op jit(solution)/shard_map/ppermute | solution.py:407
  110.1 0.6 copy-start.5
  112.5 23.6 %all-to-all-start.3 = ((bf16[8,352,128]{2,1,0:T(8,128)(2,1)}), bf16[8,352,128]{2,1,0:T(8,128)(2,1)S(1)}, u32[]{:S(2)}, u32[]{:S(2)}) async-start(bf16[8,352,128]{2,1,0:T(8,128)(2,1)} %spread.1), calls=%async_computation.3 | async-start | bytes 1441792 | tf_op jit(solution)/shard_map/all_to_all | solution.py:425
  118.8 44.8 %all-gather.6.cloned.1.call-start = ((), (), s32[]{:S(2)}) async-start(), calls=%async_computation.7 | async-start | bytes 1179648 | tf_op jit(solution)/shard_map/all_gather | solution.py:406
  122.2 3.2 %collective-permute-start = (f32[8,8,3]{1,2,0:T(4,128)S(1)}, f32[8,8,3]{1,2,0:T(4,128)S(1)}, u32[]{:S(2)}, u32[]{:S(2)}) collective-permute-start(f32[8,8,3]{1,2,0:T(4,128)S(1)} %all-to-all-done.1), channel_id=1, source_target_pairs={{0,4},{4,0},{1,5},{5,1},{2,6},{6,2},{3,7},{7,3},{8,12},{12,8},{9,1... | collective-permute-start | bytes 2312 | tf_op jit(solution)/shard_map/ppermute | solution.py:31
  136.2 27.4 %copy-start.2 = (bf16[8,352,128]{2,1,0:T(8,128)(2,1)}, bf16[8,352,128]{2,1,0:T(8,128)(2,1)S(1)}, u32[]{:S(2)}) copy-start(bf16[8,352,128]{2,1,0:T(8,128)(2,1)S(1)} %all-to-all-done.3.kv_own) | copy-start | bytes 2162692
  136.2 27.4 %collective-permute-start.4 = (bf16[8,352,128]{2,1,0:T(8,128)(2,1)S(1)}, bf16[8,352,128]{2,1,0:T(8,128)(2,1)S(1)}, u32[]{:S(2)}, u32[]{:S(2)}) collective-permute-start(bf16[8,352,128]{2,1,0:T(8,128)(2,1)S(1)} %all-to-all-done.3.kv_own), channel_id=1, source_target_pairs={{0,4},{4,0},{1,5},{5,1},{2,6},{6,2},{3,7},{7,3},{8,12},{12,8},{9,1... | collective-permute-start | bytes 2162696 | tf_op jit(solution)/shard_map/ppermute | solution.py:31
  163.6 0.9 copy-start.3
  180.9 28.8 %all-to-all-start.4 = ((bf16[8,256,256]{2,1,0:T(8,128)(2,1)}), bf16[8,256,256]{2,1,0:T(8,128)(2,1)S(1)}, u32[]{:S(2)}, u32[]{:S(2)}) async-start(bf16[8,256,256]{2,1,0:T(8,128)(2,1)} %attend.1), calls=%async_computation.4 | async-start | bytes 2097152 | tf_op jit(solution)/shard_map/all_to_all | solution.py:459
  186.2 4.2 %collective-permute-start.5 = (bf16[1024,384]{1,0:T(8,128)(2,1)S(1)}, bf16[1024,384]{1,0:T(8,128)(2,1)S(1)}, u32[]{:S(2)}, u32[]{:S(2)}) collective-permute-start(bf16[1024,384]{1,0:T(8,128)(2,1)S(1)} %slice.35), channel_id=1, source_target_pairs={{0,4},{4,0},{1,5},{5,1},{2,6},{6,2},{3,7},{7,3},{8,12},{12,8},{9,1... | collective-permute-start | bytes 2359304 | tf_op jit(solution)/shard_map/ppermute | solution.py:31
  209.6 1.0 copy-start.1
Sparse Core Ops, SparseCore 0:
  34.3 49.0 all-gather.3
  121.7 41.8 all-gather.5
